TPU v7x, 256 devices: a whole 4x4x8 slice. The times are simulated.
256 devices in a mesh: sp: 64 (over z, y, core), tp: 4 (over x).
Axes of the slice: x: 4, y: 4, z: 8, core: 2. Of those that a mesh axis runs over, the one named last changes fastest.
Arguments:
- queries: bfloat16 [8192, 1024], P('sp', 'tp'), may hold values from -600 to 600, as said below
- keys: bfloat16 [8192, 256], P('sp', 'tp'), may hold values from -6 to 6
- values: bfloat16 [8192, 256], P('sp', 'tp'), may hold values from -18 to 18
- forget_prefix_log: float32 [8192, 16], P('sp', 'tp'), as said below
- residual: bfloat16 [8192, 2048], P(('sp', 'tp')), may hold values from -6 to 6
- out_weight: bfloat16 [1024, 2048], replicated, may hold values from -0.1875 to 0.1875
- norm_gain: float32 [2048], replicated, may hold values from 0.1 to 1.9
- routes: int32 [8192, 2], P(('sp', 'tp')), may hold values from 0 to 63, all different within a row; in each aligned block of 32 rows (0 to 31, 32 to 63, ...) at most 2 rows name the same one
- route_weight: float32 [8192, 2], P(('sp', 'tp')), may hold values from 0.1 to 1
- w_gate: bfloat16 [64, 2048, 1024], P('sp', None, 'tp'), may hold values from -0.125 to 0.125
- w_up: bfloat16 [64, 2048, 1024], P('sp', None, 'tp'), may hold values from -0.125 to 0.125
- w_down: bfloat16 [64, 1024, 2048], P('sp', 'tp'), may hold values from -0.1875 to 0.1875
Outputs:
- layer_out: bfloat16 [8192, 2048], P(('sp', 'tp'))
Inputs may be any that keep to these rules, and one draw needn't show every extreme that they name: `queries`: queries are of order one except for a few positions. `forget_prefix_log`: never rising along positions. `routes`: within the rows of one device (32 positions in order), no expert is named by more than 2 rows, a bound that some block reaches; the experts of one row differ.
All inputs are finite; a program needn't handle non-finite values.
Results may differ from a plain program's by a relative error of at most 0.013.
Values may be sent and summed in bfloat16 or wider, within the bound.
No kernel may reach another device: no remote copies, remote signals or barrier semaphores. Data moves between devices by JAX's collectives and lax.ppermute only.
A program may use at most 64 MiB of HBM per device.

v0:
```python
import functools

import jax
import jax.numpy as jnp
from jax import lax
from jax.experimental import pallas as pl
from jax.experimental.pallas import tpu as pltpu
from jax.sharding import Mesh, PartitionSpec as P


NZ, NY, NC, NT = 8, 4, 2, 4
TOK = 128
HEAD = 64
HEADS = 4
ROW = 32
D = 2048
BLOCK = TOK + 16
GROUP = 2
BF16_MAX = 3.3895313892515355e38
NEG = -3.0e38
F32 = jnp.float32
BF16 = jnp.bfloat16
SP = ("z", "y", "c")
PARAMS = pltpu.CompilerParams(vmem_limit_bytes=24 * 1024 * 1024)


def in_hbm(x):
    return pltpu.with_memory_space_constraint(x, pltpu.HBM)


def in_vmem(x):
    return pltpu.with_memory_space_constraint(x, pltpu.VMEM)


def dot(a, b):
    return jnp.dot(a, b, preferred_element_type=F32)


def parts3(x):
    hi = jnp.clip(x, -BF16_MAX, BF16_MAX).astype(BF16)
    rest = x - hi.astype(F32)
    mid = rest.astype(BF16)
    low = (rest - mid.astype(F32)).astype(BF16)
    return hi, mid, low


def fetches(pairs, sems):
    return [pltpu.make_async_copy(src, dst, sems.at[i]) for i, (src, dst) in enumerate(pairs)]


def pack_kernel(keys_hbm, values_hbm, gates_hbm, out_ref, keys_ref, values_ref, gates_ref, sems):
    copies = fetches(
        [(gates_hbm, gates_ref), (keys_hbm, keys_ref), (values_hbm, values_ref)], sems
    )
    for copy in copies:
        copy.start()
    for copy in copies:
        copy.wait()
    hi, mid, low = parts3(gates_ref[...])
    rows = [hi.astype(F32), mid.astype(F32), low.astype(F32), jnp.zeros((4, TOK), F32)]
    gates = jnp.concatenate(rows, axis=0).astype(BF16)
    for z in range(NZ):
        out_ref[z, 0:HEAD, :] = keys_ref[...]
        out_ref[z, HEAD : HEAD + 16, :] = gates
        out_ref[z, HEAD + 16 : BLOCK, :] = values_ref[...]


def pack(keys, values, gates):
    hbm = pl.BlockSpec(memory_space=pltpu.HBM)
    return pl.pallas_call(
        pack_kernel,
        out_shape=jax.ShapeDtypeStruct((NZ, BLOCK, TOK), BF16),
        in_specs=[hbm] * 3,
        out_specs=pl.BlockSpec(memory_space=pltpu.VMEM),
        scratch_shapes=[
            pltpu.VMEM((HEAD, TOK), BF16),
            pltpu.VMEM((HEAD, TOK), BF16),
            pltpu.VMEM((HEADS, TOK), F32),
            pltpu.SemaphoreType.DMA((3,)),
        ],
        compiler_params=PARAMS,
        name="pack",
    )(in_hbm(keys), in_hbm(values), in_hbm(gates))


def query_rows(query_ref):
    col = lax.broadcasted_iota(jnp.int32, (TOK, 16), 1)
    rows = []
    for h in range(HEADS):
        part = query_ref[:, h * HEAD : (h + 1) * HEAD] * jnp.asarray(0.125, BF16)
        takes = (col % HEADS == h) & (col < 3 * HEADS) | (col == 3 * HEADS)
        rows.append(jnp.concatenate([part, jnp.where(takes, -1.0, 0.0).astype(BF16)], axis=1))
    return jnp.concatenate(rows, axis=0)


def attend_kernel(count, place_ref, query_hbm, source_ref, *refs):
    chunks, refs = refs[:count], refs[count:]
    out_ref, target_ref, m_ref, l_ref, acc_ref, query_ref, sems = refs
    fetch, copy = fetches([(query_hbm, query_ref), (source_ref, target_ref)], sems)
    fetch.start()
    copy.start()
    fetch.wait()
    own_z, own_order = place_ref[0], place_ref[1]
    queries = query_rows(query_ref)
    total_rows = HEADS * TOK
    blocks = GROUP * count
    row_of_gate = lax.broadcasted_iota(jnp.int32, (16, TOK), 0)

    def folded(weights):
        total = weights[:, 0:TOK]
        for j in range(1, blocks):
            total = total + weights[:, j * TOK : (j + 1) * TOK]
        return total

    def step(base, first):
        key_rows, value_rows, shifts = [], [], []
        for g in range(GROUP):
            for j, ref in enumerate(chunks):
                gates = ref[base + g, HEAD : HEAD + 16, :]
                if first:
                    order = place_ref[2 + j]
                    seen = (base + g < own_z) | ((base + g == own_z) & (order <= own_order))
                    bar = jnp.where(seen, 0.0, -NEG).astype(BF16)
                    gates = jnp.where(row_of_gate == 3 * HEADS, bar, gates)
                    shifts.append(jnp.where((base + g == own_z) & (order == own_order), 0, TOK))
                key_rows.append(jnp.concatenate([ref[base + g, 0:HEAD, :], gates], axis=0))
                value_rows.append(ref[base + g, HEAD + 16 : BLOCK, :])
        scores = dot(queries, jnp.concatenate(key_rows, axis=1))
        if first:
            ahead = lax.broadcasted_iota(jnp.int32, (total_rows, TOK), 0) % TOK
            ahead = ahead - lax.broadcasted_iota(jnp.int32, (total_rows, TOK), 1)
            pieces = []
            for i in range(blocks):
                piece = scores[:, i * TOK : (i + 1) * TOK]
                if i % count == 0:
                    piece = jnp.where(ahead + shifts[i] >= 0, piece, NEG)
                pieces.append(piece)
            scores = jnp.concatenate(pieces, axis=1)
        peak = jnp.max(scores, axis=1, keepdims=True)
        if first:
            peak = jnp.broadcast_to(peak, (total_rows, TOK))
        else:
            before = m_ref[...]
            peak = jnp.maximum(before, peak)
        weights = jnp.exp(scores - jnp.concatenate([peak] * blocks, axis=1))
        product = lax.dot_general(
            weights.astype(BF16),
            jnp.concatenate(value_rows, axis=1),
            (((1,), (1,)), ((), ())),
            preferred_element_type=F32,
        )
        m_ref[...] = peak
        if first:
            l_ref[...] = folded(weights)
            acc_ref[...] = product
        else:
            shrink = jnp.exp(before - peak)
            l_ref[...] = l_ref[...] * shrink + folded(weights)
            acc_ref[...] = acc_ref[...] * shrink[:, :HEAD] + product

    groups = own_z // GROUP
    step(groups * GROUP, True)

    def body(group, carry):
        step(group * GROUP, False)
        return carry

    lax.fori_loop(0, groups, body, 0)
    done = []
    for h in range(HEADS):
        here = slice(h * TOK, (h + 1) * TOK)
        total = jnp.sum(l_ref[here, :], axis=1, keepdims=True)
        done.append((acc_ref[here, :] / total).astype(BF16))
    out_ref[...] = jnp.concatenate(done, axis=1)
    copy.wait()


def attend(place, queries, weight, chunks):
    vmem = pl.BlockSpec(memory_space=pltpu.VMEM)
    total_rows = HEADS * TOK
    return pl.pallas_call(
        functools.partial(attend_kernel, len(chunks)),
        out_shape=[
            jax.ShapeDtypeStruct((TOK, HEADS * HEAD), BF16),
            jax.ShapeDtypeStruct(weight.shape, weight.dtype),
        ],
        in_specs=[pl.BlockSpec(memory_space=pltpu.SMEM)]
        + [pl.BlockSpec(memory_space=pltpu.HBM)] * 2
        + [vmem] * len(chunks),
        out_specs=[vmem] * 2,
        scratch_shapes=[
            pltpu.VMEM((total_rows, TOK), F32),
            pltpu.VMEM((total_rows, TOK), F32),
            pltpu.VMEM((total_rows, HEAD), F32),
            pltpu.VMEM(queries.shape, BF16),
            pltpu.SemaphoreType.DMA((2,)),
        ],
        compiler_params=PARAMS,
        name="attend",
    )(place, in_hbm(queries), in_hbm(weight), *map(in_vmem, chunks))


def picks(routes_ref, transposed_slots=128):
    slot = lax.broadcasted_iota(jnp.int32, (transposed_slots, ROW), 0)
    expert, rank = slot // 2, slot % 2
    named0 = routes_ref[0:1, :] == expert
    named1 = routes_ref[1:2, :] == expert
    named = jnp.where(named0 | named1, 1.0, 0.0)
    earlier = lax.broadcasted_iota(jnp.int32, (ROW, ROW), 0) < lax.broadcasted_iota(
        jnp.int32, (ROW, ROW), 1
    )
    before = dot(named.astype(BF16), jnp.where(earlier, 1.0, 0.0).astype(BF16))
    chosen = before == rank.astype(F32)
    return chosen & named0, chosen & named1


def project_kernel(att_ref, weight_ref, residual_ref, gain_ref, routes_ref, stream_ref, rows_ref):
    total = residual_ref[...].astype(F32)
    both = jnp.concatenate([att_ref[x] for x in range(NT)], axis=1)
    total = total + dot(both, weight_ref[...])
    stream_ref[...] = total
    mean_square = jnp.mean(total * total, axis=1, keepdims=True)
    normed = (total * lax.rsqrt(mean_square + 1e-06) * gain_ref[...]).astype(BF16)
    first, second = picks(routes_ref)
    pick = jnp.where(first | second, 1.0, 0.0).astype(BF16)
    rows_ref[...] = dot(pick, normed).astype(BF16)


def hidden(rows, gate_ref, up_ref):
    gate = dot(rows, gate_ref[...])
    up = dot(rows, up_ref[...])
    return (gate / (1.0 + jnp.exp(-gate)) * up).astype(BF16)


def near_kernel(own_ref, left_ref, right_ref, *refs):
    sources, (h_own, h_left, h_right), refs = refs[:6], refs[6:9], refs[9:]
    targets, sems = refs[:6], refs[6]
    copies = fetches(list(zip(sources, targets)), sems)
    for copy in copies:
        copy.start()
    copies[0].wait()
    copies[1].wait()
    for rows_ref, out_ref in ((own_ref, h_own), (left_ref, h_left), (right_ref, h_right)):
        out_ref[...] = hidden(rows_ref[...], targets[0], targets[1])
    for copy in copies[2:]:
        copy.wait()


def near(rows, weights):
    vmem = pl.BlockSpec(memory_space=pltpu.VMEM)
    shape = jax.ShapeDtypeStruct((TOK, weights[0].shape[1]), BF16)
    return pl.pallas_call(
        near_kernel,
        out_shape=[shape] * 3 + [jax.ShapeDtypeStruct(w.shape, w.dtype) for w in weights],
        in_specs=[vmem] * 3 + [pl.BlockSpec(memory_space=pltpu.HBM)] * 6,
        out_specs=[vmem] * 9,
        scratch_shapes=[pltpu.SemaphoreType.DMA((6,))],
        compiler_params=PARAMS,
        name="near",
    )(*rows, *map(in_hbm, weights))


def far_kernel(gate_ref, up_ref, far0_ref, far1_ref, out_ref):
    half = TOK // 2
    out_ref[:half, :] = hidden(far0_ref[...], gate_ref, up_ref)
    out_ref[half:, :] = hidden(far1_ref[...], gate_ref, up_ref)


def down_kernel(own_ref, left_ref, right_ref, far_ref, w_own, w_left, w_right, w_far, out_ref):
    total = dot(own_ref[...], w_own[...])
    total = total + dot(left_ref[...], w_left[...])
    total = total + dot(right_ref[...], w_right[...])
    out_ref[...] = (total + dot(far_ref[...], w_far[...])).astype(BF16)


def combine_kernel(stream_ref, routes_ref, weight_ref, back_ref, out_ref):
    first, second = picks(routes_ref)
    spread = jnp.where(first, weight_ref[0:1, :], 0.0) + jnp.where(second, weight_ref[1:2, :], 0.0)
    back = back_ref[...]
    total = stream_ref[...]
    for part in parts3(spread):
        total = total + lax.dot_general(
            part, back, (((0,), (0,)), ((), ())), preferred_element_type=F32
        )
    out_ref[...] = total.astype(BF16)


def call(kernel, shapes, *args):
    return pl.pallas_call(
        kernel, out_shape=[jax.ShapeDtypeStruct(s, t) for s, t in shapes], compiler_params=PARAMS
    )(*args)


def moved(x, axis, by):
    size = {"z": NZ, "y": NY, "c": NC, "tp": NT}[axis]
    return lax.ppermute(x, axis, [(i, (i + by) % size) for i in range(size)])


def shards(
    queries,
    keys,
    values,
    forget_prefix_log,
    residual,
    out_weight,
    norm_gain,
    routes,
    route_weight,
    w_gate,
    w_up,
    w_down,
):
    z, y, c = lax.axis_index("z"), lax.axis_index("y"), lax.axis_index("c")
    down_own = w_down[0]
    down_left, down_right = moved(down_own, "tp", 1), moved(down_own, "tp", -1)
    copies = pack(keys.T, values.T, forget_prefix_log.T)
    own = lax.all_to_all(copies, "z", 0, 0, tiled=True)
    chunks = [own, moved(own, "c", 1)]
    place = [z, y * NC + c, y * NC + c, y * NC + 1 - c]
    for step in (1, 3, 2):
        chunk = moved(own, "y", step)
        from_y = (y - step) % NY
        chunks += [chunk, moved(chunk, "c", 1)]
        place += [from_y * NC + c, from_y * NC + 1 - c]
    place = jnp.stack(place).astype(jnp.int32)
    attended, out_w = attend(place, queries, out_weight, chunks)

    heads = lax.all_to_all(attended.reshape(NT, ROW, -1), "tp", 0, 0, tiled=True)
    far_source, _ = lax.optimization_barrier((down_own, heads))
    down_far = moved(far_source, "tp", 2)
    routes_row = routes.T
    stream, rows = call(
        project_kernel,
        [((ROW, D), F32), ((TOK, D), BF16)],
        heads,
        out_w,
        residual,
        norm_gain.reshape(1, D),
        routes_row,
    )
    arrived = lax.all_to_all(rows.reshape(64, 2, D), SP, 0, 0, tiled=True).reshape(TOK, D)
    left, right = moved(arrived, "tp", 1), moved(arrived, "tp", -1)
    half = TOK // 2
    far0, far1 = moved(left[:half], "tp", 1), moved(right[half:], "tp", -1)
    h_own, h_left, h_right, gate_w, up_w, *down_w = near(
        (arrived, left, right),
        (w_gate[0], w_up[0], down_own, down_left, down_right, down_far),
    )
    (h_far,) = call(far_kernel, [(h_own.shape, BF16)], gate_w, up_w, far0, far1)
    (expert_out,) = call(
        down_kernel,
        [((TOK, D), BF16)],
        h_own,
        moved(h_right, "tp", 1),
        moved(h_left, "tp", -1),
        moved(h_far, "tp", 2),
        *down_w,
    )
    back = lax.all_to_all(expert_out.reshape(64, 2, D), SP, 0, 0, tiled=True).reshape(TOK, D)
    (out,) = call(
        combine_kernel, [((ROW, D), BF16)], stream, routes_row, route_weight.T, back
    )
    return out


def solution(mesh):
    split = Mesh(mesh.devices.reshape(NZ, NY, NC, NT), ("z", "y", "c", "tp"))
    rows = P(("z", "y", "c", "tp"), None)

    return jax.shard_map(
        shards,
        mesh=split,
        in_specs=(
            P(SP, "tp"),
            P(SP, "tp"),
            P(SP, "tp"),
            P(SP, "tp"),
            rows,
            P(),
            P(),
            rows,
            rows,
            P(SP, None, "tp"),
            P(SP, None, "tp"),
            P(SP, "tp", None),
        ),
        out_specs=rows,
        check_vma=False,
    )
```

profile of v0, /device:TPU:1, one launch (start us, length us, event | category | flops | bytes accessed | tf_op | source)
XLA Modules:
  0.0 174.3 jit_solution(11542766140396659098)
XLA Ops:
  0.9 19.8 %all_to_all.20.refs_0_ = bf16[8,144,128]{2,1,0:T(8,128)(2,1)S(1)} all-to-all(bf16[8,144,128]{2,1,0:T(8,128)(2,1)S(1)} %pack.1), channel_id=1, replica_groups=mesh['z'=8,'y'=4,'c'=2,'tp'=4] {'z'}, dimensions={0} | all-to-all | bytes 589824 | tf_op jit(solution)/shard_map/all_to_all | solution.py:317
  20.6 1.3 collective-permute-start.1
  21.9 1.4 collective-permute-start.3
  23.4 1.6 collective-permute-start.5
  25.0 3.4 %collective-permute-start = (bf16[8,144,128]{2,1,0:T(8,128)(2,1)S(1)}, bf16[8,144,128]{2,1,0:T(8,128)(2,1)S(1)}, u32[]{:S(2)}, u32[]{:S(2)}) collective-permute-start(bf16[8,144,128]{2,1,0:T(8,128)(2,1)S(1)} %all_to_all.20.refs_0_), channel_id=1, source_target_pairs={{0,4},{4,0},{1,5},{5,1},{2,6},{6,2},{3,7},{7,3},{8,12},{12,8},{9,1... | collective-permute-start | bytes 884744 | tf_op jit(solution)/shard_map/ppermute | solution.py:296
  28.4 4.7 %collective-permute-start.2 = (bf16[8,144,128]{2,1,0:T(8,128)(2,1)S(1)}, bf16[8,144,128]{2,1,0:T(8,128)(2,1)S(1)}, u32[]{:S(2)}, u32[]{:S(2)}) collective-permute-start(bf16[8,144,128]{2,1,0:T(8,128)(2,1)S(1)} %collective-permute-done.1.refs_2_), channel_id=1, source_target_pairs={{0,4},{4,0},{1,5},{5,1},{2,6},{6,2},{3,7},{7,3},{8,12},{12,8},{9,1... | collective-permute-start | bytes 884744 | tf_op jit(solution)/shard_map/ppermute | solution.py:296
  33.2 3.8 %collective-permute-start.4 = (bf16[8,144,128]{2,1,0:T(8,128)(2,1)S(1)}, bf16[8,144,128]{2,1,0:T(8,128)(2,1)S(1)}, u32[]{:S(2)}, u32[]{:S(2)}) collective-permute-start(bf16[8,144,128]{2,1,0:T(8,128)(2,1)S(1)} %collective-permute-done.3.refs_4_), channel_id=1, source_target_pairs={{0,4},{4,0},{1,5},{5,1},{2,6},{6,2},{3,7},{7,3},{8,12},{12,8},{9,1... | collective-permute-start | bytes 884744 | tf_op jit(solution)/shard_map/ppermute | solution.py:296
  37.0 1.9 %collective-permute-start.6 = (bf16[8,144,128]{2,1,0:T(8,128)(2,1)S(1)}, bf16[8,144,128]{2,1,0:T(8,128)(2,1)S(1)}, u32[]{:S(2)}, u32[]{:S(2)}) collective-permute-start(bf16[8,144,128]{2,1,0:T(8,128)(2,1)S(1)} %collective-permute-done.5.refs_6_), channel_id=1, source_target_pairs={{0,4},{4,0},{1,5},{5,1},{2,6},{6,2},{3,7},{7,3},{8,12},{12,8},{9,1... | collective-permute-start | bytes 884744 | tf_op jit(solution)/shard_map/ppermute | solution.py:296
  38.9 1.1 collective-permute-done.6.refs_7_
  40.0 3.8 %attend.1 = (bf16[128,256]{1,0:T(8,128)(2,1)S(1)}, bf16[1024,2048]{1,0:T(8,128)(2,1)S(1)}) custom-call(s32[10]{0:T(128)S(1)} %stack.40.place_ref, bf16[128,256]{1,0:T(8,128)(2,1)} %query_hbm.1, bf16[1024,2048]{1,0:T(8,128)(2,1)} %source_ref.1, bf16[8,144,128]{2,1,0:T(8,128)(2,1)S(1)} %all_to_all.20.refs_0_, ...), custom_call_target="tpu_custom_call" | custom-call | tf_op jit(solution)/shard_map/attend/pallas_call | solution.py:181
  43.9 8.4 %all_to_all.21.att_ref = bf16[4,32,256]{2,1,0:T(8,128)(2,1)S(1)} all-to-all(bf16[4,32,256]{2,1,0:T(8,128)(2,1)S(1)} %bitcast.19), channel_id=1, replica_groups=mesh['z'=8,'y'=4,'c'=2,'tp'=4] {'tp'}, dimensions={0} | all-to-all | bytes 131072 | tf_op jit(solution)/shard_map/all_to_all | solution.py:328
  52.3 1.2 shard_map.118
  53.5 1.1 reshape.20
  54.7 11.9 %all-to-all-start.2 = ((bf16[64,2,2048]{2,1,0:T(2,128)(2,1)}), bf16[64,2,2048]{2,1,0:T(2,128)(2,1)S(1)}, u32[]{:S(2)}, u32[]{:S(2)}) async-start(bf16[64,2,2048]{2,1,0:T(2,128)(2,1)} %reshape.20), calls=%async_computation.2 | async-start | bytes 1048576 | tf_op jit(solution)/shard_map/all_to_all | solution.py:341
  66.9 2.4 %collective-permute-start.10 = (bf16[256,2048]{1,0:T(8,128)(2,1)S(1)}, bf16[256,2048]{1,0:T(8,128)(2,1)}, u32[]{:S(2)}, u32[]{:S(2)}) collective-permute-start(bf16[256,2048]{1,0:T(8,128)(2,1)S(1)} %bitcast.28), channel_id=1, source_target_pairs={{0,3},{1,0},{2,1},{3,2},{4,7},{5,4},{6,5},{7,6},{8,11},{9,8},{10,9... | collective-permute-start | bytes 3145736 | tf_op jit(solution)/shard_map/ppermute | solution.py:296
  69.3 14.9 %all-to-all-done.2 = bf16[64,2,2048]{2,1,0:T(2,128)(2,1)S(1)} async-done(((bf16[64,2,2048]{2,1,0:T(2,128)(2,1)}), bf16[64,2,2048]{2,1,0:T(2,128)(2,1)S(1)}, u32[]{:S(2)}, u32[]{:S(2)}) %all-to-all-start.2) | async-done | bytes 524320 | tf_op jit(solution)/shard_map/all_to_all | solution.py:341
  84.8 2.4 %collective-permute-start.8 = (bf16[128,2048]{1,0:T(8,128)(2,1)S(1)}, bf16[128,2048]{1,0:T(8,128)(2,1)S(1)}, u32[]{:S(2)}, u32[]{:S(2)}) collective-permute-start(bf16[128,2048]{1,0:T(8,128)(2,1)S(1)} %reshape.21.own_ref), channel_id=1, source_target_pairs={{0,3},{1,0},{2,1},{3,2},{4,7},{5,4},{6,5},{7,6},{8,11},{9,8},{10,9... | collective-permute-start | bytes 1572872 | tf_op jit(solution)/shard_map/ppermute | solution.py:296
  87.2 38.6 %collective-permute-done.7.left_ref = bf16[128,2048]{1,0:T(8,128)(2,1)S(1)} collective-permute-done((bf16[128,2048]{1,0:T(8,128)(2,1)S(1)}, bf16[128,2048]{1,0:T(8,128)(2,1)S(1)}, u32[]{:S(2)}, u32[]{:S(2)}) %collective-permute-start.7) | collective-permute-done | bytes 524320 | tf_op jit(solution)/shard_map/ppermute | solution.py:296
  125.9 2.7 %collective-permute-start.15 = (bf16[64,2048]{1,0:T(8,128)(2,1)S(1)}, bf16[64,2048]{1,0:T(8,128)(2,1)S(1)}, u32[]{:S(2)}, u32[]{:S(2)}) collective-permute-start(bf16[64,2048]{1,0:T(8,128)(2,1)S(1)} %slice.9), channel_id=1, source_target_pairs={{0,3},{1,0},{2,1},{3,2},{4,7},{5,4},{6,5},{7,6},{8,11},{9,8},{10,9... | collective-permute-start | bytes 786440 | tf_op jit(solution)/shard_map/ppermute | solution.py:296
  129.7 2.9 %near.1 = (bf16[128,256]{1,0:T(8,128)(2,1)S(1)}, bf16[128,256]{1,0:T(8,128)(2,1)S(1)}, bf16[128,256]{1,0:T(8,128)(2,1)S(1)}, bf16[2048,256]{1,0:T(8,128)(2,1)S(1...) custom-call(bf16[128,2048]{1,0:T(8,128)(2,1)S(1)} %reshape.21.own_re, ...), custom_call_target="tpu_custom_call" | custom-call | tf_op jit(solution)/shard_map/near/pallas_call | solution.py:252
  132.6 2.7 %collective-permute-start.13 = (bf16[128,256]{1,0:T(8,128)(2,1)S(1)}, bf16[128,256]{1,0:T(8,128)(2,1)S(1)}, u32[]{:S(2)}, u32[]{:S(2)}) collective-permute-start(bf16[128,256]{1,0:T(8,128)(2,1)S(1)} %get-tuple-element.26), channel_id=1, source_target_pairs={{0,3},{1,0},{2,1},{3,2},{4,7},{5,4},{6,5},{7,6},{8,11},{9,8},{10,9... | collective-permute-start | bytes 196616 | tf_op jit(solution)/shard_map/ppermute | solution.py:296
  136.9 3.9 %collective-permute-done.16.far_ref = bf16[128,256]{1,0:T(8,128)(2,1)S(1)} collective-permute-done((bf16[128,256]{1,0:T(8,128)(2,1)S(1)}, bf16[128,256]{1,0:T(8,128)(2,1)S(1)}, u32[]{:S(2)}, u32[]{:S(2)}) %collective-permute-start.16) | collective-permute-done | bytes 65568 | tf_op jit(solution)/shard_map/ppermute | solution.py:296
  141.9 31.0 %all_to_all.22 = bf16[64,2,2048]{2,1,0:T(2,128)(2,1)S(1)} all-to-all(bf16[64,2,2048]{2,1,0:T(2,128)(2,1)S(1)} %reshape.22), channel_id=1, replica_groups=mesh['z'=8,'y'=4,'c'=2,'tp'=4] {'z','y','c'}, dimensions={0} | all-to-all | bytes 1048576 | tf_op jit(solution)/shard_map/all_to_all | solution.py:359
  173.1 1.2 shard_map.121
  (41 shorter events, 6.0 us)
Async XLA Ops:
  0.0 52.3 %copy-start = (bf16[32,2048]{1,0:T(8,128)(2,1)S(1)}, bf16[32,2048]{1,0:T(8,128)(2,1)}, u32[]{:S(2)}) copy-start(bf16[32,2048]{1,0:T(8,128)(2,1)} %residual_ref.1) | copy-start | bytes 393220
  0.0 52.3 %copy-start.1 = (f32[2048]{0:T(1024)S(1)}, f32[2048]{0:T(1024)}, u32[]{:S(2)}) copy-start(f32[2048]{0:T(1024)} %param.18) | copy-start | bytes 24580
  0.0 52.3 %copy-start.2 = (s32[32,2]{0,1:T(2,128)S(1)}, s32[32,2]{0,1:T(2,128)}, u32[]{:S(2)}) copy-start(s32[32,2]{0,1:T(2,128)} %param.19) | copy-start | bytes 772
  20.6 7.8 %collective-permute-start.1 = (bf16[8,144,128]{2,1,0:T(8,128)(2,1)S(1)}, bf16[8,144,128]{2,1,0:T(8,128)(2,1)S(1)}, u32[]{:S(2)}, u32[]{:S(2)}) collective-permute-start(bf16[8,144,128]{2,1,0:T(8,128)(2,1)S(1)} %all_to_all.20.refs_0_), channel_id=1, source_target_pairs={{0,8},{8,16},{16,24},{24,0},{1,9},{9,17},{17,25},{25,1},{2,10},{10... | collective-permute-start | bytes 884744 | tf_op jit(solution)/shard_map/ppermute | solution.py:296
  21.9 11.2 %collective-permute-start.3 = (bf16[8,144,128]{2,1,0:T(8,128)(2,1)S(1)}, bf16[8,144,128]{2,1,0:T(8,128)(2,1)S(1)}, u32[]{:S(2)}, u32[]{:S(2)}) collective-permute-start(bf16[8,144,128]{2,1,0:T(8,128)(2,1)S(1)} %all_to_all.20.refs_0_), channel_id=1, source_target_pairs={{0,24},{8,0},{16,8},{24,16},{1,25},{9,1},{17,9},{25,17},{2,26},{10... | collective-permute-start | bytes 884744 | tf_op jit(solution)/shard_map/ppermute | solution.py:296
  23.4 13.6 %collective-permute-start.5 = (bf16[8,144,128]{2,1,0:T(8,128)(2,1)S(1)}, bf16[8,144,128]{2,1,0:T(8,128)(2,1)S(1)}, u32[]{:S(2)}, u32[]{:S(2)}) collective-permute-start(bf16[8,144,128]{2,1,0:T(8,128)(2,1)S(1)} %all_to_all.20.refs_0_), channel_id=1, source_target_pairs={{0,16},{8,24},{16,0},{24,8},{1,17},{9,25},{17,1},{25,9},{2,18},{10... | collective-permute-start | bytes 884744 | tf_op jit(solution)/shard_map/ppermute | solution.py:296
  25.0 13.9 %collective-permute-start = (bf16[8,144,128]{2,1,0:T(8,128)(2,1)S(1)}, bf16[8,144,128]{2,1,0:T(8,128)(2,1)S(1)}, u32[]{:S(2)}, u32[]{:S(2)}) collective-permute-start(bf16[8,144,128]{2,1,0:T(8,128)(2,1)S(1)} %all_to_all.20.refs_0_), channel_id=1, source_target_pairs={{0,4},{4,0},{1,5},{5,1},{2,6},{6,2},{3,7},{7,3},{8,12},{12,8},{9,1... | collective-permute-start | bytes 884744 | tf_op jit(solution)/shard_map/ppermute | solution.py:296
  28.4 10.5 %collective-permute-start.2 = (bf16[8,144,128]{2,1,0:T(8,128)(2,1)S(1)}, bf16[8,144,128]{2,1,0:T(8,128)(2,1)S(1)}, u32[]{:S(2)}, u32[]{:S(2)}) collective-permute-start(bf16[8,144,128]{2,1,0:T(8,128)(2,1)S(1)} %collective-permute-done.1.refs_2_), channel_id=1, source_target_pairs={{0,4},{4,0},{1,5},{5,1},{2,6},{6,2},{3,7},{7,3},{8,12},{12,8},{9,1... | collective-permute-start | bytes 884744 | tf_op jit(solution)/shard_map/ppermute | solution.py:296
  33.2 5.8 %collective-permute-start.4 = (bf16[8,144,128]{2,1,0:T(8,128)(2,1)S(1)}, bf16[8,144,128]{2,1,0:T(8,128)(2,1)S(1)}, u32[]{:S(2)}, u32[]{:S(2)}) collective-permute-start(bf16[8,144,128]{2,1,0:T(8,128)(2,1)S(1)} %collective-permute-done.3.refs_4_), channel_id=1, source_target_pairs={{0,4},{4,0},{1,5},{5,1},{2,6},{6,2},{3,7},{7,3},{8,12},{12,8},{9,1... | collective-permute-start | bytes 884744 | tf_op jit(solution)/shard_map/ppermute | solution.py:296
  37.0 3.1 %collective-permute-start.6 = (bf16[8,144,128]{2,1,0:T(8,128)(2,1)S(1)}, bf16[8,144,128]{2,1,0:T(8,128)(2,1)S(1)}, u32[]{:S(2)}, u32[]{:S(2)}) collective-permute-start(bf16[8,144,128]{2,1,0:T(8,128)(2,1)S(1)} %collective-permute-done.5.refs_6_), channel_id=1, source_target_pairs={{0,4},{4,0},{1,5},{5,1},{2,6},{6,2},{3,7},{7,3},{8,12},{12,8},{9,1... | collective-permute-start | bytes 884744 | tf_op jit(solution)/shard_map/ppermute | solution.py:296
  43.9 22.7 %copy-start.4 = (bf16[1,256,2048]{2,1,0:T(8,128)(2,1)S(1)}, bf16[1,256,2048]{2,1,0:T(8,128)(2,1)}, u32[]{:S(2)}) copy-start(bf16[1,256,2048]{2,1,0:T(8,128)(2,1)} %param.23) | copy-start | bytes 3145732
  54.7 29.6 %all-to-all-start.2 = ((bf16[64,2,2048]{2,1,0:T(2,128)(2,1)}), bf16[64,2,2048]{2,1,0:T(2,128)(2,1)S(1)}, u32[]{:S(2)}, u32[]{:S(2)}) async-start(bf16[64,2,2048]{2,1,0:T(2,128)(2,1)} %reshape.20), calls=%async_computation.2 | async-start | bytes 1048576 | tf_op jit(solution)/shard_map/all_to_all | solution.py:341
  66.5 62.1 %collective-permute-start.9 = (bf16[256,2048]{1,0:T(8,128)(2,1)S(1)}, bf16[256,2048]{1,0:T(8,128)(2,1)S(1)}, u32[]{:S(2)}, u32[]{:S(2)}) collective-permute-start(bf16[256,2048]{1,0:T(8,128)(2,1)S(1)} %bitcast.27), channel_id=1, source_target_pairs={{0,1},{1,2},{2,3},{3,0},{4,5},{5,6},{6,7},{7,4},{8,9},{9,10},{10,1... | collective-permute-start | bytes 3145736 | tf_op jit(solution)/shard_map/ppermute | solution.py:296
  66.9 61.8 %collective-permute-start.10 = (bf16[256,2048]{1,0:T(8,128)(2,1)S(1)}, bf16[256,2048]{1,0:T(8,128)(2,1)}, u32[]{:S(2)}, u32[]{:S(2)}) collective-permute-start(bf16[256,2048]{1,0:T(8,128)(2,1)S(1)} %bitcast.28), channel_id=1, source_target_pairs={{0,3},{1,0},{2,1},{3,2},{4,7},{5,4},{6,5},{7,6},{8,11},{9,8},{10,9... | collective-permute-start | bytes 3145736 | tf_op jit(solution)/shard_map/ppermute | solution.py:296
  69.3 59.4 %collective-permute-start.11 = (bf16[256,2048]{1,0:T(8,128)(2,1)S(1)}, bf16[256,2048]{1,0:T(8,128)(2,1)}, u32[]{:S(2)}, u32[]{:S(2)}) collective-permute-start(bf16[256,2048]{1,0:T(8,128)(2,1)S(1)} %bitcast.29), channel_id=1, source_target_pairs={{0,2},{1,3},{2,0},{3,1},{4,6},{5,7},{6,4},{7,5},{8,10},{9,11},{10,... | collective-permute-start | bytes 3145736 | tf_op jit(solution)/shard_map/ppermute | solution.py:296
  84.4 41.4 %collective-permute-start.7 = (bf16[128,2048]{1,0:T(8,128)(2,1)S(1)}, bf16[128,2048]{1,0:T(8,128)(2,1)S(1)}, u32[]{:S(2)}, u32[]{:S(2)}) collective-permute-start(bf16[128,2048]{1,0:T(8,128)(2,1)S(1)} %reshape.21.own_ref), channel_id=1, source_target_pairs={{0,1},{1,2},{2,3},{3,0},{4,5},{5,6},{6,7},{7,4},{8,9},{9,10},{10,1... | collective-permute-start | bytes 1572872 | tf_op jit(solution)/shard_map/ppermute | solution.py:296
  84.8 41.1 %collective-permute-start.8 = (bf16[128,2048]{1,0:T(8,128)(2,1)S(1)}, bf16[128,2048]{1,0:T(8,128)(2,1)S(1)}, u32[]{:S(2)}, u32[]{:S(2)}) collective-permute-start(bf16[128,2048]{1,0:T(8,128)(2,1)S(1)} %reshape.21.own_ref), channel_id=1, source_target_pairs={{0,3},{1,0},{2,1},{3,2},{4,7},{5,4},{6,5},{7,6},{8,11},{9,8},{10,9... | collective-permute-start | bytes 1572872 | tf_op jit(solution)/shard_map/ppermute | solution.py:296
  125.8 9.5 %collective-permute-start.14 = (bf16[64,2048]{1,0:T(8,128)(2,1)S(1)}, bf16[64,2048]{1,0:T(8,128)(2,1)S(1)}, u32[]{:S(2)}, u32[]{:S(2)}) collective-permute-start(bf16[64,2048]{1,0:T(8,128)(2,1)S(1)} %slice.8), channel_id=1, source_target_pairs={{0,1},{1,2},{2,3},{3,0},{4,5},{5,6},{6,7},{7,4},{8,9},{9,10},{10,1... | collective-permute-start | bytes 786440 | tf_op jit(solution)/shard_map/ppermute | solution.py:296
  125.9 9.3 %collective-permute-start.15 = (bf16[64,2048]{1,0:T(8,128)(2,1)S(1)}, bf16[64,2048]{1,0:T(8,128)(2,1)S(1)}, u32[]{:S(2)}, u32[]{:S(2)}) collective-permute-start(bf16[64,2048]{1,0:T(8,128)(2,1)S(1)} %slice.9), channel_id=1, source_target_pairs={{0,3},{1,0},{2,1},{3,2},{4,7},{5,4},{6,5},{7,6},{8,11},{9,8},{10,9... | collective-permute-start | bytes 786440 | tf_op jit(solution)/shard_map/ppermute | solution.py:296
  128.7 1.0 copy-start.5
  132.5 4.4 %collective-permute-start.12 = (bf16[128,256]{1,0:T(8,128)(2,1)S(1)}, bf16[128,256]{1,0:T(8,128)(2,1)S(1)}, u32[]{:S(2)}, u32[]{:S(2)}) collective-permute-start(bf16[128,256]{1,0:T(8,128)(2,1)S(1)} %get-tuple-element.25), channel_id=1, source_target_pairs={{0,1},{1,2},{2,3},{3,0},{4,5},{5,6},{6,7},{7,4},{8,9},{9,10},{10,1... | collective-permute-start | bytes 196616 | tf_op jit(solution)/shard_map/ppermute | solution.py:296
  132.6 4.3 %collective-permute-start.13 = (bf16[128,256]{1,0:T(8,128)(2,1)S(1)}, bf16[128,256]{1,0:T(8,128)(2,1)S(1)}, u32[]{:S(2)}, u32[]{:S(2)}) collective-permute-start(bf16[128,256]{1,0:T(8,128)(2,1)S(1)} %get-tuple-element.26), channel_id=1, source_target_pairs={{0,3},{1,0},{2,1},{3,2},{4,7},{5,4},{6,5},{7,6},{8,11},{9,8},{10,9... | collective-permute-start | bytes 196616 | tf_op jit(solution)/shard_map/ppermute | solution.py:296
  136.2 37.0 %copy-start.3 = (f32[32,2]{0,1:T(2,128)S(1)}, f32[32,2]{0,1:T(2,128)}, u32[]{:S(2)}) copy-start(f32[32,2]{0,1:T(2,128)} %param.20) | copy-start | bytes 772
  136.2 4.7 %collective-permute-start.16 = (bf16[128,256]{1,0:T(8,128)(2,1)S(1)}, bf16[128,256]{1,0:T(8,128)(2,1)S(1)}, u32[]{:S(2)}, u32[]{:S(2)}) collective-permute-start(bf16[128,256]{1,0:T(8,128)(2,1)S(1)} %shard_map.119), channel_id=1, source_target_pairs={{0,2},{1,3},{2,0},{3,1},{4,6},{5,7},{6,4},{7,5},{8,10},{9,11},{10,... | collective-permute-start | bytes 196616 | tf_op jit(solution)/shard_map/ppermute | solution.py:296
where the time goes:
time: 175 us; the launch traced here: 174 us
  waiting for transfers between devices  59.3 us (34%)
  blocking collectives  59.2 us (34%)
  starting transfers between devices  41.2 us (24%)
  Pallas kernels  11.5 us (7%)
  local copies, waits for them, and re-layouts  3 us (2%)
    ppermute x17, waiting for transfers between devices, moved(): return lax.ppermute(x, axis, [(i, (i + by) % size) for i in range(size)])  44.4 us
    all_to_all x1, blocking collectives, shards(): lax.all_to_all(expert_out.reshape(64, 2, D), SP, 0, 0, tiled=True)  31 us
    ppermute x17, starting transfers between devices, moved(): return lax.ppermute(x, axis, [(i, (i + by) % size) for i in range(size)])  29.3 us
    all_to_all x1, blocking collectives, shards(): own = lax.all_to_all(copies, 'z', 0, 0, tiled=True)  19.8 us
    all_to_all x1, waiting for transfers between devices, shards(): lax.all_to_all(rows.reshape(64, 2, D), SP, 0, 0, tiled=True).reshape(TOK, D)  14.9 us
    all_to_all x1, starting transfers between devices, shards(): lax.all_to_all(rows.reshape(64, 2, D), SP, 0, 0, tiled=True).reshape(TOK, D)  11.9 us
    all_to_all x1, blocking collectives, shards(): lax.all_to_all(attended.reshape(NT, ROW, -1), 'tp', 0, 0, tiled=True)  8.42 us
    pallas_call x4, Pallas kernels, call(): pl.pallas_call(kernel, out_shape=[jax.ShapeDtypeStruct(s, t) for s, t in...  3.92 us
  transfers between devices with their start and end apart: 18, of which 5 were waited for; matrix products, arithmetic and copies ran while one was open for 0% of the time, Pallas kernels for 2%

commit v1 on v0

--- a/solution.py
+++ b/solution.py
@@ -93,15 +93,17 @@
     return jnp.concatenate(rows, axis=0)
 
 
-def attend_kernel(count, place_ref, query_hbm, source_ref, *refs):
+def query_kernel(query_ref, out_ref):
+    out_ref[...] = query_rows(query_ref)
+
+
+def attend_kernel(count, place_ref, query_ref, source_ref, *refs):
     chunks, refs = refs[:count], refs[count:]
-    out_ref, target_ref, m_ref, l_ref, acc_ref, query_ref, sems = refs
-    fetch, copy = fetches([(query_hbm, query_ref), (source_ref, target_ref)], sems)
-    fetch.start()
+    out_ref, target_ref, m_ref, l_ref, acc_ref, sem = refs
+    copy = pltpu.make_async_copy(source_ref, target_ref, sem)
     copy.start()
-    fetch.wait()
     own_z, own_order = place_ref[0], place_ref[1]
-    queries = query_rows(query_ref)
+    queries = query_ref[...]
     total_rows = HEADS * TOK
     blocks = GROUP * count
     row_of_gate = lax.broadcasted_iota(jnp.int32, (16, TOK), 0)
@@ -184,20 +186,19 @@
             jax.ShapeDtypeStruct((TOK, HEADS * HEAD), BF16),
             jax.ShapeDtypeStruct(weight.shape, weight.dtype),
         ],
-        in_specs=[pl.BlockSpec(memory_space=pltpu.SMEM)]
-        + [pl.BlockSpec(memory_space=pltpu.HBM)] * 2
+        in_specs=[pl.BlockSpec(memory_space=pltpu.SMEM), vmem]
+        + [pl.BlockSpec(memory_space=pltpu.HBM)]
         + [vmem] * len(chunks),
         out_specs=[vmem] * 2,
         scratch_shapes=[
             pltpu.VMEM((total_rows, TOK), F32),
             pltpu.VMEM((total_rows, TOK), F32),
             pltpu.VMEM((total_rows, HEAD), F32),
-            pltpu.VMEM(queries.shape, BF16),
-            pltpu.SemaphoreType.DMA((2,)),
+            pltpu.SemaphoreType.DMA,
         ],
         compiler_params=PARAMS,
         name="attend",
-    )(place, in_hbm(queries), in_hbm(weight), *map(in_vmem, chunks))
+    )(place, in_vmem(queries), in_hbm(weight), *map(in_vmem, chunks))
 
 
 def picks(routes_ref, transposed_slots=128):
@@ -232,38 +233,45 @@
     return (gate / (1.0 + jnp.exp(-gate)) * up).astype(BF16)
 
 
-def near_kernel(own_ref, left_ref, right_ref, *refs):
-    sources, (h_own, h_left, h_right), refs = refs[:6], refs[6:9], refs[9:]
-    targets, sems = refs[:6], refs[6]
+def near_kernel(own, left0, right1, *refs):
+    sources, outs, targets, sems = refs[:6], refs[6:9], refs[9:15], refs[15]
     copies = fetches(list(zip(sources, targets)), sems)
     for copy in copies:
         copy.start()
     copies[0].wait()
     copies[1].wait()
-    for rows_ref, out_ref in ((own_ref, h_own), (left_ref, h_left), (right_ref, h_right)):
-        out_ref[...] = hidden(rows_ref[...], targets[0], targets[1])
+    for rows, out_ref in zip((own, left0, right1), outs):
+        out_ref[...] = hidden(rows[...], targets[0], targets[1])
     for copy in copies[2:]:
         copy.wait()
 
 
 def near(rows, weights):
     vmem = pl.BlockSpec(memory_space=pltpu.VMEM)
-    shape = jax.ShapeDtypeStruct((TOK, weights[0].shape[1]), BF16)
+    wide = weights[0].shape[1]
     return pl.pallas_call(
         near_kernel,
-        out_shape=[shape] * 3 + [jax.ShapeDtypeStruct(w.shape, w.dtype) for w in weights],
-        in_specs=[vmem] * 3 + [pl.BlockSpec(memory_space=pltpu.HBM)] * 6,
-        out_specs=[vmem] * 9,
-        scratch_shapes=[pltpu.SemaphoreType.DMA((6,))],
+        out_shape=[jax.ShapeDtypeStruct((r.shape[0], wide), BF16) for r in rows]
+        + [jax.ShapeDtypeStruct(w.shape, w.dtype) for w in weights],
+        in_specs=[vmem] * len(rows) + [pl.BlockSpec(memory_space=pltpu.HBM)] * len(weights),
+        out_specs=[vmem] * (len(rows) + len(weights)),
+        scratch_shapes=[pltpu.SemaphoreType.DMA((len(weights),))],
         compiler_params=PARAMS,
         name="near",
     )(*rows, *map(in_hbm, weights))
 
 
-def far_kernel(gate_ref, up_ref, far0_ref, far1_ref, out_ref):
+def rest_kernel(gate_ref, up_ref, left1, right0, h_left0, h_right1, h_left, h_right):
     half = TOK // 2
-    out_ref[:half, :] = hidden(far0_ref[...], gate_ref, up_ref)
-    out_ref[half:, :] = hidden(far1_ref[...], gate_ref, up_ref)
+    h_left[:half, :] = h_left0[...]
+    h_left[half:, :] = hidden(left1[...], gate_ref, up_ref)
+    h_right[:half, :] = hidden(right0[...], gate_ref, up_ref)
+    h_right[half:, :] = h_right1[...]
+
+
+def far_kernel(gate_ref, up_ref, far0, far1, h_far):
+    rows = jnp.concatenate([far0[...], far1[...]], axis=0)
+    h_far[...] = hidden(rows, gate_ref, up_ref)
 
 
 def down_kernel(own_ref, left_ref, right_ref, far_ref, w_own, w_left, w_right, w_far, out_ref):
@@ -315,6 +323,7 @@
     down_left, down_right = moved(down_own, "tp", 1), moved(down_own, "tp", -1)
     copies = pack(keys.T, values.T, forget_prefix_log.T)
     own = lax.all_to_all(copies, "z", 0, 0, tiled=True)
+    (rows_of_q,) = call(query_kernel, [((HEADS * TOK, HEAD + 16), BF16)], queries)
     chunks = [own, moved(own, "c", 1)]
     place = [z, y * NC + c, y * NC + c, y * NC + 1 - c]
     for step in (1, 3, 2):
@@ -323,7 +332,7 @@
         chunks += [chunk, moved(chunk, "c", 1)]
         place += [from_y * NC + c, from_y * NC + 1 - c]
     place = jnp.stack(place).astype(jnp.int32)
-    attended, out_w = attend(place, queries, out_weight, chunks)
+    attended, out_w = attend(place, rows_of_q, out_weight, chunks)
 
     heads = lax.all_to_all(attended.reshape(NT, ROW, -1), "tp", 0, 0, tiled=True)
     far_source, _ = lax.optimization_barrier((down_own, heads))
@@ -339,20 +348,25 @@
         routes_row,
     )
     arrived = lax.all_to_all(rows.reshape(64, 2, D), SP, 0, 0, tiled=True).reshape(TOK, D)
-    left, right = moved(arrived, "tp", 1), moved(arrived, "tp", -1)
     half = TOK // 2
-    far0, far1 = moved(left[:half], "tp", 1), moved(right[half:], "tp", -1)
-    h_own, h_left, h_right, gate_w, up_w, *down_w = near(
-        (arrived, left, right),
+    top, bottom = arrived[:half], arrived[half:]
+    left0, right1 = moved(top, "tp", 1), moved(bottom, "tp", -1)
+    left1, right0 = moved(bottom, "tp", 1), moved(top, "tp", -1)
+    far0, far1 = moved(left0, "tp", 1), moved(right1, "tp", -1)
+    h_own, h_left0, h_right1, gate_w, up_w, *down_w = near(
+        (arrived, left0, right1),
         (w_gate[0], w_up[0], down_own, down_left, down_right, down_far),
     )
-    (h_far,) = call(far_kernel, [(h_own.shape, BF16)], gate_w, up_w, far0, far1)
+    shape = (h_own.shape, BF16)
+    h_left, h_right = call(rest_kernel, [shape] * 2, gate_w, up_w, left1, right0, h_left0, h_right1)
+    from_left, from_right = moved(h_right, "tp", 1), moved(h_left, "tp", -1)
+    (h_far,) = call(far_kernel, [shape], gate_w, up_w, far0, far1)
     (expert_out,) = call(
         down_kernel,
         [((TOK, D), BF16)],
         h_own,
-        moved(h_right, "tp", 1),
-        moved(h_left, "tp", -1),
+        from_left,
+        from_right,
         moved(h_far, "tp", 2),
         *down_w,
     )

time: 175 us -> 169 us (0.966)
  waiting for transfers between devices: 59.3 us -> 50.1 us
  starting transfers between devices: 41.2 us -> 43.9 us
    ppermute x17 -> x19, waiting for transfers between devices: 44.4 us -> 35.1 us  [moved(): return lax.ppermute(x, axis, [(i, (i + by) % size) for i in range(size)])]
    ppermute x17 -> x19, starting transfers between devices: 29.3 us -> 33.5 us  [moved(): return lax.ppermute(x, axis, [(i, (i + by) % size) for i in range(size)])]
    pallas_call x4 -> x6, Pallas kernels: 3.92 us -> 4.49 us  [call(): pl.pallas_call(kernel, out_shape=[jax.ShapeDtypeStruct(s, t) for s, t in...]
  transfers between devices with their start and end apart: 18 -> 20, of which waited for: 5 -> 6; matrix products, arithmetic and copies ran while one was open for 0% -> 1% of each run, Pallas kernels for 2% -> 3%
where the time goes in v1:
time: 169 us
  blocking collectives  58.6 us (35%)
  waiting for transfers between devices  50.1 us (30%)
  starting transfers between devices  43.9 us (26%)
  Pallas kernels  12.6 us (7%)
  local copies, waits for them, and re-layouts  3.4 us (2%)
    ppermute x19, waiting for transfers between devices, moved(): return lax.ppermute(x, axis, [(i, (i + by) % size) for i in range(size)])  35.1 us
    ppermute x19, starting transfers between devices, moved(): return lax.ppermute(x, axis, [(i, (i + by) % size) for i in range(size)])  33.5 us
    all_to_all x1, blocking collectives, shards(): lax.all_to_all(expert_out.reshape(64, 2, D), SP, 0, 0, tiled=True)  30.5 us
    all_to_all x1, blocking collectives, shards(): own = lax.all_to_all(copies, 'z', 0, 0, tiled=True)  19.8 us
    all_to_all x1, waiting for transfers between devices, shards(): lax.all_to_all(rows.reshape(64, 2, D), SP, 0, 0, tiled=True).reshape(TOK, D)  14.9 us
    all_to_all x1, starting transfers between devices, shards(): lax.all_to_all(rows.reshape(64, 2, D), SP, 0, 0, tiled=True).reshape(TOK, D)  10.4 us
    all_to_all x1, blocking collectives, shards(): lax.all_to_all(attended.reshape(NT, ROW, -1), 'tp', 0, 0, tiled=True)  8.29 us
    pallas_call x6, Pallas kernels, call(): pl.pallas_call(kernel, out_shape=[jax.ShapeDtypeStruct(s, t) for s, t in...  4.49 us
  transfers between devices with their start and end apart: 20, of which 6 were waited for; matrix products, arithmetic and copies ran while one was open for 1% of the time, Pallas kernels for 3%

profile of v1, /device:TPU:1, one launch (start us, length us, event | category | flops | bytes accessed | tf_op | source)
XLA Modules:
  0.0 168.8 jit_solution(3580768020411191540)
XLA Ops:
  0.9 19.8 %all_to_all.20.refs_0_ = bf16[8,144,128]{2,1,0:T(8,128)(2,1)S(1)} all-to-all(bf16[8,144,128]{2,1,0:T(8,128)(2,1)S(1)} %pack.1), channel_id=1, replica_groups=mesh['z'=8,'y'=4,'c'=2,'tp'=4] {'z'}, dimensions={0} | all-to-all | bytes 589824 | tf_op jit(solution)/shard_map/all_to_all | solution.py:325
  20.6 1.3 collective-permute-start.1
  21.9 1.4 collective-permute-start.3
  23.4 1.6 collective-permute-start.5
  25.0 3.4 %collective-permute-start = (bf16[8,144,128]{2,1,0:T(8,128)(2,1)S(1)}, bf16[8,144,128]{2,1,0:T(8,128)(2,1)S(1)}, u32[]{:S(2)}, u32[]{:S(2)}) collective-permute-start(bf16[8,144,128]{2,1,0:T(8,128)(2,1)S(1)} %all_to_all.20.refs_0_), channel_id=1, source_target_pairs={{0,4},{4,0},{1,5},{5,1},{2,6},{6,2},{3,7},{7,3},{8,12},{12,8},{9,1... | collective-permute-start | bytes 884744 | tf_op jit(solution)/shard_map/ppermute | solution.py:304
  28.4 4.7 %collective-permute-start.2 = (bf16[8,144,128]{2,1,0:T(8,128)(2,1)S(1)}, bf16[8,144,128]{2,1,0:T(8,128)(2,1)S(1)}, u32[]{:S(2)}, u32[]{:S(2)}) collective-permute-start(bf16[8,144,128]{2,1,0:T(8,128)(2,1)S(1)} %collective-permute-done.1.refs_2_), channel_id=1, source_target_pairs={{0,4},{4,0},{1,5},{5,1},{2,6},{6,2},{3,7},{7,3},{8,12},{12,8},{9,1... | collective-permute-start | bytes 884744 | tf_op jit(solution)/shard_map/ppermute | solution.py:304
  33.2 3.8 %collective-permute-start.4 = (bf16[8,144,128]{2,1,0:T(8,128)(2,1)S(1)}, bf16[8,144,128]{2,1,0:T(8,128)(2,1)S(1)}, u32[]{:S(2)}, u32[]{:S(2)}) collective-permute-start(bf16[8,144,128]{2,1,0:T(8,128)(2,1)S(1)} %collective-permute-done.3.refs_4_), channel_id=1, source_target_pairs={{0,4},{4,0},{1,5},{5,1},{2,6},{6,2},{3,7},{7,3},{8,12},{12,8},{9,1... | collective-permute-start | bytes 884744 | tf_op jit(solution)/shard_map/ppermute | solution.py:304
  37.0 1.9 %collective-permute-start.6 = (bf16[8,144,128]{2,1,0:T(8,128)(2,1)S(1)}, bf16[8,144,128]{2,1,0:T(8,128)(2,1)S(1)}, u32[]{:S(2)}, u32[]{:S(2)}) collective-permute-start(bf16[8,144,128]{2,1,0:T(8,128)(2,1)S(1)} %collective-permute-done.5.refs_6_), channel_id=1, source_target_pairs={{0,4},{4,0},{1,5},{5,1},{2,6},{6,2},{3,7},{7,3},{8,12},{12,8},{9,1... | collective-permute-start | bytes 884744 | tf_op jit(solution)/shard_map/ppermute | solution.py:304
  40.0 4.4 %attend.1 = (bf16[128,256]{1,0:T(8,128)(2,1)S(1)}, bf16[1024,2048]{1,0:T(8,128)(2,1)S(1)}) custom-call(s32[10]{0:T(128)S(1)} %stack.40.place_ref, bf16[512,80]{1,0:T(8,128)(2,1)S(1)} %shard_map.118.query_ref, bf16[1024,2048]{1,0:T(8,128)(2,1)} %source_ref.1, bf16[8,144,128]{2,1,0:T(8,128)(2,1)S(1)} %all_to_all.20.refs_0_, ...), custom_call_target="tpu_custom_call" | custom-call | tf_op jit(solution)/shard_map/attend/pallas_call | solution.py:183
  44.5 8.3 %all_to_all.21.att_ref = bf16[4,32,256]{2,1,0:T(8,128)(2,1)S(1)} all-to-all(bf16[4,32,256]{2,1,0:T(8,128)(2,1)S(1)} %bitcast.19), channel_id=1, replica_groups=mesh['z'=8,'y'=4,'c'=2,'tp'=4] {'tp'}, dimensions={0} | all-to-all | bytes 131072 | tf_op jit(solution)/shard_map/all_to_all | solution.py:337
  55.1 10.4 %all-to-all-start.2 = ((bf16[64,2,2048]{2,1,0:T(2,128)(2,1)}), bf16[64,2,2048]{2,1,0:T(2,128)(2,1)S(1)}, u32[]{:S(2)}, u32[]{:S(2)}) async-start(bf16[64,2,2048]{2,1,0:T(2,128)(2,1)} %reshape.22), calls=%async_computation.2 | async-start | bytes 1048576 | tf_op jit(solution)/shard_map/all_to_all | solution.py:350
  65.9 2.4 %collective-permute-start.10 = (bf16[256,2048]{1,0:T(8,128)(2,1)}, bf16[256,2048]{1,0:T(8,128)(2,1)}, u32[]{:S(2)}, u32[]{:S(2)}) collective-permute-start(bf16[256,2048]{1,0:T(8,128)(2,1)} %bitcast.18.refs_2_), channel_id=1, source_target_pairs={{0,3},{1,0},{2,1},{3,2},{4,7},{5,4},{6,5},{7,6},{8,11},{9,8},{10,9... | collective-permute-start | bytes 3145736 | tf_op jit(solution)/shard_map/ppermute | solution.py:304
  68.3 14.9 %all-to-all-done.2 = bf16[64,2,2048]{2,1,0:T(2,128)(2,1)S(1)} async-done(((bf16[64,2,2048]{2,1,0:T(2,128)(2,1)}), bf16[64,2,2048]{2,1,0:T(2,128)(2,1)S(1)}, u32[]{:S(2)}, u32[]{:S(2)}) %all-to-all-start.2) | async-done | bytes 524320 | tf_op jit(solution)/shard_map/all_to_all | solution.py:350
  84.1 2.5 %collective-permute-start.8 = (bf16[64,2048]{1,0:T(8,128)(2,1)S(1)}, bf16[64,2048]{1,0:T(8,128)(2,1)S(1)}, u32[]{:S(2)}, u32[]{:S(2)}) collective-permute-start(bf16[64,2048]{1,0:T(8,128)(2,1)S(1)} %slice.15), channel_id=1, source_target_pairs={{0,3},{1,0},{2,1},{3,2},{4,7},{5,4},{6,5},{7,6},{8,11},{9,8},{10,9... | collective-permute-start | bytes 786440 | tf_op jit(solution)/shard_map/ppermute | solution.py:304
  86.6 5.4 %collective-permute-done.9.refs_3_ = bf16[256,2048]{1,0:T(8,128)(2,1)} collective-permute-done((bf16[256,2048]{1,0:T(8,128)(2,1)}, bf16[256,2048]{1,0:T(8,128)(2,1)}, u32[]{:S(2)}, u32[]{:S(2)}) %collective-permute-start.9) | collective-permute-done | bytes 1048608 | tf_op jit(solution)/shard_map/ppermute | solution.py:304
  92.0 3.0 %collective-permute-start.13 = (bf16[64,2048]{1,0:T(8,128)(2,1)S(1)}, bf16[64,2048]{1,0:T(8,128)(2,1)S(1)}, u32[]{:S(2)}, u32[]{:S(2)}) collective-permute-start(bf16[64,2048]{1,0:T(8,128)(2,1)S(1)} %slice.13), channel_id=1, source_target_pairs={{0,3},{1,0},{2,1},{3,2},{4,7},{5,4},{6,5},{7,6},{8,11},{9,8},{10,9... | collective-permute-start | bytes 786440 | tf_op jit(solution)/shard_map/ppermute | solution.py:304
  95.0 24.4 %collective-permute-done.7.left0 = bf16[64,2048]{1,0:T(8,128)(2,1)S(1)} collective-permute-done((bf16[64,2048]{1,0:T(8,128)(2,1)S(1)}, bf16[64,2048]{1,0:T(8,128)(2,1)S(1)}, u32[]{:S(2)}, u32[]{:S(2)}) %collective-permute-start.7) | collective-permute-done | bytes 262176 | tf_op jit(solution)/shard_map/ppermute | solution.py:304
  119.4 2.7 %collective-permute-start.17 = (bf16[64,2048]{1,0:T(8,128)(2,1)S(1)}, bf16[64,2048]{1,0:T(8,128)(2,1)S(1)}, u32[]{:S(2)}, u32[]{:S(2)}) collective-permute-start(bf16[64,2048]{1,0:T(8,128)(2,1)S(1)} %collective-permute-done.8.right1), channel_id=1, source_target_pairs={{0,3},{1,0},{2,1},{3,2},{4,7},{5,4},{6,5},{7,6},{8,11},{9,8},{10,9... | collective-permute-start | bytes 786440 | tf_op jit(solution)/shard_map/ppermute | solution.py:304
  122.3 2.9 %near.1 = (bf16[128,256]{1,0:T(8,128)(2,1)S(1)}, bf16[64,256]{1,0:T(8,128)(2,1)S(1)}, bf16[64,256]{1,0:T(8,128)(2,1)S(1)}, bf16[2048,256]{1,0:T(8,128)(2,1)S(1)}...) custom-call(bf16[128,2048]{1,0:T(8,128)(2,1)S(1)} %reshape.23.own, ...), custom_call_target="tpu_custom_call" | custom-call | tf_op jit(solution)/shard_map/near/pallas_call | solution.py:252
  126.1 2.7 %collective-permute-start.15 = (bf16[128,256]{1,0:T(8,128)(2,1)S(1)}, bf16[128,256]{1,0:T(8,128)(2,1)S(1)}, u32[]{:S(2)}, u32[]{:S(2)}) collective-permute-start(bf16[128,256]{1,0:T(8,128)(2,1)S(1)} %get-tuple-element.32), channel_id=1, source_target_pairs={{0,3},{1,0},{2,1},{3,2},{4,7},{5,4},{6,5},{7,6},{8,11},{9,8},{10,9... | collective-permute-start | bytes 196616 | tf_op jit(solution)/shard_map/ppermute | solution.py:304
  128.8 1.8 %collective-permute-done.16.far0 = bf16[64,2048]{1,0:T(8,128)(2,1)S(1)} collective-permute-done((bf16[64,2048]{1,0:T(8,128)(2,1)S(1)}, bf16[64,2048]{1,0:T(8,128)(2,1)S(1)}, u32[]{:S(2)}, u32[]{:S(2)}) %collective-permute-start.16) | collective-permute-done | bytes 262176 | tf_op jit(solution)/shard_map/ppermute | solution.py:304
  131.1 1.3 collective-permute-start.18
  132.4 3.4 %collective-permute-done.18.far_ref = bf16[128,256]{1,0:T(8,128)(2,1)S(1)} collective-permute-done((bf16[128,256]{1,0:T(8,128)(2,1)S(1)}, bf16[128,256]{1,0:T(8,128)(2,1)S(1)}, u32[]{:S(2)}, u32[]{:S(2)}) %collective-permute-start.18) | collective-permute-done | bytes 65568 | tf_op jit(solution)/shard_map/ppermute | solution.py:304
  136.9 30.5 %all_to_all.22 = bf16[64,2,2048]{2,1,0:T(2,128)(2,1)S(1)} all-to-all(bf16[64,2,2048]{2,1,0:T(2,128)(2,1)S(1)} %reshape.24), channel_id=1, replica_groups=mesh['z'=8,'y'=4,'c'=2,'tp'=4] {'z','y','c'}, dimensions={0} | all-to-all | bytes 1048576 | tf_op jit(solution)/shard_map/all_to_all | solution.py:373
  (46 shorter events, 9.7 us)
Async XLA Ops:
  0.0 52.8 %copy-start = (bf16[32,2048]{1,0:T(8,128)(2,1)S(1)}, bf16[32,2048]{1,0:T(8,128)(2,1)}, u32[]{:S(2)}) copy-start(bf16[32,2048]{1,0:T(8,128)(2,1)} %residual_ref.1) | copy-start | bytes 393220
  0.0 52.8 %copy-start.2 = (f32[2048]{0:T(1024)S(1)}, f32[2048]{0:T(1024)}, u32[]{:S(2)}) copy-start(f32[2048]{0:T(1024)} %param.18) | copy-start | bytes 24580
  0.0 52.8 %copy-start.3 = (s32[32,2]{0,1:T(2,128)S(1)}, s32[32,2]{0,1:T(2,128)}, u32[]{:S(2)}) copy-start(s32[32,2]{0,1:T(2,128)} %param.19) | copy-start | bytes 772
  20.6 7.8 %collective-permute-start.1 = (bf16[8,144,128]{2,1,0:T(8,128)(2,1)S(1)}, bf16[8,144,128]{2,1,0:T(8,128)(2,1)S(1)}, u32[]{:S(2)}, u32[]{:S(2)}) collective-permute-start(bf16[8,144,128]{2,1,0:T(8,128)(2,1)S(1)} %all_to_all.20.refs_0_), channel_id=1, source_target_pairs={{0,8},{8,16},{16,24},{24,0},{1,9},{9,17},{17,25},{25,1},{2,10},{10... | collective-permute-start | bytes 884744 | tf_op jit(solution)/shard_map/ppermute | solution.py:304
  21.9 11.2 %collective-permute-start.3 = (bf16[8,144,128]{2,1,0:T(8,128)(2,1)S(1)}, bf16[8,144,128]{2,1,0:T(8,128)(2,1)S(1)}, u32[]{:S(2)}, u32[]{:S(2)}) collective-permute-start(bf16[8,144,128]{2,1,0:T(8,128)(2,1)S(1)} %all_to_all.20.refs_0_), channel_id=1, source_target_pairs={{0,24},{8,0},{16,8},{24,16},{1,25},{9,1},{17,9},{25,17},{2,26},{10... | collective-permute-start | bytes 884744 | tf_op jit(solution)/shard_map/ppermute | solution.py:304
  23.4 13.6 %collective-permute-start.5 = (bf16[8,144,128]{2,1,0:T(8,128)(2,1)S(1)}, bf16[8,144,128]{2,1,0:T(8,128)(2,1)S(1)}, u32[]{:S(2)}, u32[]{:S(2)}) collective-permute-start(bf16[8,144,128]{2,1,0:T(8,128)(2,1)S(1)} %all_to_all.20.refs_0_), channel_id=1, source_target_pairs={{0,16},{8,24},{16,0},{24,8},{1,17},{9,25},{17,1},{25,9},{2,18},{10... | collective-permute-start | bytes 884744 | tf_op jit(solution)/shard_map/ppermute | solution.py:304
  25.0 14.8 %collective-permute-start = (bf16[8,144,128]{2,1,0:T(8,128)(2,1)S(1)}, bf16[8,144,128]{2,1,0:T(8,128)(2,1)S(1)}, u32[]{:S(2)}, u32[]{:S(2)}) collective-permute-start(bf16[8,144,128]{2,1,0:T(8,128)(2,1)S(1)} %all_to_all.20.refs_0_), channel_id=1, source_target_pairs={{0,4},{4,0},{1,5},{5,1},{2,6},{6,2},{3,7},{7,3},{8,12},{12,8},{9,1... | collective-permute-start | bytes 884744 | tf_op jit(solution)/shard_map/ppermute | solution.py:304
  28.4 11.4 %collective-permute-start.2 = (bf16[8,144,128]{2,1,0:T(8,128)(2,1)S(1)}, bf16[8,144,128]{2,1,0:T(8,128)(2,1)S(1)}, u32[]{:S(2)}, u32[]{:S(2)}) collective-permute-start(bf16[8,144,128]{2,1,0:T(8,128)(2,1)S(1)} %collective-permute-done.1.refs_2_), channel_id=1, source_target_pairs={{0,4},{4,0},{1,5},{5,1},{2,6},{6,2},{3,7},{7,3},{8,12},{12,8},{9,1... | collective-permute-start | bytes 884744 | tf_op jit(solution)/shard_map/ppermute | solution.py:304
  33.2 6.7 %collective-permute-start.4 = (bf16[8,144,128]{2,1,0:T(8,128)(2,1)S(1)}, bf16[8,144,128]{2,1,0:T(8,128)(2,1)S(1)}, u32[]{:S(2)}, u32[]{:S(2)}) collective-permute-start(bf16[8,144,128]{2,1,0:T(8,128)(2,1)S(1)} %collective-permute-done.3.refs_4_), channel_id=1, source_target_pairs={{0,4},{4,0},{1,5},{5,1},{2,6},{6,2},{3,7},{7,3},{8,12},{12,8},{9,1... | collective-permute-start | bytes 884744 | tf_op jit(solution)/shard_map/ppermute | solution.py:304
  37.0 3.1 %collective-permute-start.6 = (bf16[8,144,128]{2,1,0:T(8,128)(2,1)S(1)}, bf16[8,144,128]{2,1,0:T(8,128)(2,1)S(1)}, u32[]{:S(2)}, u32[]{:S(2)}) collective-permute-start(bf16[8,144,128]{2,1,0:T(8,128)(2,1)S(1)} %collective-permute-done.5.refs_6_), channel_id=1, source_target_pairs={{0,4},{4,0},{1,5},{5,1},{2,6},{6,2},{3,7},{7,3},{8,12},{12,8},{9,1... | collective-permute-start | bytes 884744 | tf_op jit(solution)/shard_map/ppermute | solution.py:304
  55.1 28.1 %all-to-all-start.2 = ((bf16[64,2,2048]{2,1,0:T(2,128)(2,1)}), bf16[64,2,2048]{2,1,0:T(2,128)(2,1)S(1)}, u32[]{:S(2)}, u32[]{:S(2)}) async-start(bf16[64,2,2048]{2,1,0:T(2,128)(2,1)} %reshape.22), calls=%async_computation.2 | async-start | bytes 1048576 | tf_op jit(solution)/shard_map/all_to_all | solution.py:350
  65.5 26.5 %collective-permute-start.9 = (bf16[256,2048]{1,0:T(8,128)(2,1)}, bf16[256,2048]{1,0:T(8,128)(2,1)}, u32[]{:S(2)}, u32[]{:S(2)}) collective-permute-start(bf16[256,2048]{1,0:T(8,128)(2,1)} %bitcast.18.refs_2_), channel_id=1, source_target_pairs={{0,1},{1,2},{2,3},{3,0},{4,5},{5,6},{6,7},{7,4},{8,9},{9,10},{10,1... | collective-permute-start | bytes 3145736 | tf_op jit(solution)/shard_map/ppermute | solution.py:304
  65.9 26.1 %collective-permute-start.10 = (bf16[256,2048]{1,0:T(8,128)(2,1)}, bf16[256,2048]{1,0:T(8,128)(2,1)}, u32[]{:S(2)}, u32[]{:S(2)}) collective-permute-start(bf16[256,2048]{1,0:T(8,128)(2,1)} %bitcast.18.refs_2_), channel_id=1, source_target_pairs={{0,3},{1,0},{2,1},{3,2},{4,7},{5,4},{6,5},{7,6},{8,11},{9,8},{10,9... | collective-permute-start | bytes 3145736 | tf_op jit(solution)/shard_map/ppermute | solution.py:304
  68.3 54.0 %collective-permute-start.11 = (bf16[256,2048]{1,0:T(8,128)(2,1)}, bf16[256,2048]{1,0:T(8,128)(2,1)}, u32[]{:S(2)}, u32[]{:S(2)}) collective-permute-start(bf16[256,2048]{1,0:T(8,128)(2,1)} %bitcast.18.refs_2_), channel_id=1, source_target_pairs={{0,2},{1,3},{2,0},{3,1},{4,6},{5,7},{6,4},{7,5},{8,10},{9,11},{10,... | collective-permute-start | bytes 3145736 | tf_op jit(solution)/shard_map/ppermute | solution.py:304
  83.7 35.7 %collective-permute-start.7 = (bf16[64,2048]{1,0:T(8,128)(2,1)S(1)}, bf16[64,2048]{1,0:T(8,128)(2,1)S(1)}, u32[]{:S(2)}, u32[]{:S(2)}) collective-permute-start(bf16[64,2048]{1,0:T(8,128)(2,1)S(1)} %slice.13), channel_id=1, source_target_pairs={{0,1},{1,2},{2,3},{3,0},{4,5},{5,6},{6,7},{7,4},{8,9},{9,10},{10,1... | collective-permute-start | bytes 786440 | tf_op jit(solution)/shard_map/ppermute | solution.py:304
  84.1 35.2 %collective-permute-start.8 = (bf16[64,2048]{1,0:T(8,128)(2,1)S(1)}, bf16[64,2048]{1,0:T(8,128)(2,1)S(1)}, u32[]{:S(2)}, u32[]{:S(2)}) collective-permute-start(bf16[64,2048]{1,0:T(8,128)(2,1)S(1)} %slice.15), channel_id=1, source_target_pairs={{0,3},{1,0},{2,1},{3,2},{4,7},{5,4},{6,5},{7,6},{8,11},{9,8},{10,9... | collective-permute-start | bytes 786440 | tf_op jit(solution)/shard_map/ppermute | solution.py:304
  92.0 33.1 %collective-permute-start.12 = (bf16[64,2048]{1,0:T(8,128)(2,1)S(1)}, bf16[64,2048]{1,0:T(8,128)(2,1)S(1)}, u32[]{:S(2)}, u32[]{:S(2)}) collective-permute-start(bf16[64,2048]{1,0:T(8,128)(2,1)S(1)} %slice.15), channel_id=1, source_target_pairs={{0,1},{1,2},{2,3},{3,0},{4,5},{5,6},{6,7},{7,4},{8,9},{9,10},{10,1... | collective-permute-start | bytes 786440 | tf_op jit(solution)/shard_map/ppermute | solution.py:304
  92.0 33.2 %collective-permute-start.13 = (bf16[64,2048]{1,0:T(8,128)(2,1)S(1)}, bf16[64,2048]{1,0:T(8,128)(2,1)S(1)}, u32[]{:S(2)}, u32[]{:S(2)}) collective-permute-start(bf16[64,2048]{1,0:T(8,128)(2,1)S(1)} %slice.13), channel_id=1, source_target_pairs={{0,3},{1,0},{2,1},{3,2},{4,7},{5,4},{6,5},{7,6},{8,11},{9,8},{10,9... | collective-permute-start | bytes 786440 | tf_op jit(solution)/shard_map/ppermute | solution.py:304
  119.4 11.2 %collective-permute-start.16 = (bf16[64,2048]{1,0:T(8,128)(2,1)S(1)}, bf16[64,2048]{1,0:T(8,128)(2,1)S(1)}, u32[]{:S(2)}, u32[]{:S(2)}) collective-permute-start(bf16[64,2048]{1,0:T(8,128)(2,1)S(1)} %collective-permute-done.7.left0), channel_id=1, source_target_pairs={{0,1},{1,2},{2,3},{3,0},{4,5},{5,6},{6,7},{7,4},{8,9},{9,10},{10,1... | collective-permute-start | bytes 786440 | tf_op jit(solution)/shard_map/ppermute | solution.py:304
  119.4 11.2 %collective-permute-start.17 = (bf16[64,2048]{1,0:T(8,128)(2,1)S(1)}, bf16[64,2048]{1,0:T(8,128)(2,1)S(1)}, u32[]{:S(2)}, u32[]{:S(2)}) collective-permute-start(bf16[64,2048]{1,0:T(8,128)(2,1)S(1)} %collective-permute-done.8.right1), channel_id=1, source_target_pairs={{0,3},{1,0},{2,1},{3,2},{4,7},{5,4},{6,5},{7,6},{8,11},{9,8},{10,9... | collective-permute-start | bytes 786440 | tf_op jit(solution)/shard_map/ppermute | solution.py:304
  126.0 6.4 %collective-permute-start.14 = (bf16[128,256]{1,0:T(8,128)(2,1)S(1)}, bf16[128,256]{1,0:T(8,128)(2,1)S(1)}, u32[]{:S(2)}, u32[]{:S(2)}) collective-permute-start(bf16[128,256]{1,0:T(8,128)(2,1)S(1)} %get-tuple-element.31), channel_id=1, source_target_pairs={{0,1},{1,2},{2,3},{3,0},{4,5},{5,6},{6,7},{7,4},{8,9},{9,10},{10,1... | collective-permute-start | bytes 196616 | tf_op jit(solution)/shard_map/ppermute | solution.py:304
  126.1 6.3 %collective-permute-start.15 = (bf16[128,256]{1,0:T(8,128)(2,1)S(1)}, bf16[128,256]{1,0:T(8,128)(2,1)S(1)}, u32[]{:S(2)}, u32[]{:S(2)}) collective-permute-start(bf16[128,256]{1,0:T(8,128)(2,1)S(1)} %get-tuple-element.32), channel_id=1, source_target_pairs={{0,3},{1,0},{2,1},{3,2},{4,7},{5,4},{6,5},{7,6},{8,11},{9,8},{10,9... | collective-permute-start | bytes 196616 | tf_op jit(solution)/shard_map/ppermute | solution.py:304
  131.1 36.5 %copy-start.4 = (f32[32,2]{0,1:T(2,128)S(1)}, f32[32,2]{0,1:T(2,128)}, u32[]{:S(2)}) copy-start(f32[32,2]{0,1:T(2,128)} %param.20) | copy-start | bytes 772
  131.1 4.7 %collective-permute-start.18 = (bf16[128,256]{1,0:T(8,128)(2,1)S(1)}, bf16[128,256]{1,0:T(8,128)(2,1)S(1)}, u32[]{:S(2)}, u32[]{:S(2)}) collective-permute-start(bf16[128,256]{1,0:T(8,128)(2,1)S(1)} %shard_map.121), channel_id=1, source_target_pairs={{0,2},{1,3},{2,0},{3,1},{4,6},{5,7},{6,4},{7,5},{8,10},{9,11},{10,... | collective-permute-start | bytes 196616 | tf_op jit(solution)/shard_map/ppermute | solution.py:304
  (1 other events, 0.8 us)

commit v2 on v1

--- a/solution.py
+++ b/solution.py
@@ -15,7 +15,6 @@
 ROW = 32
 D = 2048
 BLOCK = TOK + 16
-GROUP = 2
 BF16_MAX = 3.3895313892515355e38
 NEG = -3.0e38
 F32 = jnp.float32
@@ -57,19 +56,18 @@
     for copy in copies:
         copy.wait()
     hi, mid, low = parts3(gates_ref[...])
-    rows = [hi.astype(F32), mid.astype(F32), low.astype(F32), jnp.zeros((4, TOK), F32)]
-    gates = jnp.concatenate(rows, axis=0).astype(BF16)
-    for z in range(NZ):
-        out_ref[z, 0:HEAD, :] = keys_ref[...]
-        out_ref[z, HEAD : HEAD + 16, :] = gates
-        out_ref[z, HEAD + 16 : BLOCK, :] = values_ref[...]
+    ones = jnp.where(lax.broadcasted_iota(jnp.int32, (HEADS, TOK), 0) == 1, 1.0, 0.0)
+    rows = [hi.astype(F32), mid.astype(F32), low.astype(F32), ones]
+    out_ref[0:HEAD, :] = keys_ref[...]
+    out_ref[HEAD : HEAD + 16, :] = jnp.concatenate(rows, axis=0).astype(BF16)
+    out_ref[HEAD + 16 : BLOCK, :] = values_ref[...]
 
 
 def pack(keys, values, gates):
     hbm = pl.BlockSpec(memory_space=pltpu.HBM)
     return pl.pallas_call(
         pack_kernel,
-        out_shape=jax.ShapeDtypeStruct((NZ, BLOCK, TOK), BF16),
+        out_shape=jax.ShapeDtypeStruct((BLOCK, TOK), BF16),
         in_specs=[hbm] * 3,
         out_specs=pl.BlockSpec(memory_space=pltpu.VMEM),
         scratch_shapes=[
@@ -99,80 +97,58 @@
 
 def attend_kernel(count, place_ref, query_ref, source_ref, *refs):
     chunks, refs = refs[:count], refs[count:]
-    out_ref, target_ref, m_ref, l_ref, acc_ref, sem = refs
+    out_ref, target_ref, m_ref, acc_ref, sem = refs
     copy = pltpu.make_async_copy(source_ref, target_ref, sem)
     copy.start()
-    own_z, own_order = place_ref[0], place_ref[1]
     queries = query_ref[...]
     total_rows = HEADS * TOK
-    blocks = GROUP * count
     row_of_gate = lax.broadcasted_iota(jnp.int32, (16, TOK), 0)
 
-    def folded(weights):
-        total = weights[:, 0:TOK]
-        for j in range(1, blocks):
-            total = total + weights[:, j * TOK : (j + 1) * TOK]
-        return total
-
-    def step(base, first):
-        key_rows, value_rows, shifts = [], [], []
-        for g in range(GROUP):
-            for j, ref in enumerate(chunks):
-                gates = ref[base + g, HEAD : HEAD + 16, :]
-                if first:
-                    order = place_ref[2 + j]
-                    seen = (base + g < own_z) | ((base + g == own_z) & (order <= own_order))
-                    bar = jnp.where(seen, 0.0, -NEG).astype(BF16)
-                    gates = jnp.where(row_of_gate == 3 * HEADS, bar, gates)
-                    shifts.append(jnp.where((base + g == own_z) & (order == own_order), 0, TOK))
-                key_rows.append(jnp.concatenate([ref[base + g, 0:HEAD, :], gates], axis=0))
-                value_rows.append(ref[base + g, HEAD + 16 : BLOCK, :])
+    def step(slot, fresh):
+        key_rows = []
+        for j, ref in enumerate(chunks):
+            if fresh:
+                bar = jnp.where(place_ref[1 + j] != 0, 0.0, -NEG).astype(BF16)
+                gates = ref[slot, HEAD : HEAD + 16, :]
+                gates = jnp.where(row_of_gate == 3 * HEADS, bar, gates)
+                key_rows.append(jnp.concatenate([ref[slot, 0:HEAD, :], gates], axis=0))
+            else:
+                key_rows.append(ref[slot, 0 : HEAD + 16, :])
+        value_rows = jnp.concatenate([ref[slot, HEAD:BLOCK, :] for ref in chunks], axis=1)
         scores = dot(queries, jnp.concatenate(key_rows, axis=1))
-        if first:
-            ahead = lax.broadcasted_iota(jnp.int32, (total_rows, TOK), 0) % TOK
-            ahead = ahead - lax.broadcasted_iota(jnp.int32, (total_rows, TOK), 1)
-            pieces = []
-            for i in range(blocks):
-                piece = scores[:, i * TOK : (i + 1) * TOK]
-                if i % count == 0:
-                    piece = jnp.where(ahead + shifts[i] >= 0, piece, NEG)
-                pieces.append(piece)
-            scores = jnp.concatenate(pieces, axis=1)
+        if fresh:
+            row = lax.broadcasted_iota(jnp.int32, (total_rows, TOK), 0) % TOK
+            col = lax.broadcasted_iota(jnp.int32, (total_rows, TOK), 1)
+            own = jnp.where(row >= col, scores[:, :TOK], NEG)
+            scores = jnp.concatenate([own, scores[:, TOK:]], axis=1)
         peak = jnp.max(scores, axis=1, keepdims=True)
-        if first:
+        if fresh:
             peak = jnp.broadcast_to(peak, (total_rows, TOK))
         else:
             before = m_ref[...]
             peak = jnp.maximum(before, peak)
-        weights = jnp.exp(scores - jnp.concatenate([peak] * blocks, axis=1))
+        weights = jnp.exp(scores - jnp.concatenate([peak] * count, axis=1))
         product = lax.dot_general(
-            weights.astype(BF16),
-            jnp.concatenate(value_rows, axis=1),
-            (((1,), (1,)), ((), ())),
-            preferred_element_type=F32,
+            weights.astype(BF16), value_rows, (((1,), (1,)), ((), ())), preferred_element_type=F32
         )
         m_ref[...] = peak
-        if first:
-            l_ref[...] = folded(weights)
+        if fresh:
             acc_ref[...] = product
         else:
-            shrink = jnp.exp(before - peak)
-            l_ref[...] = l_ref[...] * shrink + folded(weights)
-            acc_ref[...] = acc_ref[...] * shrink[:, :HEAD] + product
-
-    groups = own_z // GROUP
-    step(groups * GROUP, True)
-
-    def body(group, carry):
-        step(group * GROUP, False)
+            acc_ref[...] = acc_ref[...] * jnp.exp(before - peak)[:, : HEAD + 16] + product
+
+    step(0, True)
+
+    def body(slot, carry):
+        step(slot, False)
         return carry
 
-    lax.fori_loop(0, groups, body, 0)
+    lax.fori_loop(1, place_ref[0] + 1, body, 0)
+    ones = 3 * HEADS + 1
     done = []
     for h in range(HEADS):
         here = slice(h * TOK, (h + 1) * TOK)
-        total = jnp.sum(l_ref[here, :], axis=1, keepdims=True)
-        done.append((acc_ref[here, :] / total).astype(BF16))
+        done.append((acc_ref[here, 16:] / acc_ref[here, ones : ones + 1]).astype(BF16))
     out_ref[...] = jnp.concatenate(done, axis=1)
     copy.wait()
 
@@ -192,8 +168,7 @@
         out_specs=[vmem] * 2,
         scratch_shapes=[
             pltpu.VMEM((total_rows, TOK), F32),
-            pltpu.VMEM((total_rows, TOK), F32),
-            pltpu.VMEM((total_rows, HEAD), F32),
+            pltpu.VMEM((total_rows, HEAD + 16), F32),
             pltpu.SemaphoreType.DMA,
         ],
         compiler_params=PARAMS,
@@ -321,17 +296,20 @@
     z, y, c = lax.axis_index("z"), lax.axis_index("y"), lax.axis_index("c")
     down_own = w_down[0]
     down_left, down_right = moved(down_own, "tp", 1), moved(down_own, "tp", -1)
-    copies = pack(keys.T, values.T, forget_prefix_log.T)
-    own = lax.all_to_all(copies, "z", 0, 0, tiled=True)
+    block = pack(keys.T, values.T, forget_prefix_log.T)
     (rows_of_q,) = call(query_kernel, [((HEADS * TOK, HEAD + 16), BF16)], queries)
-    chunks = [own, moved(own, "c", 1)]
-    place = [z, y * NC + c, y * NC + c, y * NC + 1 - c]
-    for step in (1, 3, 2):
-        chunk = moved(own, "y", step)
-        from_y = (y - step) % NY
-        chunks += [chunk, moved(chunk, "c", 1)]
-        place += [from_y * NC + c, from_y * NC + 1 - c]
-    place = jnp.stack(place).astype(jnp.int32)
+    fours = jnp.stack([block] + [moved(block, "z", step) for step in (2, 4, 6)])
+    others = lax.ppermute(fours, "z", [(i, i ^ 1) for i in range(NZ)])
+    own_order = y * NC + c
+    chunks, kinds = [], []
+    for name, group in (("first", fours), ("second", others)):
+        for step in (0, 1, 3, 2):
+            chunk = moved(group, "y", step) if step else group
+            chunks += [chunk, moved(chunk, "c", 1)]
+            for parity in (c, 1 - c):
+                seen = (y - step) % NY * NC + parity <= own_order
+                kinds.append(jnp.where(seen, 1, 0) if name == "first" else z % 2)
+    place = jnp.stack([z // 2] + kinds).astype(jnp.int32)
     attended, out_w = attend(place, rows_of_q, out_weight, chunks)
 
     heads = lax.all_to_all(attended.reshape(NT, ROW, -1), "tp", 0, 0, tiled=True)

time: 169 us -> 166 us (0.982)
  blocking collectives: 58.6 us -> 38.9 us
  starting transfers between devices: 43.9 us -> 56.6 us
  waiting for transfers between devices: 50.1 us -> 55 us
    all_to_all x1 -> x0, blocking collectives: 19.8 us -> none  [shards(): own = lax.all_to_all(copies, 'z', 0, 0, tiled=True)]
    ppermute x19 -> x29, starting transfers between devices: 33.5 us -> 44.3 us  [moved(): return lax.ppermute(x, axis, [(i, (i + by) % size) for i in range(size)])]
    ppermute x19 -> x29, waiting for transfers between devices: 35.1 us -> 40.1 us  [moved(): return lax.ppermute(x, axis, [(i, (i + by) % size) for i in range(size)])]
  transfers between devices with their start and end apart: 20 -> 31, of which waited for: 6 -> 7; matrix products, arithmetic and copies ran while one was open for 1% -> 1% of each run, Pallas kernels for 3% -> 3%
where the time goes in v2:
time: 166 us
  starting transfers between devices  56.6 us (34%)
  waiting for transfers between devices  55 us (33%)
  blocking collectives  38.9 us (23%)
  Pallas kernels  11.8 us (7%)
  local copies, waits for them, and re-layouts  3.39 us (2%)
    ppermute x29, starting transfers between devices, moved(): return lax.ppermute(x, axis, [(i, (i + by) % size) for i in range(size)])  44.3 us
    ppermute x29, waiting for transfers between devices, moved(): return lax.ppermute(x, axis, [(i, (i + by) % size) for i in range(size)])  40.1 us
    all_to_all x1, blocking collectives, shards(): lax.all_to_all(expert_out.reshape(64, 2, D), SP, 0, 0, tiled=True)  30.6 us
    all_to_all x1, waiting for transfers between devices, shards(): lax.all_to_all(rows.reshape(64, 2, D), SP, 0, 0, tiled=True).reshape(TOK, D)  14.9 us
    all_to_all x1, starting transfers between devices, shards(): lax.all_to_all(rows.reshape(64, 2, D), SP, 0, 0, tiled=True).reshape(TOK, D)  11.6 us
    all_to_all x1, blocking collectives, shards(): lax.all_to_all(attended.reshape(NT, ROW, -1), 'tp', 0, 0, tiled=True)  8.29 us
    pallas_call x6, Pallas kernels, call(): pl.pallas_call(kernel, out_shape=[jax.ShapeDtypeStruct(s, t) for s, t in...  4.48 us
    pallas_call x1, Pallas kernels, attend(): pl.pallas_call(functools.partial(attend_kernel, len(chunks)), out_shape=[...  3.65 us
  transfers between devices with their start and end apart: 31, of which 7 were waited for; matrix products, arithmetic and copies ran while one was open for 1% of the time, Pallas kernels for 3%

profile of v2, /device:TPU:1, one launch (start us, length us, event | category | flops | bytes accessed | tf_op | source)
XLA Modules:
  0.0 165.9 jit_solution(14830090951160997071)
XLA Ops:
  0.8 6.9 %collective-permute-start.2 = (bf16[144,128]{1,0:T(8,128)(2,1)S(1)}, bf16[144,128]{1,0:T(8,128)(2,1)S(1)}, u32[]{:S(2)}, u32[]{:S(2)}) collective-permute-start(bf16[144,128]{1,0:T(8,128)(2,1)S(1)} %pack.1), channel_id=1, source_target_pairs={{0,192},{32,224},{64,0},{96,32},{128,64},{160,96},{192,128},{224,1... | collective-permute-start | bytes 110600 | tf_op jit(solution)/shard_map/ppermute | solution.py:279
  8.7 2.3 %collective-permute-start = (bf16[144,128]{1,0:T(8,128)(2,1)S(1)}, bf16[144,128]{1,0:T(8,128)(2,1)S(1)}, u32[]{:S(2)}, u32[]{:S(2)}) collective-permute-start(bf16[144,128]{1,0:T(8,128)(2,1)S(1)} %pack.1), channel_id=1, source_target_pairs={{0,64},{32,96},{64,128},{96,160},{128,192},{160,224},{192,0},{224,... | collective-permute-start | bytes 110600 | tf_op jit(solution)/shard_map/ppermute | solution.py:279
  11.0 3.5 %collective-permute-done.1 = bf16[144,128]{1,0:T(8,128)(2,1)S(1)} collective-permute-done((bf16[144,128]{1,0:T(8,128)(2,1)S(1)}, bf16[144,128]{1,0:T(8,128)(2,1)S(1)}, u32[]{:S(2)}, u32[]{:S(2)}) %collective-permute-start.1) | collective-permute-done | bytes 36896 | tf_op jit(solution)/shard_map/ppermute | solution.py:279
  18.1 2.8 %collective-permute-start.3 = (bf16[4,144,128]{2,1,0:T(8,128)(2,1)S(1)}, bf16[4,144,128]{2,1,0:T(8,128)(2,1)S(1)}, u32[]{:S(2)}, u32[]{:S(2)}) collective-permute-start(bf16[4,144,128]{2,1,0:T(8,128)(2,1)S(1)} %pad_maximum_fusion.refs_0_), channel_id=1, source_target_pairs={{0,4},{4,0},{1,5},{5,1},{2,6},{6,2},{3,7},{7,3},{8,12},{12,8},{9,1... | collective-permute-start | bytes 442376 | tf_op jit(solution)/shard_map/ppermute | solution.py:279
  21.0 1.7 %collective-permute-start.8 = (bf16[4,144,128]{2,1,0:T(8,128)(2,1)S(1)}, bf16[4,144,128]{2,1,0:T(8,128)(2,1)S(1)}, u32[]{:S(2)}, u32[]{:S(2)}) collective-permute-start(bf16[4,144,128]{2,1,0:T(8,128)(2,1)S(1)} %pad_maximum_fusion.refs_0_), channel_id=1, source_target_pairs={{0,16},{8,24},{16,0},{24,8},{1,17},{9,25},{17,1},{25,9},{2,18},{10... | collective-permute-start | bytes 442376 | tf_op jit(solution)/shard_map/ppermute | solution.py:279
  26.3 1.6 collective-permute-done.8.refs_6_
  27.9 1.7 %collective-permute-start.16 = (bf16[4,144,128]{2,1,0:T(8,128)(2,1)S(1)}, bf16[4,144,128]{2,1,0:T(8,128)(2,1)S(1)}, u32[]{:S(2)}, u32[]{:S(2)}) collective-permute-start(bf16[4,144,128]{2,1,0:T(8,128)(2,1)S(1)} %collective-permute-done.10.refs_8_), channel_id=1, source_target_pairs={{0,16},{8,24},{16,0},{24,8},{1,17},{9,25},{17,1},{25,9},{2,18},{10... | collective-permute-start | bytes 442376 | tf_op jit(solution)/shard_map/ppermute | solution.py:279
  29.6 1.6 collective-permute-start.11
  31.9 2.4 %collective-permute-start.15 = (bf16[4,144,128]{2,1,0:T(8,128)(2,1)S(1)}, bf16[4,144,128]{2,1,0:T(8,128)(2,1)S(1)}, u32[]{:S(2)}, u32[]{:S(2)}) collective-permute-start(bf16[4,144,128]{2,1,0:T(8,128)(2,1)S(1)} %collective-permute-done.14.refs_12_), channel_id=1, source_target_pairs={{0,4},{4,0},{1,5},{5,1},{2,6},{6,2},{3,7},{7,3},{8,12},{12,8},{9,1... | collective-permute-start | bytes 442376 | tf_op jit(solution)/shard_map/ppermute | solution.py:279
  36.8 3.6 %attend.1 = (bf16[128,256]{1,0:T(8,128)(2,1)S(1)}, bf16[1024,2048]{1,0:T(8,128)(2,1)S(1)}) custom-call(s32[17]{0:T(128)S(1)} %stack.65.place_ref, bf16[512,80]{1,0:T(8,128)(2,1)S(1)} %shard_map.118.query_ref, bf16[1024,2048]{1,0:T(8,128)(2,1)} %source_ref.1, bf16[4,144,128]{2,1,0:T(8,128)(2,1)S(1)} %pad_maximum_fusion.refs_0_, ...), custom_call_target="tpu_custom_call" | custom-call | tf_op jit(solution)/shard_map/attend/pallas_call | solution.py:159
  40.4 8.3 %all_to_all.15.att_ref = bf16[4,32,256]{2,1,0:T(8,128)(2,1)S(1)} all-to-all(bf16[4,32,256]{2,1,0:T(8,128)(2,1)S(1)} %bitcast.25), channel_id=1, replica_groups=mesh['z'=8,'y'=4,'c'=2,'tp'=4] {'tp'}, dimensions={0} | all-to-all | bytes 131072 | tf_op jit(solution)/shard_map/all_to_all | solution.py:315
  51.0 11.6 %all-to-all-start.1 = ((bf16[64,2,2048]{2,1,0:T(2,128)(2,1)}), bf16[64,2,2048]{2,1,0:T(2,128)(2,1)S(1)}, u32[]{:S(2)}, u32[]{:S(2)}) async-start(bf16[64,2,2048]{2,1,0:T(2,128)(2,1)} %reshape.22), calls=%async_computation.1 | async-start | bytes 1048576 | tf_op jit(solution)/shard_map/all_to_all | solution.py:328
  63.0 2.4 %collective-permute-start.21 = (bf16[256,2048]{1,0:T(8,128)(2,1)}, bf16[256,2048]{1,0:T(8,128)(2,1)}, u32[]{:S(2)}, u32[]{:S(2)}) collective-permute-start(bf16[256,2048]{1,0:T(8,128)(2,1)} %bitcast.23.refs_2_), channel_id=1, source_target_pairs={{0,3},{1,0},{2,1},{3,2},{4,7},{5,4},{6,5},{7,6},{8,11},{9,8},{10,9... | collective-permute-start | bytes 3145736 | tf_op jit(solution)/shard_map/ppermute | solution.py:279
  65.4 14.9 %all-to-all-done.1 = bf16[64,2,2048]{2,1,0:T(2,128)(2,1)S(1)} async-done(((bf16[64,2,2048]{2,1,0:T(2,128)(2,1)}), bf16[64,2,2048]{2,1,0:T(2,128)(2,1)S(1)}, u32[]{:S(2)}, u32[]{:S(2)}) %all-to-all-start.1) | async-done | bytes 524320 | tf_op jit(solution)/shard_map/all_to_all | solution.py:328
  81.2 2.5 %collective-permute-start.19 = (bf16[64,2048]{1,0:T(8,128)(2,1)S(1)}, bf16[64,2048]{1,0:T(8,128)(2,1)S(1)}, u32[]{:S(2)}, u32[]{:S(2)}) collective-permute-start(bf16[64,2048]{1,0:T(8,128)(2,1)S(1)} %slice.15), channel_id=1, source_target_pairs={{0,3},{1,0},{2,1},{3,2},{4,7},{5,4},{6,5},{7,6},{8,11},{9,8},{10,9... | collective-permute-start | bytes 786440 | tf_op jit(solution)/shard_map/ppermute | solution.py:279
  83.7 5.4 %collective-permute-done.20.refs_3_ = bf16[256,2048]{1,0:T(8,128)(2,1)} collective-permute-done((bf16[256,2048]{1,0:T(8,128)(2,1)}, bf16[256,2048]{1,0:T(8,128)(2,1)}, u32[]{:S(2)}, u32[]{:S(2)}) %collective-permute-start.20) | collective-permute-done | bytes 1048608 | tf_op jit(solution)/shard_map/ppermute | solution.py:279
  89.1 3.0 %collective-permute-start.24 = (bf16[64,2048]{1,0:T(8,128)(2,1)S(1)}, bf16[64,2048]{1,0:T(8,128)(2,1)S(1)}, u32[]{:S(2)}, u32[]{:S(2)}) collective-permute-start(bf16[64,2048]{1,0:T(8,128)(2,1)S(1)} %slice.13), channel_id=1, source_target_pairs={{0,3},{1,0},{2,1},{3,2},{4,7},{5,4},{6,5},{7,6},{8,11},{9,8},{10,9... | collective-permute-start | bytes 786440 | tf_op jit(solution)/shard_map/ppermute | solution.py:279
  92.1 24.4 %collective-permute-done.18.left0 = bf16[64,2048]{1,0:T(8,128)(2,1)S(1)} collective-permute-done((bf16[64,2048]{1,0:T(8,128)(2,1)S(1)}, bf16[64,2048]{1,0:T(8,128)(2,1)S(1)}, u32[]{:S(2)}, u32[]{:S(2)}) %collective-permute-start.18) | collective-permute-done | bytes 262176 | tf_op jit(solution)/shard_map/ppermute | solution.py:279
  116.5 2.7 %collective-permute-start.28 = (bf16[64,2048]{1,0:T(8,128)(2,1)S(1)}, bf16[64,2048]{1,0:T(8,128)(2,1)S(1)}, u32[]{:S(2)}, u32[]{:S(2)}) collective-permute-start(bf16[64,2048]{1,0:T(8,128)(2,1)S(1)} %collective-permute-done.19.right1), channel_id=1, source_target_pairs={{0,3},{1,0},{2,1},{3,2},{4,7},{5,4},{6,5},{7,6},{8,11},{9,8},{10,9... | collective-permute-start | bytes 786440 | tf_op jit(solution)/shard_map/ppermute | solution.py:279
  119.3 2.9 %near.1 = (bf16[128,256]{1,0:T(8,128)(2,1)S(1)}, bf16[64,256]{1,0:T(8,128)(2,1)S(1)}, bf16[64,256]{1,0:T(8,128)(2,1)S(1)}, bf16[2048,256]{1,0:T(8,128)(2,1)S(1)}...) custom-call(bf16[128,2048]{1,0:T(8,128)(2,1)S(1)} %reshape.23.own, ...), custom_call_target="tpu_custom_call" | custom-call | tf_op jit(solution)/shard_map/near/pallas_call | solution.py:227
  123.2 2.7 %collective-permute-start.26 = (bf16[128,256]{1,0:T(8,128)(2,1)S(1)}, bf16[128,256]{1,0:T(8,128)(2,1)S(1)}, u32[]{:S(2)}, u32[]{:S(2)}) collective-permute-start(bf16[128,256]{1,0:T(8,128)(2,1)S(1)} %get-tuple-element.32), channel_id=1, source_target_pairs={{0,3},{1,0},{2,1},{3,2},{4,7},{5,4},{6,5},{7,6},{8,11},{9,8},{10,9... | collective-permute-start | bytes 196616 | tf_op jit(solution)/shard_map/ppermute | solution.py:279
  125.9 1.8 %collective-permute-done.27.far0 = bf16[64,2048]{1,0:T(8,128)(2,1)S(1)} collective-permute-done((bf16[64,2048]{1,0:T(8,128)(2,1)S(1)}, bf16[64,2048]{1,0:T(8,128)(2,1)S(1)}, u32[]{:S(2)}, u32[]{:S(2)}) %collective-permute-start.27) | collective-permute-done | bytes 262176 | tf_op jit(solution)/shard_map/ppermute | solution.py:279
  129.5 3.4 %collective-permute-done.29.far_ref = bf16[128,256]{1,0:T(8,128)(2,1)S(1)} collective-permute-done((bf16[128,256]{1,0:T(8,128)(2,1)S(1)}, bf16[128,256]{1,0:T(8,128)(2,1)S(1)}, u32[]{:S(2)}, u32[]{:S(2)}) %collective-permute-start.29) | collective-permute-done | bytes 65568 | tf_op jit(solution)/shard_map/ppermute | solution.py:279
  133.9 30.6 %all_to_all.16 = bf16[64,2,2048]{2,1,0:T(2,128)(2,1)S(1)} all-to-all(bf16[64,2,2048]{2,1,0:T(2,128)(2,1)S(1)} %reshape.24), channel_id=1, replica_groups=mesh['z'=8,'y'=4,'c'=2,'tp'=4] {'z','y','c'}, dimensions={0} | all-to-all | bytes 1048576 | tf_op jit(solution)/shard_map/all_to_all | solution.py:351
  (68 shorter events, 21.1 us)
Async XLA Ops:
  0.8 10.2 %collective-permute-start.2 = (bf16[144,128]{1,0:T(8,128)(2,1)S(1)}, bf16[144,128]{1,0:T(8,128)(2,1)S(1)}, u32[]{:S(2)}, u32[]{:S(2)}) collective-permute-start(bf16[144,128]{1,0:T(8,128)(2,1)S(1)} %pack.1), channel_id=1, source_target_pairs={{0,192},{32,224},{64,0},{96,32},{128,64},{160,96},{192,128},{224,1... | collective-permute-start | bytes 110600 | tf_op jit(solution)/shard_map/ppermute | solution.py:279
  7.8 6.7 %collective-permute-start.1 = (bf16[144,128]{1,0:T(8,128)(2,1)S(1)}, bf16[144,128]{1,0:T(8,128)(2,1)S(1)}, u32[]{:S(2)}, u32[]{:S(2)}) collective-permute-start(bf16[144,128]{1,0:T(8,128)(2,1)S(1)} %pack.1), channel_id=1, source_target_pairs={{0,128},{32,160},{64,192},{96,224},{128,0},{160,32},{192,64},{224,... | collective-permute-start | bytes 110600 | tf_op jit(solution)/shard_map/ppermute | solution.py:279
  14.5 8.2 %collective-permute-start.4 = (bf16[4,144,128]{2,1,0:T(8,128)(2,1)S(1)}, bf16[4,144,128]{2,1,0:T(8,128)(2,1)S(1)}, u32[]{:S(2)}, u32[]{:S(2)}) collective-permute-start(bf16[4,144,128]{2,1,0:T(8,128)(2,1)S(1)} %pad_maximum_fusion.refs_0_), channel_id=1, source_target_pairs={{0,8},{8,16},{16,24},{24,0},{1,9},{9,17},{17,25},{25,1},{2,10},{10... | collective-permute-start | bytes 442376 | tf_op jit(solution)/shard_map/ppermute | solution.py:279
  15.9 7.3 %collective-permute-start.6 = (bf16[4,144,128]{2,1,0:T(8,128)(2,1)S(1)}, bf16[4,144,128]{2,1,0:T(8,128)(2,1)S(1)}, u32[]{:S(2)}, u32[]{:S(2)}) collective-permute-start(bf16[4,144,128]{2,1,0:T(8,128)(2,1)S(1)} %pad_maximum_fusion.refs_0_), channel_id=1, source_target_pairs={{0,24},{8,0},{16,8},{24,16},{1,25},{9,1},{17,9},{25,17},{2,26},{10... | collective-permute-start | bytes 442376 | tf_op jit(solution)/shard_map/ppermute | solution.py:279
  18.1 6.7 %collective-permute-start.3 = (bf16[4,144,128]{2,1,0:T(8,128)(2,1)S(1)}, bf16[4,144,128]{2,1,0:T(8,128)(2,1)S(1)}, u32[]{:S(2)}, u32[]{:S(2)}) collective-permute-start(bf16[4,144,128]{2,1,0:T(8,128)(2,1)S(1)} %pad_maximum_fusion.refs_0_), channel_id=1, source_target_pairs={{0,4},{4,0},{1,5},{5,1},{2,6},{6,2},{3,7},{7,3},{8,12},{12,8},{9,1... | collective-permute-start | bytes 442376 | tf_op jit(solution)/shard_map/ppermute | solution.py:279
  21.0 6.9 %collective-permute-start.8 = (bf16[4,144,128]{2,1,0:T(8,128)(2,1)S(1)}, bf16[4,144,128]{2,1,0:T(8,128)(2,1)S(1)}, u32[]{:S(2)}, u32[]{:S(2)}) collective-permute-start(bf16[4,144,128]{2,1,0:T(8,128)(2,1)S(1)} %pad_maximum_fusion.refs_0_), channel_id=1, source_target_pairs={{0,16},{8,24},{16,0},{24,8},{1,17},{9,25},{17,1},{25,9},{2,18},{10... | collective-permute-start | bytes 442376 | tf_op jit(solution)/shard_map/ppermute | solution.py:279
  22.7 6.9 %collective-permute-start.5 = (bf16[4,144,128]{2,1,0:T(8,128)(2,1)S(1)}, bf16[4,144,128]{2,1,0:T(8,128)(2,1)S(1)}, u32[]{:S(2)}, u32[]{:S(2)}) collective-permute-start(bf16[4,144,128]{2,1,0:T(8,128)(2,1)S(1)} %collective-permute-done.4.refs_2_), channel_id=1, source_target_pairs={{0,4},{4,0},{1,5},{5,1},{2,6},{6,2},{3,7},{7,3},{8,12},{12,8},{9,1... | collective-permute-start | bytes 442376 | tf_op jit(solution)/shard_map/ppermute | solution.py:279
  23.2 8.0 %collective-permute-start.7 = (bf16[4,144,128]{2,1,0:T(8,128)(2,1)S(1)}, bf16[4,144,128]{2,1,0:T(8,128)(2,1)S(1)}, u32[]{:S(2)}, u32[]{:S(2)}) collective-permute-start(bf16[4,144,128]{2,1,0:T(8,128)(2,1)S(1)} %collective-permute-done.6.refs_4_), channel_id=1, source_target_pairs={{0,4},{4,0},{1,5},{5,1},{2,6},{6,2},{3,7},{7,3},{8,12},{12,8},{9,1... | collective-permute-start | bytes 442376 | tf_op jit(solution)/shard_map/ppermute | solution.py:279
  23.6 7.7 %collective-permute-start.12 = (bf16[4,144,128]{2,1,0:T(8,128)(2,1)S(1)}, bf16[4,144,128]{2,1,0:T(8,128)(2,1)S(1)}, u32[]{:S(2)}, u32[]{:S(2)}) collective-permute-start(bf16[4,144,128]{2,1,0:T(8,128)(2,1)S(1)} %collective-permute-done.10.refs_8_), channel_id=1, source_target_pairs={{0,8},{8,16},{16,24},{24,0},{1,9},{9,17},{17,25},{25,1},{2,10},{10... | collective-permute-start | bytes 442376 | tf_op jit(solution)/shard_map/ppermute | solution.py:279
  24.9 7.0 %collective-permute-start.14 = (bf16[4,144,128]{2,1,0:T(8,128)(2,1)S(1)}, bf16[4,144,128]{2,1,0:T(8,128)(2,1)S(1)}, u32[]{:S(2)}, u32[]{:S(2)}) collective-permute-start(bf16[4,144,128]{2,1,0:T(8,128)(2,1)S(1)} %collective-permute-done.10.refs_8_), channel_id=1, source_target_pairs={{0,24},{8,0},{16,8},{24,16},{1,25},{9,1},{17,9},{25,17},{2,26},{10... | collective-permute-start | bytes 442376 | tf_op jit(solution)/shard_map/ppermute | solution.py:279
  27.9 6.5 %collective-permute-start.16 = (bf16[4,144,128]{2,1,0:T(8,128)(2,1)S(1)}, bf16[4,144,128]{2,1,0:T(8,128)(2,1)S(1)}, u32[]{:S(2)}, u32[]{:S(2)}) collective-permute-start(bf16[4,144,128]{2,1,0:T(8,128)(2,1)S(1)} %collective-permute-done.10.refs_8_), channel_id=1, source_target_pairs={{0,16},{8,24},{16,0},{24,8},{1,17},{9,25},{17,1},{25,9},{2,18},{10... | collective-permute-start | bytes 442376 | tf_op jit(solution)/shard_map/ppermute | solution.py:279
  29.6 7.1 %collective-permute-start.11 = (bf16[4,144,128]{2,1,0:T(8,128)(2,1)S(1)}, bf16[4,144,128]{2,1,0:T(8,128)(2,1)S(1)}, u32[]{:S(2)}, u32[]{:S(2)}) collective-permute-start(bf16[4,144,128]{2,1,0:T(8,128)(2,1)S(1)} %collective-permute-done.10.refs_8_), channel_id=1, source_target_pairs={{0,4},{4,0},{1,5},{5,1},{2,6},{6,2},{3,7},{7,3},{8,12},{12,8},{9,1... | collective-permute-start | bytes 442376 | tf_op jit(solution)/shard_map/ppermute | solution.py:279
  51.0 29.3 %all-to-all-start.1 = ((bf16[64,2,2048]{2,1,0:T(2,128)(2,1)}), bf16[64,2,2048]{2,1,0:T(2,128)(2,1)S(1)}, u32[]{:S(2)}, u32[]{:S(2)}) async-start(bf16[64,2,2048]{2,1,0:T(2,128)(2,1)} %reshape.22), calls=%async_computation.1 | async-start | bytes 1048576 | tf_op jit(solution)/shard_map/all_to_all | solution.py:328
  62.6 26.5 %collective-permute-start.20 = (bf16[256,2048]{1,0:T(8,128)(2,1)}, bf16[256,2048]{1,0:T(8,128)(2,1)}, u32[]{:S(2)}, u32[]{:S(2)}) collective-permute-start(bf16[256,2048]{1,0:T(8,128)(2,1)} %bitcast.23.refs_2_), channel_id=1, source_target_pairs={{0,1},{1,2},{2,3},{3,0},{4,5},{5,6},{6,7},{7,4},{8,9},{9,10},{10,1... | collective-permute-start | bytes 3145736 | tf_op jit(solution)/shard_map/ppermute | solution.py:279
  63.0 26.1 %collective-permute-start.21 = (bf16[256,2048]{1,0:T(8,128)(2,1)}, bf16[256,2048]{1,0:T(8,128)(2,1)}, u32[]{:S(2)}, u32[]{:S(2)}) collective-permute-start(bf16[256,2048]{1,0:T(8,128)(2,1)} %bitcast.23.refs_2_), channel_id=1, source_target_pairs={{0,3},{1,0},{2,1},{3,2},{4,7},{5,4},{6,5},{7,6},{8,11},{9,8},{10,9... | collective-permute-start | bytes 3145736 | tf_op jit(solution)/shard_map/ppermute | solution.py:279
  65.4 54.0 %collective-permute-start.22 = (bf16[256,2048]{1,0:T(8,128)(2,1)}, bf16[256,2048]{1,0:T(8,128)(2,1)}, u32[]{:S(2)}, u32[]{:S(2)}) collective-permute-start(bf16[256,2048]{1,0:T(8,128)(2,1)} %bitcast.23.refs_2_), channel_id=1, source_target_pairs={{0,2},{1,3},{2,0},{3,1},{4,6},{5,7},{6,4},{7,5},{8,10},{9,11},{10,... | collective-permute-start | bytes 3145736 | tf_op jit(solution)/shard_map/ppermute | solution.py:279
  80.8 35.7 %collective-permute-start.18 = (bf16[64,2048]{1,0:T(8,128)(2,1)S(1)}, bf16[64,2048]{1,0:T(8,128)(2,1)S(1)}, u32[]{:S(2)}, u32[]{:S(2)}) collective-permute-start(bf16[64,2048]{1,0:T(8,128)(2,1)S(1)} %slice.13), channel_id=1, source_target_pairs={{0,1},{1,2},{2,3},{3,0},{4,5},{5,6},{6,7},{7,4},{8,9},{9,10},{10,1... | collective-permute-start | bytes 786440 | tf_op jit(solution)/shard_map/ppermute | solution.py:279
  81.2 35.2 %collective-permute-start.19 = (bf16[64,2048]{1,0:T(8,128)(2,1)S(1)}, bf16[64,2048]{1,0:T(8,128)(2,1)S(1)}, u32[]{:S(2)}, u32[]{:S(2)}) collective-permute-start(bf16[64,2048]{1,0:T(8,128)(2,1)S(1)} %slice.15), channel_id=1, source_target_pairs={{0,3},{1,0},{2,1},{3,2},{4,7},{5,4},{6,5},{7,6},{8,11},{9,8},{10,9... | collective-permute-start | bytes 786440 | tf_op jit(solution)/shard_map/ppermute | solution.py:279
  89.1 33.1 %collective-permute-start.23 = (bf16[64,2048]{1,0:T(8,128)(2,1)S(1)}, bf16[64,2048]{1,0:T(8,128)(2,1)S(1)}, u32[]{:S(2)}, u32[]{:S(2)}) collective-permute-start(bf16[64,2048]{1,0:T(8,128)(2,1)S(1)} %slice.15), channel_id=1, source_target_pairs={{0,1},{1,2},{2,3},{3,0},{4,5},{5,6},{6,7},{7,4},{8,9},{9,10},{10,1... | collective-permute-start | bytes 786440 | tf_op jit(solution)/shard_map/ppermute | solution.py:279
  89.1 33.2 %collective-permute-start.24 = (bf16[64,2048]{1,0:T(8,128)(2,1)S(1)}, bf16[64,2048]{1,0:T(8,128)(2,1)S(1)}, u32[]{:S(2)}, u32[]{:S(2)}) collective-permute-start(bf16[64,2048]{1,0:T(8,128)(2,1)S(1)} %slice.13), channel_id=1, source_target_pairs={{0,3},{1,0},{2,1},{3,2},{4,7},{5,4},{6,5},{7,6},{8,11},{9,8},{10,9... | collective-permute-start | bytes 786440 | tf_op jit(solution)/shard_map/ppermute | solution.py:279
  116.5 11.2 %collective-permute-start.27 = (bf16[64,2048]{1,0:T(8,128)(2,1)S(1)}, bf16[64,2048]{1,0:T(8,128)(2,1)S(1)}, u32[]{:S(2)}, u32[]{:S(2)}) collective-permute-start(bf16[64,2048]{1,0:T(8,128)(2,1)S(1)} %collective-permute-done.18.left0), channel_id=1, source_target_pairs={{0,1},{1,2},{2,3},{3,0},{4,5},{5,6},{6,7},{7,4},{8,9},{9,10},{10,1... | collective-permute-start | bytes 786440 | tf_op jit(solution)/shard_map/ppermute | solution.py:279
  116.5 11.2 %collective-permute-start.28 = (bf16[64,2048]{1,0:T(8,128)(2,1)S(1)}, bf16[64,2048]{1,0:T(8,128)(2,1)S(1)}, u32[]{:S(2)}, u32[]{:S(2)}) collective-permute-start(bf16[64,2048]{1,0:T(8,128)(2,1)S(1)} %collective-permute-done.19.right1), channel_id=1, source_target_pairs={{0,3},{1,0},{2,1},{3,2},{4,7},{5,4},{6,5},{7,6},{8,11},{9,8},{10,9... | collective-permute-start | bytes 786440 | tf_op jit(solution)/shard_map/ppermute | solution.py:279
  123.1 6.4 %collective-permute-start.25 = (bf16[128,256]{1,0:T(8,128)(2,1)S(1)}, bf16[128,256]{1,0:T(8,128)(2,1)S(1)}, u32[]{:S(2)}, u32[]{:S(2)}) collective-permute-start(bf16[128,256]{1,0:T(8,128)(2,1)S(1)} %get-tuple-element.31), channel_id=1, source_target_pairs={{0,1},{1,2},{2,3},{3,0},{4,5},{5,6},{6,7},{7,4},{8,9},{9,10},{10,1... | collective-permute-start | bytes 196616 | tf_op jit(solution)/shard_map/ppermute | solution.py:279
  123.2 6.3 %collective-permute-start.26 = (bf16[128,256]{1,0:T(8,128)(2,1)S(1)}, bf16[128,256]{1,0:T(8,128)(2,1)S(1)}, u32[]{:S(2)}, u32[]{:S(2)}) collective-permute-start(bf16[128,256]{1,0:T(8,128)(2,1)S(1)} %get-tuple-element.32), channel_id=1, source_target_pairs={{0,3},{1,0},{2,1},{3,2},{4,7},{5,4},{6,5},{7,6},{8,11},{9,8},{10,9... | collective-permute-start | bytes 196616 | tf_op jit(solution)/shard_map/ppermute | solution.py:279
  (12 other events, 218.3 us)

commit v3 on v2

--- a/solution.py
+++ b/solution.py
@@ -199,17 +199,18 @@
     normed = (total * lax.rsqrt(mean_square + 1e-06) * gain_ref[...]).astype(BF16)
     first, second = picks(routes_ref)
     pick = jnp.where(first | second, 1.0, 0.0).astype(BF16)
-    rows_ref[...] = dot(pick, normed).astype(BF16)
+    rows_ref[...] = dot(pick, normed).astype(BF16).reshape(rows_ref.shape)
 
 
 def hidden(rows, gate_ref, up_ref):
+    rows = rows.reshape(-1, D)
     gate = dot(rows, gate_ref[...])
     up = dot(rows, up_ref[...])
     return (gate / (1.0 + jnp.exp(-gate)) * up).astype(BF16)
 
 
 def near_kernel(own, left0, right1, *refs):
-    sources, outs, targets, sems = refs[:6], refs[6:9], refs[9:15], refs[15]
+    sources, outs, targets, sems = refs[:5], refs[5:8], refs[8:13], refs[13]
     copies = fetches(list(zip(sources, targets)), sems)
     for copy in copies:
         copy.start()
@@ -226,7 +227,7 @@
     wide = weights[0].shape[1]
     return pl.pallas_call(
         near_kernel,
-        out_shape=[jax.ShapeDtypeStruct((r.shape[0], wide), BF16) for r in rows]
+        out_shape=[jax.ShapeDtypeStruct((2 * r.shape[0], wide), BF16) for r in rows]
         + [jax.ShapeDtypeStruct(w.shape, w.dtype) for w in weights],
         in_specs=[vmem] * len(rows) + [pl.BlockSpec(memory_space=pltpu.HBM)] * len(weights),
         out_specs=[vmem] * (len(rows) + len(weights)),
@@ -253,13 +254,14 @@
     total = dot(own_ref[...], w_own[...])
     total = total + dot(left_ref[...], w_left[...])
     total = total + dot(right_ref[...], w_right[...])
-    out_ref[...] = (total + dot(far_ref[...], w_far[...])).astype(BF16)
+    total = total + dot(far_ref[...], w_far[...])
+    out_ref[...] = total.astype(BF16).reshape(out_ref.shape)
 
 
 def combine_kernel(stream_ref, routes_ref, weight_ref, back_ref, out_ref):
     first, second = picks(routes_ref)
     spread = jnp.where(first, weight_ref[0:1, :], 0.0) + jnp.where(second, weight_ref[1:2, :], 0.0)
-    back = back_ref[...]
+    back = back_ref[...].reshape(TOK, D)
     total = stream_ref[...]
     for part in parts3(spread):
         total = total + lax.dot_general(
@@ -318,22 +320,22 @@
     routes_row = routes.T
     stream, rows = call(
         project_kernel,
-        [((ROW, D), F32), ((TOK, D), BF16)],
+        [((ROW, D), F32), ((TOK // 2, 2, D), BF16)],
         heads,
         out_w,
         residual,
         norm_gain.reshape(1, D),
         routes_row,
     )
-    arrived = lax.all_to_all(rows.reshape(64, 2, D), SP, 0, 0, tiled=True).reshape(TOK, D)
-    half = TOK // 2
+    arrived = lax.all_to_all(rows, SP, 0, 0, tiled=True)
+    half = arrived.shape[0] // 2
     top, bottom = arrived[:half], arrived[half:]
     left0, right1 = moved(top, "tp", 1), moved(bottom, "tp", -1)
     left1, right0 = moved(bottom, "tp", 1), moved(top, "tp", -1)
     far0, far1 = moved(left0, "tp", 1), moved(right1, "tp", -1)
     h_own, h_left0, h_right1, gate_w, up_w, *down_w = near(
         (arrived, left0, right1),
-        (w_gate[0], w_up[0], down_own, down_left, down_right, down_far),
+        (w_gate[0], w_up[0], down_own, down_left, down_right),
     )
     shape = (h_own.shape, BF16)
     h_left, h_right = call(rest_kernel, [shape] * 2, gate_w, up_w, left1, right0, h_left0, h_right1)
@@ -341,14 +343,15 @@
     (h_far,) = call(far_kernel, [shape], gate_w, up_w, far0, far1)
     (expert_out,) = call(
         down_kernel,
-        [((TOK, D), BF16)],
+        [((TOK // 2, 2, D), BF16)],
         h_own,
         from_left,
         from_right,
         moved(h_far, "tp", 2),
         *down_w,
-    )
-    back = lax.all_to_all(expert_out.reshape(64, 2, D), SP, 0, 0, tiled=True).reshape(TOK, D)
+        down_far,
+    )
+    back = lax.all_to_all(expert_out, SP, 0, 0, tiled=True)
     (out,) = call(
         combine_kernel, [((ROW, D), BF16)], stream, routes_row, route_weight.T, back
     )

time: 166 us -> 165 us (level)
  local copies, waits for them, and re-layouts: 3.39 us -> 1.32 us
    reshape x4 -> x0, local copies, waits for them, and re-layouts: 1.87 us -> none  [the longest x1 1.13 us: shards(): rows.reshape(64, 2, D)]
  transfers between devices with their start and end apart: 31 -> 31, of which waited for: 7 -> 8; matrix products, arithmetic and copies ran while one was open for 1% -> 0% of each run, Pallas kernels for 3% -> 3%
where the time goes in v3:
time: 165 us
  starting transfers between devices  56.5 us (34%)
  waiting for transfers between devices  55.6 us (34%)
  blocking collectives  38.9 us (24%)
  Pallas kernels  12.5 us (8%)
    ppermute x29, starting transfers between devices, moved(): return lax.ppermute(x, axis, [(i, (i + by) % size) for i in range(size)])  44.2 us
    ppermute x29, waiting for transfers between devices, moved(): return lax.ppermute(x, axis, [(i, (i + by) % size) for i in range(size)])  40.7 us
    all_to_all x1, blocking collectives, shards(): back = lax.all_to_all(expert_out, SP, 0, 0, tiled=True)  30.6 us
    all_to_all x1, waiting for transfers between devices, shards(): arrived = lax.all_to_all(rows, SP, 0, 0, tiled=True)  14.9 us
    all_to_all x1, starting transfers between devices, shards(): arrived = lax.all_to_all(rows, SP, 0, 0, tiled=True)  11.6 us
    all_to_all x1, blocking collectives, shards(): lax.all_to_all(attended.reshape(NT, ROW, -1), 'tp', 0, 0, tiled=True)  8.29 us
    pallas_call x6, Pallas kernels, call(): pl.pallas_call(kernel, out_shape=[jax.ShapeDtypeStruct(s, t) for s, t in...  5.31 us
    pallas_call x1, Pallas kernels, attend(): pl.pallas_call(functools.partial(attend_kernel, len(chunks)), out_shape=[...  3.65 us
  transfers between devices with their start and end apart: 31, of which 8 were waited for; matrix products, arithmetic and copies ran while one was open for 0% of the time, Pallas kernels for 3%

profile of v3, /device:TPU:1, one launch (start us, length us, event | category | flops | bytes accessed | tf_op | source)
XLA Modules:
  0.0 165.0 jit_solution(7454319991160533978)
XLA Ops:
  0.8 6.9 %collective-permute-start.2 = (bf16[144,128]{1,0:T(8,128)(2,1)S(1)}, bf16[144,128]{1,0:T(8,128)(2,1)S(1)}, u32[]{:S(2)}, u32[]{:S(2)}) collective-permute-start(bf16[144,128]{1,0:T(8,128)(2,1)S(1)} %pack.1), channel_id=1, source_target_pairs={{0,192},{32,224},{64,0},{96,32},{128,64},{160,96},{192,128},{224,1... | collective-permute-start | bytes 110600 | tf_op jit(solution)/shard_map/ppermute | solution.py:281
  8.7 2.3 %collective-permute-start = (bf16[144,128]{1,0:T(8,128)(2,1)S(1)}, bf16[144,128]{1,0:T(8,128)(2,1)S(1)}, u32[]{:S(2)}, u32[]{:S(2)}) collective-permute-start(bf16[144,128]{1,0:T(8,128)(2,1)S(1)} %pack.1), channel_id=1, source_target_pairs={{0,64},{32,96},{64,128},{96,160},{128,192},{160,224},{192,0},{224,... | collective-permute-start | bytes 110600 | tf_op jit(solution)/shard_map/ppermute | solution.py:281
  11.0 3.5 %collective-permute-done.1 = bf16[144,128]{1,0:T(8,128)(2,1)S(1)} collective-permute-done((bf16[144,128]{1,0:T(8,128)(2,1)S(1)}, bf16[144,128]{1,0:T(8,128)(2,1)S(1)}, u32[]{:S(2)}, u32[]{:S(2)}) %collective-permute-start.1) | collective-permute-done | bytes 36896 | tf_op jit(solution)/shard_map/ppermute | solution.py:281
  18.1 2.8 %collective-permute-start.3 = (bf16[4,144,128]{2,1,0:T(8,128)(2,1)S(1)}, bf16[4,144,128]{2,1,0:T(8,128)(2,1)S(1)}, u32[]{:S(2)}, u32[]{:S(2)}) collective-permute-start(bf16[4,144,128]{2,1,0:T(8,128)(2,1)S(1)} %pad_maximum_fusion.refs_0_), channel_id=1, source_target_pairs={{0,4},{4,0},{1,5},{5,1},{2,6},{6,2},{3,7},{7,3},{8,12},{12,8},{9,1... | collective-permute-start | bytes 442376 | tf_op jit(solution)/shard_map/ppermute | solution.py:281
  21.0 1.7 %collective-permute-start.8 = (bf16[4,144,128]{2,1,0:T(8,128)(2,1)S(1)}, bf16[4,144,128]{2,1,0:T(8,128)(2,1)S(1)}, u32[]{:S(2)}, u32[]{:S(2)}) collective-permute-start(bf16[4,144,128]{2,1,0:T(8,128)(2,1)S(1)} %pad_maximum_fusion.refs_0_), channel_id=1, source_target_pairs={{0,16},{8,24},{16,0},{24,8},{1,17},{9,25},{17,1},{25,9},{2,18},{10... | collective-permute-start | bytes 442376 | tf_op jit(solution)/shard_map/ppermute | solution.py:281
  26.3 1.6 collective-permute-done.8.refs_6_
  27.9 1.7 %collective-permute-start.16 = (bf16[4,144,128]{2,1,0:T(8,128)(2,1)S(1)}, bf16[4,144,128]{2,1,0:T(8,128)(2,1)S(1)}, u32[]{:S(2)}, u32[]{:S(2)}) collective-permute-start(bf16[4,144,128]{2,1,0:T(8,128)(2,1)S(1)} %collective-permute-done.10.refs_8_), channel_id=1, source_target_pairs={{0,16},{8,24},{16,0},{24,8},{1,17},{9,25},{17,1},{25,9},{2,18},{10... | collective-permute-start | bytes 442376 | tf_op jit(solution)/shard_map/ppermute | solution.py:281
  31.9 2.4 %collective-permute-start.15 = (bf16[4,144,128]{2,1,0:T(8,128)(2,1)S(1)}, bf16[4,144,128]{2,1,0:T(8,128)(2,1)S(1)}, u32[]{:S(2)}, u32[]{:S(2)}) collective-permute-start(bf16[4,144,128]{2,1,0:T(8,128)(2,1)S(1)} %collective-permute-done.14.refs_12_), channel_id=1, source_target_pairs={{0,4},{4,0},{1,5},{5,1},{2,6},{6,2},{3,7},{7,3},{8,12},{12,8},{9,1... | collective-permute-start | bytes 442376 | tf_op jit(solution)/shard_map/ppermute | solution.py:281
  36.8 3.6 %attend.1 = (bf16[128,256]{1,0:T(8,128)(2,1)S(1)}, bf16[1024,2048]{1,0:T(8,128)(2,1)S(1)}) custom-call(s32[17]{0:T(128)S(1)} %stack.65.place_ref, bf16[512,80]{1,0:T(8,128)(2,1)S(1)} %shard_map.118.query_ref, bf16[1024,2048]{1,0:T(8,128)(2,1)} %source_ref.1, bf16[4,144,128]{2,1,0:T(8,128)(2,1)S(1)} %pad_maximum_fusion.refs_0_, ...), custom_call_target="tpu_custom_call" | custom-call | tf_op jit(solution)/shard_map/attend/pallas_call | solution.py:159
  40.4 8.3 %all_to_all.15.att_ref = bf16[4,32,256]{2,1,0:T(8,128)(2,1)S(1)} all-to-all(bf16[4,32,256]{2,1,0:T(8,128)(2,1)S(1)} %bitcast.25), channel_id=1, replica_groups=mesh['z'=8,'y'=4,'c'=2,'tp'=4] {'tp'}, dimensions={0} | all-to-all | bytes 131072 | tf_op jit(solution)/shard_map/all_to_all | solution.py:317
  48.7 2.0 %shard_map.119 = (f32[32,2048]{1,0:T(8,128)S(1)}, bf16[64,2,2048]{2,1,0:T(2,128)(2,1)}) custom-call(bf16[4,32,256]{2,1,0:T(8,128)(2,1)S(1)} %all_to_all.15.att_ref, bf16[1024,2048]{1,0:T(8,128)(2,1)S(1)} %get-tuple-element.21.weight_ref, bf16[32,2048]{1,0:T(8,128)(2,1)S(1)} %copy-done, f32[1,2048]{1,0:T(1,128)S(1)} %bitcast.26, s32[2,32]{1,0:T(2,128)S(1)} %bitcast.27), custom_call_target="tpu_custom_call" | custom-call | tf_op jit(solution)/shard_map/pallas_call | solution.py:274
  50.7 11.6 %all-to-all-start.1 = ((bf16[64,2,2048]{2,1,0:T(2,128)(2,1)}), bf16[64,2,2048]{2,1,0:T(2,128)(2,1)S(1)}, u32[]{:S(2)}, u32[]{:S(2)}) async-start(bf16[64,2,2048]{2,1,0:T(2,128)(2,1)} %get-tuple-element.23), calls=%async_computation.1 | async-start | bytes 1048576 | tf_op jit(solution)/shard_map/all_to_all | solution.py:330
  62.6 2.4 %collective-permute-start.21 = (bf16[256,2048]{1,0:T(8,128)(2,1)}, bf16[256,2048]{1,0:T(8,128)(2,1)}, u32[]{:S(2)}, u32[]{:S(2)}) collective-permute-start(bf16[256,2048]{1,0:T(8,128)(2,1)} %bitcast.23.refs_2_), channel_id=1, source_target_pairs={{0,3},{1,0},{2,1},{3,2},{4,7},{5,4},{6,5},{7,6},{8,11},{9,8},{10,9... | collective-permute-start | bytes 3145736 | tf_op jit(solution)/shard_map/ppermute | solution.py:281
  65.0 14.9 %all-to-all-done.1.own = bf16[64,2,2048]{2,1,0:T(2,128)(2,1)S(1)} async-done(((bf16[64,2,2048]{2,1,0:T(2,128)(2,1)}), bf16[64,2,2048]{2,1,0:T(2,128)(2,1)S(1)}, u32[]{:S(2)}, u32[]{:S(2)}) %all-to-all-start.1) | async-done | bytes 524320 | tf_op jit(solution)/shard_map/all_to_all | solution.py:330
  80.7 2.4 %collective-permute-start.19 = (bf16[32,2,2048]{2,1,0:T(2,128)(2,1)S(1)}, bf16[32,2,2048]{2,1,0:T(2,128)(2,1)S(1)}, u32[]{:S(2)}, u32[]{:S(2)}) collective-permute-start(bf16[32,2,2048]{2,1,0:T(2,128)(2,1)S(1)} %get-tuple-element.35), channel_id=1, source_target_pairs={{0,3},{1,0},{2,1},{3,2},{4,7},{5,4},{6,5},{7,6},{8,11},{9,8},{10,9... | collective-permute-start | bytes 786440 | tf_op jit(solution)/shard_map/ppermute | solution.py:281
  83.1 5.7 %collective-permute-done.20.refs_3_ = bf16[256,2048]{1,0:T(8,128)(2,1)} collective-permute-done((bf16[256,2048]{1,0:T(8,128)(2,1)}, bf16[256,2048]{1,0:T(8,128)(2,1)}, u32[]{:S(2)}, u32[]{:S(2)}) %collective-permute-start.20) | collective-permute-done | bytes 1048608 | tf_op jit(solution)/shard_map/ppermute | solution.py:281
  88.8 3.0 %collective-permute-start.23 = (bf16[32,2,2048]{2,1,0:T(2,128)(2,1)S(1)}, bf16[32,2,2048]{2,1,0:T(2,128)(2,1)S(1)}, u32[]{:S(2)}, u32[]{:S(2)}) collective-permute-start(bf16[32,2,2048]{2,1,0:T(2,128)(2,1)S(1)} %get-tuple-element.36), channel_id=1, source_target_pairs={{0,3},{1,0},{2,1},{3,2},{4,7},{5,4},{6,5},{7,6},{8,11},{9,8},{10,9... | collective-permute-start | bytes 786440 | tf_op jit(solution)/shard_map/ppermute | solution.py:281
  91.8 24.4 %collective-permute-done.18.left0 = bf16[32,2,2048]{2,1,0:T(2,128)(2,1)S(1)} collective-permute-done((bf16[32,2,2048]{2,1,0:T(2,128)(2,1)S(1)}, bf16[32,2,2048]{2,1,0:T(2,128)(2,1)S(1)}, u32[]{:S(2)}, u32[]{:S(2)}) %collective-permute-start.18) | collective-permute-done | bytes 262176 | tf_op jit(solution)/shard_map/ppermute | solution.py:281
  116.1 2.7 %collective-permute-start.27 = (bf16[32,2,2048]{2,1,0:T(2,128)(2,1)S(1)}, bf16[32,2,2048]{2,1,0:T(2,128)(2,1)S(1)}, u32[]{:S(2)}, u32[]{:S(2)}) collective-permute-start(bf16[32,2,2048]{2,1,0:T(2,128)(2,1)S(1)} %collective-permute-done.19.right1), channel_id=1, source_target_pairs={{0,3},{1,0},{2,1},{3,2},{4,7},{5,4},{6,5},{7,6},{8,11},{9,8},{10,9... | collective-permute-start | bytes 786440 | tf_op jit(solution)/shard_map/ppermute | solution.py:281
  118.8 2.7 %near.1 = (bf16[128,256]{1,0:T(8,128)(2,1)S(1)}, bf16[64,256]{1,0:T(8,128)(2,1)S(1)}, bf16[64,256]{1,0:T(8,128)(2,1)S(1)}, bf16[2048,256]{1,0:T(8,128)(2,1)S(1)}...) custom-call(bf16[64,2,2048]{2,1,0:T(2,128)(2,1)S(1)} %all-to-all-don, ...), custom_call_target="tpu_custom_call" | custom-call | tf_op jit(solution)/shard_map/near/pallas_call | solution.py:228
  122.7 2.7 %collective-permute-start.25 = (bf16[128,256]{1,0:T(8,128)(2,1)S(1)}, bf16[128,256]{1,0:T(8,128)(2,1)S(1)}, u32[]{:S(2)}, u32[]{:S(2)}) collective-permute-start(bf16[128,256]{1,0:T(8,128)(2,1)S(1)} %get-tuple-element.30), channel_id=1, source_target_pairs={{0,3},{1,0},{2,1},{3,2},{4,7},{5,4},{6,5},{7,6},{8,11},{9,8},{10,9... | collective-permute-start | bytes 196616 | tf_op jit(solution)/shard_map/ppermute | solution.py:281
  125.4 2.0 %collective-permute-done.26.far0 = bf16[32,2,2048]{2,1,0:T(2,128)(2,1)S(1)} collective-permute-done((bf16[32,2,2048]{2,1,0:T(2,128)(2,1)S(1)}, bf16[32,2,2048]{2,1,0:T(2,128)(2,1)S(1)}, u32[]{:S(2)}, u32[]{:S(2)}) %collective-permute-start.26) | collective-permute-done | bytes 262176 | tf_op jit(solution)/shard_map/ppermute | solution.py:281
  129.2 3.4 %collective-permute-done.28.far_ref = bf16[128,256]{1,0:T(8,128)(2,1)S(1)} collective-permute-done((bf16[128,256]{1,0:T(8,128)(2,1)S(1)}, bf16[128,256]{1,0:T(8,128)(2,1)S(1)}, u32[]{:S(2)}, u32[]{:S(2)}) %collective-permute-start.28) | collective-permute-done | bytes 65568 | tf_op jit(solution)/shard_map/ppermute | solution.py:281
  133.3 30.6 %all_to_all.16.back_ref = bf16[64,2,2048]{2,1,0:T(2,128)(2,1)S(1)} all-to-all(bf16[64,2,2048]{2,1,0:T(2,128)(2,1)S(1)} %shard_map.122), channel_id=1, replica_groups=mesh['z'=8,'y'=4,'c'=2,'tp'=4] {'z','y','c'}, dimensions={0} | all-to-all | bytes 1048576 | tf_op jit(solution)/shard_map/all_to_all | solution.py:354
  (62 shorter events, 19.7 us)
Async XLA Ops:
  0.8 10.2 %collective-permute-start.2 = (bf16[144,128]{1,0:T(8,128)(2,1)S(1)}, bf16[144,128]{1,0:T(8,128)(2,1)S(1)}, u32[]{:S(2)}, u32[]{:S(2)}) collective-permute-start(bf16[144,128]{1,0:T(8,128)(2,1)S(1)} %pack.1), channel_id=1, source_target_pairs={{0,192},{32,224},{64,0},{96,32},{128,64},{160,96},{192,128},{224,1... | collective-permute-start | bytes 110600 | tf_op jit(solution)/shard_map/ppermute | solution.py:281
  7.8 6.7 %collective-permute-start.1 = (bf16[144,128]{1,0:T(8,128)(2,1)S(1)}, bf16[144,128]{1,0:T(8,128)(2,1)S(1)}, u32[]{:S(2)}, u32[]{:S(2)}) collective-permute-start(bf16[144,128]{1,0:T(8,128)(2,1)S(1)} %pack.1), channel_id=1, source_target_pairs={{0,128},{32,160},{64,192},{96,224},{128,0},{160,32},{192,64},{224,... | collective-permute-start | bytes 110600 | tf_op jit(solution)/shard_map/ppermute | solution.py:281
  14.5 8.2 %collective-permute-start.4 = (bf16[4,144,128]{2,1,0:T(8,128)(2,1)S(1)}, bf16[4,144,128]{2,1,0:T(8,128)(2,1)S(1)}, u32[]{:S(2)}, u32[]{:S(2)}) collective-permute-start(bf16[4,144,128]{2,1,0:T(8,128)(2,1)S(1)} %pad_maximum_fusion.refs_0_), channel_id=1, source_target_pairs={{0,8},{8,16},{16,24},{24,0},{1,9},{9,17},{17,25},{25,1},{2,10},{10... | collective-permute-start | bytes 442376 | tf_op jit(solution)/shard_map/ppermute | solution.py:281
  15.9 7.3 %collective-permute-start.6 = (bf16[4,144,128]{2,1,0:T(8,128)(2,1)S(1)}, bf16[4,144,128]{2,1,0:T(8,128)(2,1)S(1)}, u32[]{:S(2)}, u32[]{:S(2)}) collective-permute-start(bf16[4,144,128]{2,1,0:T(8,128)(2,1)S(1)} %pad_maximum_fusion.refs_0_), channel_id=1, source_target_pairs={{0,24},{8,0},{16,8},{24,16},{1,25},{9,1},{17,9},{25,17},{2,26},{10... | collective-permute-start | bytes 442376 | tf_op jit(solution)/shard_map/ppermute | solution.py:281
  18.1 6.7 %collective-permute-start.3 = (bf16[4,144,128]{2,1,0:T(8,128)(2,1)S(1)}, bf16[4,144,128]{2,1,0:T(8,128)(2,1)S(1)}, u32[]{:S(2)}, u32[]{:S(2)}) collective-permute-start(bf16[4,144,128]{2,1,0:T(8,128)(2,1)S(1)} %pad_maximum_fusion.refs_0_), channel_id=1, source_target_pairs={{0,4},{4,0},{1,5},{5,1},{2,6},{6,2},{3,7},{7,3},{8,12},{12,8},{9,1... | collective-permute-start | bytes 442376 | tf_op jit(solution)/shard_map/ppermute | solution.py:281
  21.0 6.9 %collective-permute-start.8 = (bf16[4,144,128]{2,1,0:T(8,128)(2,1)S(1)}, bf16[4,144,128]{2,1,0:T(8,128)(2,1)S(1)}, u32[]{:S(2)}, u32[]{:S(2)}) collective-permute-start(bf16[4,144,128]{2,1,0:T(8,128)(2,1)S(1)} %pad_maximum_fusion.refs_0_), channel_id=1, source_target_pairs={{0,16},{8,24},{16,0},{24,8},{1,17},{9,25},{17,1},{25,9},{2,18},{10... | collective-permute-start | bytes 442376 | tf_op jit(solution)/shard_map/ppermute | solution.py:281
  22.7 6.9 %collective-permute-start.5 = (bf16[4,144,128]{2,1,0:T(8,128)(2,1)S(1)}, bf16[4,144,128]{2,1,0:T(8,128)(2,1)S(1)}, u32[]{:S(2)}, u32[]{:S(2)}) collective-permute-start(bf16[4,144,128]{2,1,0:T(8,128)(2,1)S(1)} %collective-permute-done.4.refs_2_), channel_id=1, source_target_pairs={{0,4},{4,0},{1,5},{5,1},{2,6},{6,2},{3,7},{7,3},{8,12},{12,8},{9,1... | collective-permute-start | bytes 442376 | tf_op jit(solution)/shard_map/ppermute | solution.py:281
  23.2 8.0 %collective-permute-start.7 = (bf16[4,144,128]{2,1,0:T(8,128)(2,1)S(1)}, bf16[4,144,128]{2,1,0:T(8,128)(2,1)S(1)}, u32[]{:S(2)}, u32[]{:S(2)}) collective-permute-start(bf16[4,144,128]{2,1,0:T(8,128)(2,1)S(1)} %collective-permute-done.6.refs_4_), channel_id=1, source_target_pairs={{0,4},{4,0},{1,5},{5,1},{2,6},{6,2},{3,7},{7,3},{8,12},{12,8},{9,1... | collective-permute-start | bytes 442376 | tf_op jit(solution)/shard_map/ppermute | solution.py:281
  23.6 7.7 %collective-permute-start.12 = (bf16[4,144,128]{2,1,0:T(8,128)(2,1)S(1)}, bf16[4,144,128]{2,1,0:T(8,128)(2,1)S(1)}, u32[]{:S(2)}, u32[]{:S(2)}) collective-permute-start(bf16[4,144,128]{2,1,0:T(8,128)(2,1)S(1)} %collective-permute-done.10.refs_8_), channel_id=1, source_target_pairs={{0,8},{8,16},{16,24},{24,0},{1,9},{9,17},{17,25},{25,1},{2,10},{10... | collective-permute-start | bytes 442376 | tf_op jit(solution)/shard_map/ppermute | solution.py:281
  24.9 7.0 %collective-permute-start.14 = (bf16[4,144,128]{2,1,0:T(8,128)(2,1)S(1)}, bf16[4,144,128]{2,1,0:T(8,128)(2,1)S(1)}, u32[]{:S(2)}, u32[]{:S(2)}) collective-permute-start(bf16[4,144,128]{2,1,0:T(8,128)(2,1)S(1)} %collective-permute-done.10.refs_8_), channel_id=1, source_target_pairs={{0,24},{8,0},{16,8},{24,16},{1,25},{9,1},{17,9},{25,17},{2,26},{10... | collective-permute-start | bytes 442376 | tf_op jit(solution)/shard_map/ppermute | solution.py:281
  27.9 6.5 %collective-permute-start.16 = (bf16[4,144,128]{2,1,0:T(8,128)(2,1)S(1)}, bf16[4,144,128]{2,1,0:T(8,128)(2,1)S(1)}, u32[]{:S(2)}, u32[]{:S(2)}) collective-permute-start(bf16[4,144,128]{2,1,0:T(8,128)(2,1)S(1)} %collective-permute-done.10.refs_8_), channel_id=1, source_target_pairs={{0,16},{8,24},{16,0},{24,8},{1,17},{9,25},{17,1},{25,9},{2,18},{10... | collective-permute-start | bytes 442376 | tf_op jit(solution)/shard_map/ppermute | solution.py:281
  29.6 7.1 %collective-permute-start.11 = (bf16[4,144,128]{2,1,0:T(8,128)(2,1)S(1)}, bf16[4,144,128]{2,1,0:T(8,128)(2,1)S(1)}, u32[]{:S(2)}, u32[]{:S(2)}) collective-permute-start(bf16[4,144,128]{2,1,0:T(8,128)(2,1)S(1)} %collective-permute-done.10.refs_8_), channel_id=1, source_target_pairs={{0,4},{4,0},{1,5},{5,1},{2,6},{6,2},{3,7},{7,3},{8,12},{12,8},{9,1... | collective-permute-start | bytes 442376 | tf_op jit(solution)/shard_map/ppermute | solution.py:281
  50.7 29.3 %all-to-all-start.1 = ((bf16[64,2,2048]{2,1,0:T(2,128)(2,1)}), bf16[64,2,2048]{2,1,0:T(2,128)(2,1)S(1)}, u32[]{:S(2)}, u32[]{:S(2)}) async-start(bf16[64,2,2048]{2,1,0:T(2,128)(2,1)} %get-tuple-element.23), calls=%async_computation.1 | async-start | bytes 1048576 | tf_op jit(solution)/shard_map/all_to_all | solution.py:330
  62.3 26.5 %collective-permute-start.20 = (bf16[256,2048]{1,0:T(8,128)(2,1)}, bf16[256,2048]{1,0:T(8,128)(2,1)}, u32[]{:S(2)}, u32[]{:S(2)}) collective-permute-start(bf16[256,2048]{1,0:T(8,128)(2,1)} %bitcast.23.refs_2_), channel_id=1, source_target_pairs={{0,1},{1,2},{2,3},{3,0},{4,5},{5,6},{6,7},{7,4},{8,9},{9,10},{10,1... | collective-permute-start | bytes 3145736 | tf_op jit(solution)/shard_map/ppermute | solution.py:281
  62.6 26.1 %collective-permute-start.21 = (bf16[256,2048]{1,0:T(8,128)(2,1)}, bf16[256,2048]{1,0:T(8,128)(2,1)}, u32[]{:S(2)}, u32[]{:S(2)}) collective-permute-start(bf16[256,2048]{1,0:T(8,128)(2,1)} %bitcast.23.refs_2_), channel_id=1, source_target_pairs={{0,3},{1,0},{2,1},{3,2},{4,7},{5,4},{6,5},{7,6},{8,11},{9,8},{10,9... | collective-permute-start | bytes 3145736 | tf_op jit(solution)/shard_map/ppermute | solution.py:281
  65.0 64.2 %collective-permute-start.29 = (bf16[256,2048]{1,0:T(8,128)(2,1)}, bf16[256,2048]{1,0:T(8,128)(2,1)S(1)}, u32[]{:S(2)}, u32[]{:S(2)}) collective-permute-start(bf16[256,2048]{1,0:T(8,128)(2,1)} %bitcast.23.refs_2_), channel_id=1, source_target_pairs={{0,2},{1,3},{2,0},{3,1},{4,6},{5,7},{6,4},{7,5},{8,10},{9,11},{10,... | collective-permute-start | bytes 3145736 | tf_op jit(solution)/shard_map/ppermute | solution.py:281
  80.3 35.8 %collective-permute-start.18 = (bf16[32,2,2048]{2,1,0:T(2,128)(2,1)S(1)}, bf16[32,2,2048]{2,1,0:T(2,128)(2,1)S(1)}, u32[]{:S(2)}, u32[]{:S(2)}) collective-permute-start(bf16[32,2,2048]{2,1,0:T(2,128)(2,1)S(1)} %get-tuple-element.36), channel_id=1, source_target_pairs={{0,1},{1,2},{2,3},{3,0},{4,5},{5,6},{6,7},{7,4},{8,9},{9,10},{10,1... | collective-permute-start | bytes 786440 | tf_op jit(solution)/shard_map/ppermute | solution.py:281
  80.7 35.4 %collective-permute-start.19 = (bf16[32,2,2048]{2,1,0:T(2,128)(2,1)S(1)}, bf16[32,2,2048]{2,1,0:T(2,128)(2,1)S(1)}, u32[]{:S(2)}, u32[]{:S(2)}) collective-permute-start(bf16[32,2,2048]{2,1,0:T(2,128)(2,1)S(1)} %get-tuple-element.35), channel_id=1, source_target_pairs={{0,3},{1,0},{2,1},{3,2},{4,7},{5,4},{6,5},{7,6},{8,11},{9,8},{10,9... | collective-permute-start | bytes 786440 | tf_op jit(solution)/shard_map/ppermute | solution.py:281
  88.8 33.0 %collective-permute-start.22 = (bf16[32,2,2048]{2,1,0:T(2,128)(2,1)S(1)}, bf16[32,2,2048]{2,1,0:T(2,128)(2,1)S(1)}, u32[]{:S(2)}, u32[]{:S(2)}) collective-permute-start(bf16[32,2,2048]{2,1,0:T(2,128)(2,1)S(1)} %get-tuple-element.35), channel_id=1, source_target_pairs={{0,1},{1,2},{2,3},{3,0},{4,5},{5,6},{6,7},{7,4},{8,9},{9,10},{10,1... | collective-permute-start | bytes 786440 | tf_op jit(solution)/shard_map/ppermute | solution.py:281
  88.8 33.0 %collective-permute-start.23 = (bf16[32,2,2048]{2,1,0:T(2,128)(2,1)S(1)}, bf16[32,2,2048]{2,1,0:T(2,128)(2,1)S(1)}, u32[]{:S(2)}, u32[]{:S(2)}) collective-permute-start(bf16[32,2,2048]{2,1,0:T(2,128)(2,1)S(1)} %get-tuple-element.36), channel_id=1, source_target_pairs={{0,3},{1,0},{2,1},{3,2},{4,7},{5,4},{6,5},{7,6},{8,11},{9,8},{10,9... | collective-permute-start | bytes 786440 | tf_op jit(solution)/shard_map/ppermute | solution.py:281
  116.1 11.2 %collective-permute-start.26 = (bf16[32,2,2048]{2,1,0:T(2,128)(2,1)S(1)}, bf16[32,2,2048]{2,1,0:T(2,128)(2,1)S(1)}, u32[]{:S(2)}, u32[]{:S(2)}) collective-permute-start(bf16[32,2,2048]{2,1,0:T(2,128)(2,1)S(1)} %collective-permute-done.18.left0), channel_id=1, source_target_pairs={{0,1},{1,2},{2,3},{3,0},{4,5},{5,6},{6,7},{7,4},{8,9},{9,10},{10,1... | collective-permute-start | bytes 786440 | tf_op jit(solution)/shard_map/ppermute | solution.py:281
  116.1 11.2 %collective-permute-start.27 = (bf16[32,2,2048]{2,1,0:T(2,128)(2,1)S(1)}, bf16[32,2,2048]{2,1,0:T(2,128)(2,1)S(1)}, u32[]{:S(2)}, u32[]{:S(2)}) collective-permute-start(bf16[32,2,2048]{2,1,0:T(2,128)(2,1)S(1)} %collective-permute-done.19.right1), channel_id=1, source_target_pairs={{0,3},{1,0},{2,1},{3,2},{4,7},{5,4},{6,5},{7,6},{8,11},{9,8},{10,9... | collective-permute-start | bytes 786440 | tf_op jit(solution)/shard_map/ppermute | solution.py:281
  122.6 6.6 %collective-permute-start.24 = (bf16[128,256]{1,0:T(8,128)(2,1)S(1)}, bf16[128,256]{1,0:T(8,128)(2,1)S(1)}, u32[]{:S(2)}, u32[]{:S(2)}) collective-permute-start(bf16[128,256]{1,0:T(8,128)(2,1)S(1)} %get-tuple-element.29), channel_id=1, source_target_pairs={{0,1},{1,2},{2,3},{3,0},{4,5},{5,6},{6,7},{7,4},{8,9},{9,10},{10,1... | collective-permute-start | bytes 196616 | tf_op jit(solution)/shard_map/ppermute | solution.py:281
  122.7 6.5 %collective-permute-start.25 = (bf16[128,256]{1,0:T(8,128)(2,1)S(1)}, bf16[128,256]{1,0:T(8,128)(2,1)S(1)}, u32[]{:S(2)}, u32[]{:S(2)}) collective-permute-start(bf16[128,256]{1,0:T(8,128)(2,1)S(1)} %get-tuple-element.30), channel_id=1, source_target_pairs={{0,3},{1,0},{2,1},{3,2},{4,7},{5,4},{6,5},{7,6},{8,11},{9,8},{10,9... | collective-permute-start | bytes 196616 | tf_op jit(solution)/shard_map/ppermute | solution.py:281
  (12 other events, 222.9 us)

commit v4 on v3

--- a/solution.py
+++ b/solution.py
@@ -250,11 +250,14 @@
     h_far[...] = hidden(rows, gate_ref, up_ref)
 
 
-def down_kernel(own_ref, left_ref, right_ref, far_ref, w_own, w_left, w_right, w_far, out_ref):
+def part_kernel(own_ref, left_ref, right_ref, w_own, w_left, w_right, out_ref):
     total = dot(own_ref[...], w_own[...])
     total = total + dot(left_ref[...], w_left[...])
-    total = total + dot(right_ref[...], w_right[...])
-    total = total + dot(far_ref[...], w_far[...])
+    out_ref[...] = total + dot(right_ref[...], w_right[...])
+
+
+def down_kernel(part_ref, far_ref, w_far, out_ref):
+    total = part_ref[...] + dot(far_ref[...], w_far[...])
     out_ref[...] = total.astype(BF16).reshape(out_ref.shape)
 
 
@@ -341,15 +344,12 @@
     h_left, h_right = call(rest_kernel, [shape] * 2, gate_w, up_w, left1, right0, h_left0, h_right1)
     from_left, from_right = moved(h_right, "tp", 1), moved(h_left, "tp", -1)
     (h_far,) = call(far_kernel, [shape], gate_w, up_w, far0, far1)
+    from_far = moved(h_far, "tp", 2)
+    (part,) = call(
+        part_kernel, [((TOK, D), F32)], h_own, from_left, from_right, *down_w
+    )
     (expert_out,) = call(
-        down_kernel,
-        [((TOK // 2, 2, D), BF16)],
-        h_own,
-        from_left,
-        from_right,
-        moved(h_far, "tp", 2),
-        *down_w,
-        down_far,
+        down_kernel, [((TOK // 2, 2, D), BF16)], in_vmem(part), from_far, down_far
     )
     back = lax.all_to_all(expert_out, SP, 0, 0, tiled=True)
     (out,) = call(

time: 165 us -> 165 us (level)
    pallas_call x6 -> x7, Pallas kernels: 5.31 us -> 5.49 us  [call(): pl.pallas_call(kernel, out_shape=[jax.ShapeDtypeStruct(s, t) for s, t in...]
where the time goes in v4:
time: 165 us
  starting transfers between devices  56.5 us (34%)
  waiting for transfers between devices  55.1 us (33%)
  blocking collectives  38.8 us (24%)
  Pallas kernels  12.7 us (8%)
    ppermute x29, starting transfers between devices, moved(): return lax.ppermute(x, axis, [(i, (i + by) % size) for i in range(size)])  44.2 us
    ppermute x29, waiting for transfers between devices, moved(): return lax.ppermute(x, axis, [(i, (i + by) % size) for i in range(size)])  40.1 us
    all_to_all x1, blocking collectives, shards(): back = lax.all_to_all(expert_out, SP, 0, 0, tiled=True)  30.6 us
    all_to_all x1, waiting for transfers between devices, shards(): arrived = lax.all_to_all(rows, SP, 0, 0, tiled=True)  14.9 us
    all_to_all x1, starting transfers between devices, shards(): arrived = lax.all_to_all(rows, SP, 0, 0, tiled=True)  11.6 us
    all_to_all x1, blocking collectives, shards(): lax.all_to_all(attended.reshape(NT, ROW, -1), 'tp', 0, 0, tiled=True)  8.29 us
    pallas_call x7, Pallas kernels, call(): pl.pallas_call(kernel, out_shape=[jax.ShapeDtypeStruct(s, t) for s, t in...  5.49 us
    pallas_call x1, Pallas kernels, attend(): pl.pallas_call(functools.partial(attend_kernel, len(chunks)), out_shape=[...  3.65 us
  transfers between devices with their start and end apart: 31, of which 8 were waited for; matrix products, arithmetic and copies ran while one was open for 0% of the time, Pallas kernels for 3%

profile of v4, /device:TPU:1, one launch (start us, length us, event | category | flops | bytes accessed | tf_op | source)
XLA Modules:
  0.0 164.6 jit_solution(1252526282955256652)
XLA Ops:
  0.8 6.9 %collective-permute-start.2 = (bf16[144,128]{1,0:T(8,128)(2,1)S(1)}, bf16[144,128]{1,0:T(8,128)(2,1)S(1)}, u32[]{:S(2)}, u32[]{:S(2)}) collective-permute-start(bf16[144,128]{1,0:T(8,128)(2,1)S(1)} %pack.1), channel_id=1, source_target_pairs={{0,192},{32,224},{64,0},{96,32},{128,64},{160,96},{192,128},{224,1... | collective-permute-start | bytes 110600 | tf_op jit(solution)/shard_map/ppermute | solution.py:284
  8.7 2.3 %collective-permute-start = (bf16[144,128]{1,0:T(8,128)(2,1)S(1)}, bf16[144,128]{1,0:T(8,128)(2,1)S(1)}, u32[]{:S(2)}, u32[]{:S(2)}) collective-permute-start(bf16[144,128]{1,0:T(8,128)(2,1)S(1)} %pack.1), channel_id=1, source_target_pairs={{0,64},{32,96},{64,128},{96,160},{128,192},{160,224},{192,0},{224,... | collective-permute-start | bytes 110600 | tf_op jit(solution)/shard_map/ppermute | solution.py:284
  11.0 3.5 %collective-permute-done.1 = bf16[144,128]{1,0:T(8,128)(2,1)S(1)} collective-permute-done((bf16[144,128]{1,0:T(8,128)(2,1)S(1)}, bf16[144,128]{1,0:T(8,128)(2,1)S(1)}, u32[]{:S(2)}, u32[]{:S(2)}) %collective-permute-start.1) | collective-permute-done | bytes 36896 | tf_op jit(solution)/shard_map/ppermute | solution.py:284
  18.1 2.8 %collective-permute-start.3 = (bf16[4,144,128]{2,1,0:T(8,128)(2,1)S(1)}, bf16[4,144,128]{2,1,0:T(8,128)(2,1)S(1)}, u32[]{:S(2)}, u32[]{:S(2)}) collective-permute-start(bf16[4,144,128]{2,1,0:T(8,128)(2,1)S(1)} %pad_maximum_fusion.refs_0_), channel_id=1, source_target_pairs={{0,4},{4,0},{1,5},{5,1},{2,6},{6,2},{3,7},{7,3},{8,12},{12,8},{9,1... | collective-permute-start | bytes 442376 | tf_op jit(solution)/shard_map/ppermute | solution.py:284
  21.0 1.7 %collective-permute-start.8 = (bf16[4,144,128]{2,1,0:T(8,128)(2,1)S(1)}, bf16[4,144,128]{2,1,0:T(8,128)(2,1)S(1)}, u32[]{:S(2)}, u32[]{:S(2)}) collective-permute-start(bf16[4,144,128]{2,1,0:T(8,128)(2,1)S(1)} %pad_maximum_fusion.refs_0_), channel_id=1, source_target_pairs={{0,16},{8,24},{16,0},{24,8},{1,17},{9,25},{17,1},{25,9},{2,18},{10... | collective-permute-start | bytes 442376 | tf_op jit(solution)/shard_map/ppermute | solution.py:284
  26.3 1.6 collective-permute-done.8.refs_6_
  27.9 1.7 %collective-permute-start.16 = (bf16[4,144,128]{2,1,0:T(8,128)(2,1)S(1)}, bf16[4,144,128]{2,1,0:T(8,128)(2,1)S(1)}, u32[]{:S(2)}, u32[]{:S(2)}) collective-permute-start(bf16[4,144,128]{2,1,0:T(8,128)(2,1)S(1)} %collective-permute-done.10.refs_8_), channel_id=1, source_target_pairs={{0,16},{8,24},{16,0},{24,8},{1,17},{9,25},{17,1},{25,9},{2,18},{10... | collective-permute-start | bytes 442376 | tf_op jit(solution)/shard_map/ppermute | solution.py:284
  31.9 2.4 %collective-permute-start.15 = (bf16[4,144,128]{2,1,0:T(8,128)(2,1)S(1)}, bf16[4,144,128]{2,1,0:T(8,128)(2,1)S(1)}, u32[]{:S(2)}, u32[]{:S(2)}) collective-permute-start(bf16[4,144,128]{2,1,0:T(8,128)(2,1)S(1)} %collective-permute-done.14.refs_12_), channel_id=1, source_target_pairs={{0,4},{4,0},{1,5},{5,1},{2,6},{6,2},{3,7},{7,3},{8,12},{12,8},{9,1... | collective-permute-start | bytes 442376 | tf_op jit(solution)/shard_map/ppermute | solution.py:284
  36.8 3.6 %attend.1 = (bf16[128,256]{1,0:T(8,128)(2,1)S(1)}, bf16[1024,2048]{1,0:T(8,128)(2,1)S(1)}) custom-call(s32[17]{0:T(128)S(1)} %stack.65.place_ref, bf16[512,80]{1,0:T(8,128)(2,1)S(1)} %shard_map.118.query_ref, bf16[1024,2048]{1,0:T(8,128)(2,1)} %source_ref.1, bf16[4,144,128]{2,1,0:T(8,128)(2,1)S(1)} %pad_maximum_fusion.refs_0_, ...), custom_call_target="tpu_custom_call" | custom-call | tf_op jit(solution)/shard_map/attend/pallas_call | solution.py:159
  40.4 8.3 %all_to_all.15.att_ref = bf16[4,32,256]{2,1,0:T(8,128)(2,1)S(1)} all-to-all(bf16[4,32,256]{2,1,0:T(8,128)(2,1)S(1)} %bitcast.25), channel_id=1, replica_groups=mesh['z'=8,'y'=4,'c'=2,'tp'=4] {'tp'}, dimensions={0} | all-to-all | bytes 131072 | tf_op jit(solution)/shard_map/all_to_all | solution.py:320
  48.7 2.0 %shard_map.119 = (f32[32,2048]{1,0:T(8,128)S(1)}, bf16[64,2,2048]{2,1,0:T(2,128)(2,1)}) custom-call(bf16[4,32,256]{2,1,0:T(8,128)(2,1)S(1)} %all_to_all.15.att_ref, bf16[1024,2048]{1,0:T(8,128)(2,1)S(1)} %get-tuple-element.21.weight_ref, bf16[32,2048]{1,0:T(8,128)(2,1)S(1)} %copy-done, f32[1,2048]{1,0:T(1,128)S(1)} %bitcast.26, s32[2,32]{1,0:T(2,128)S(1)} %bitcast.27), custom_call_target="tpu_custom_call" | custom-call | tf_op jit(solution)/shard_map/pallas_call | solution.py:277
  50.7 11.6 %all-to-all-start.1 = ((bf16[64,2,2048]{2,1,0:T(2,128)(2,1)}), bf16[64,2,2048]{2,1,0:T(2,128)(2,1)S(1)}, u32[]{:S(2)}, u32[]{:S(2)}) async-start(bf16[64,2,2048]{2,1,0:T(2,128)(2,1)} %get-tuple-element.23), calls=%async_computation.1 | async-start | bytes 1048576 | tf_op jit(solution)/shard_map/all_to_all | solution.py:333
  62.6 2.4 %collective-permute-start.21 = (bf16[256,2048]{1,0:T(8,128)(2,1)}, bf16[256,2048]{1,0:T(8,128)(2,1)}, u32[]{:S(2)}, u32[]{:S(2)}) collective-permute-start(bf16[256,2048]{1,0:T(8,128)(2,1)} %bitcast.23.refs_2_), channel_id=1, source_target_pairs={{0,3},{1,0},{2,1},{3,2},{4,7},{5,4},{6,5},{7,6},{8,11},{9,8},{10,9... | collective-permute-start | bytes 3145736 | tf_op jit(solution)/shard_map/ppermute | solution.py:284
  65.0 14.9 %all-to-all-done.1.own = bf16[64,2,2048]{2,1,0:T(2,128)(2,1)S(1)} async-done(((bf16[64,2,2048]{2,1,0:T(2,128)(2,1)}), bf16[64,2,2048]{2,1,0:T(2,128)(2,1)S(1)}, u32[]{:S(2)}, u32[]{:S(2)}) %all-to-all-start.1) | async-done | bytes 524320 | tf_op jit(solution)/shard_map/all_to_all | solution.py:333
  80.7 2.4 %collective-permute-start.19 = (bf16[32,2,2048]{2,1,0:T(2,128)(2,1)S(1)}, bf16[32,2,2048]{2,1,0:T(2,128)(2,1)S(1)}, u32[]{:S(2)}, u32[]{:S(2)}) collective-permute-start(bf16[32,2,2048]{2,1,0:T(2,128)(2,1)S(1)} %get-tuple-element.35), channel_id=1, source_target_pairs={{0,3},{1,0},{2,1},{3,2},{4,7},{5,4},{6,5},{7,6},{8,11},{9,8},{10,9... | collective-permute-start | bytes 786440 | tf_op jit(solution)/shard_map/ppermute | solution.py:284
  83.1 5.7 %collective-permute-done.20.refs_3_ = bf16[256,2048]{1,0:T(8,128)(2,1)} collective-permute-done((bf16[256,2048]{1,0:T(8,128)(2,1)}, bf16[256,2048]{1,0:T(8,128)(2,1)}, u32[]{:S(2)}, u32[]{:S(2)}) %collective-permute-start.20) | collective-permute-done | bytes 1048608 | tf_op jit(solution)/shard_map/ppermute | solution.py:284
  88.8 3.0 %collective-permute-start.23 = (bf16[32,2,2048]{2,1,0:T(2,128)(2,1)S(1)}, bf16[32,2,2048]{2,1,0:T(2,128)(2,1)S(1)}, u32[]{:S(2)}, u32[]{:S(2)}) collective-permute-start(bf16[32,2,2048]{2,1,0:T(2,128)(2,1)S(1)} %get-tuple-element.36), channel_id=1, source_target_pairs={{0,3},{1,0},{2,1},{3,2},{4,7},{5,4},{6,5},{7,6},{8,11},{9,8},{10,9... | collective-permute-start | bytes 786440 | tf_op jit(solution)/shard_map/ppermute | solution.py:284
  91.8 24.4 %collective-permute-done.18.left0 = bf16[32,2,2048]{2,1,0:T(2,128)(2,1)S(1)} collective-permute-done((bf16[32,2,2048]{2,1,0:T(2,128)(2,1)S(1)}, bf16[32,2,2048]{2,1,0:T(2,128)(2,1)S(1)}, u32[]{:S(2)}, u32[]{:S(2)}) %collective-permute-start.18) | collective-permute-done | bytes 262176 | tf_op jit(solution)/shard_map/ppermute | solution.py:284
  116.1 2.7 %collective-permute-start.27 = (bf16[32,2,2048]{2,1,0:T(2,128)(2,1)S(1)}, bf16[32,2,2048]{2,1,0:T(2,128)(2,1)S(1)}, u32[]{:S(2)}, u32[]{:S(2)}) collective-permute-start(bf16[32,2,2048]{2,1,0:T(2,128)(2,1)S(1)} %collective-permute-done.19.right1), channel_id=1, source_target_pairs={{0,3},{1,0},{2,1},{3,2},{4,7},{5,4},{6,5},{7,6},{8,11},{9,8},{10,9... | collective-permute-start | bytes 786440 | tf_op jit(solution)/shard_map/ppermute | solution.py:284
  118.8 2.7 %near.1 = (bf16[128,256]{1,0:T(8,128)(2,1)S(1)}, bf16[64,256]{1,0:T(8,128)(2,1)S(1)}, bf16[64,256]{1,0:T(8,128)(2,1)S(1)}, bf16[2048,256]{1,0:T(8,128)(2,1)S(1)}...) custom-call(bf16[64,2,2048]{2,1,0:T(2,128)(2,1)S(1)} %all-to-all-don, ...), custom_call_target="tpu_custom_call" | custom-call | tf_op jit(solution)/shard_map/near/pallas_call | solution.py:228
  122.7 2.7 %collective-permute-start.25 = (bf16[128,256]{1,0:T(8,128)(2,1)S(1)}, bf16[128,256]{1,0:T(8,128)(2,1)S(1)}, u32[]{:S(2)}, u32[]{:S(2)}) collective-permute-start(bf16[128,256]{1,0:T(8,128)(2,1)S(1)} %get-tuple-element.30), channel_id=1, source_target_pairs={{0,3},{1,0},{2,1},{3,2},{4,7},{5,4},{6,5},{7,6},{8,11},{9,8},{10,9... | collective-permute-start | bytes 196616 | tf_op jit(solution)/shard_map/ppermute | solution.py:284
  125.4 2.0 %collective-permute-done.26.far0 = bf16[32,2,2048]{2,1,0:T(2,128)(2,1)S(1)} collective-permute-done((bf16[32,2,2048]{2,1,0:T(2,128)(2,1)S(1)}, bf16[32,2,2048]{2,1,0:T(2,128)(2,1)S(1)}, u32[]{:S(2)}, u32[]{:S(2)}) %collective-permute-start.26) | collective-permute-done | bytes 262176 | tf_op jit(solution)/shard_map/ppermute | solution.py:284
  129.8 2.8 %collective-permute-done.28.far_ref = bf16[128,256]{1,0:T(8,128)(2,1)S(1)} collective-permute-done((bf16[128,256]{1,0:T(8,128)(2,1)S(1)}, bf16[128,256]{1,0:T(8,128)(2,1)S(1)}, u32[]{:S(2)}, u32[]{:S(2)}) %collective-permute-start.28) | collective-permute-done | bytes 65568 | tf_op jit(solution)/shard_map/ppermute | solution.py:284
  132.9 30.6 %all_to_all.16.back_ref = bf16[64,2,2048]{2,1,0:T(2,128)(2,1)S(1)} all-to-all(bf16[64,2,2048]{2,1,0:T(2,128)(2,1)S(1)} %shard_map.123), channel_id=1, replica_groups=mesh['z'=8,'y'=4,'c'=2,'tp'=4] {'z','y','c'}, dimensions={0} | all-to-all | bytes 1048576 | tf_op jit(solution)/shard_map/all_to_all | solution.py:354
  (63 shorter events, 19.9 us)
Async XLA Ops:
  0.8 10.2 %collective-permute-start.2 = (bf16[144,128]{1,0:T(8,128)(2,1)S(1)}, bf16[144,128]{1,0:T(8,128)(2,1)S(1)}, u32[]{:S(2)}, u32[]{:S(2)}) collective-permute-start(bf16[144,128]{1,0:T(8,128)(2,1)S(1)} %pack.1), channel_id=1, source_target_pairs={{0,192},{32,224},{64,0},{96,32},{128,64},{160,96},{192,128},{224,1... | collective-permute-start | bytes 110600 | tf_op jit(solution)/shard_map/ppermute | solution.py:284
  7.8 6.7 %collective-permute-start.1 = (bf16[144,128]{1,0:T(8,128)(2,1)S(1)}, bf16[144,128]{1,0:T(8,128)(2,1)S(1)}, u32[]{:S(2)}, u32[]{:S(2)}) collective-permute-start(bf16[144,128]{1,0:T(8,128)(2,1)S(1)} %pack.1), channel_id=1, source_target_pairs={{0,128},{32,160},{64,192},{96,224},{128,0},{160,32},{192,64},{224,... | collective-permute-start | bytes 110600 | tf_op jit(solution)/shard_map/ppermute | solution.py:284
  14.5 8.2 %collective-permute-start.4 = (bf16[4,144,128]{2,1,0:T(8,128)(2,1)S(1)}, bf16[4,144,128]{2,1,0:T(8,128)(2,1)S(1)}, u32[]{:S(2)}, u32[]{:S(2)}) collective-permute-start(bf16[4,144,128]{2,1,0:T(8,128)(2,1)S(1)} %pad_maximum_fusion.refs_0_), channel_id=1, source_target_pairs={{0,8},{8,16},{16,24},{24,0},{1,9},{9,17},{17,25},{25,1},{2,10},{10... | collective-permute-start | bytes 442376 | tf_op jit(solution)/shard_map/ppermute | solution.py:284
  15.9 7.3 %collective-permute-start.6 = (bf16[4,144,128]{2,1,0:T(8,128)(2,1)S(1)}, bf16[4,144,128]{2,1,0:T(8,128)(2,1)S(1)}, u32[]{:S(2)}, u32[]{:S(2)}) collective-permute-start(bf16[4,144,128]{2,1,0:T(8,128)(2,1)S(1)} %pad_maximum_fusion.refs_0_), channel_id=1, source_target_pairs={{0,24},{8,0},{16,8},{24,16},{1,25},{9,1},{17,9},{25,17},{2,26},{10... | collective-permute-start | bytes 442376 | tf_op jit(solution)/shard_map/ppermute | solution.py:284
  18.1 6.7 %collective-permute-start.3 = (bf16[4,144,128]{2,1,0:T(8,128)(2,1)S(1)}, bf16[4,144,128]{2,1,0:T(8,128)(2,1)S(1)}, u32[]{:S(2)}, u32[]{:S(2)}) collective-permute-start(bf16[4,144,128]{2,1,0:T(8,128)(2,1)S(1)} %pad_maximum_fusion.refs_0_), channel_id=1, source_target_pairs={{0,4},{4,0},{1,5},{5,1},{2,6},{6,2},{3,7},{7,3},{8,12},{12,8},{9,1... | collective-permute-start | bytes 442376 | tf_op jit(solution)/shard_map/ppermute | solution.py:284
  21.0 6.9 %collective-permute-start.8 = (bf16[4,144,128]{2,1,0:T(8,128)(2,1)S(1)}, bf16[4,144,128]{2,1,0:T(8,128)(2,1)S(1)}, u32[]{:S(2)}, u32[]{:S(2)}) collective-permute-start(bf16[4,144,128]{2,1,0:T(8,128)(2,1)S(1)} %pad_maximum_fusion.refs_0_), channel_id=1, source_target_pairs={{0,16},{8,24},{16,0},{24,8},{1,17},{9,25},{17,1},{25,9},{2,18},{10... | collective-permute-start | bytes 442376 | tf_op jit(solution)/shard_map/ppermute | solution.py:284
  22.7 6.9 %collective-permute-start.5 = (bf16[4,144,128]{2,1,0:T(8,128)(2,1)S(1)}, bf16[4,144,128]{2,1,0:T(8,128)(2,1)S(1)}, u32[]{:S(2)}, u32[]{:S(2)}) collective-permute-start(bf16[4,144,128]{2,1,0:T(8,128)(2,1)S(1)} %collective-permute-done.4.refs_2_), channel_id=1, source_target_pairs={{0,4},{4,0},{1,5},{5,1},{2,6},{6,2},{3,7},{7,3},{8,12},{12,8},{9,1... | collective-permute-start | bytes 442376 | tf_op jit(solution)/shard_map/ppermute | solution.py:284
  23.2 8.0 %collective-permute-start.7 = (bf16[4,144,128]{2,1,0:T(8,128)(2,1)S(1)}, bf16[4,144,128]{2,1,0:T(8,128)(2,1)S(1)}, u32[]{:S(2)}, u32[]{:S(2)}) collective-permute-start(bf16[4,144,128]{2,1,0:T(8,128)(2,1)S(1)} %collective-permute-done.6.refs_4_), channel_id=1, source_target_pairs={{0,4},{4,0},{1,5},{5,1},{2,6},{6,2},{3,7},{7,3},{8,12},{12,8},{9,1... | collective-permute-start | bytes 442376 | tf_op jit(solution)/shard_map/ppermute | solution.py:284
  23.6 7.7 %collective-permute-start.12 = (bf16[4,144,128]{2,1,0:T(8,128)(2,1)S(1)}, bf16[4,144,128]{2,1,0:T(8,128)(2,1)S(1)}, u32[]{:S(2)}, u32[]{:S(2)}) collective-permute-start(bf16[4,144,128]{2,1,0:T(8,128)(2,1)S(1)} %collective-permute-done.10.refs_8_), channel_id=1, source_target_pairs={{0,8},{8,16},{16,24},{24,0},{1,9},{9,17},{17,25},{25,1},{2,10},{10... | collective-permute-start | bytes 442376 | tf_op jit(solution)/shard_map/ppermute | solution.py:284
  24.9 7.0 %collective-permute-start.14 = (bf16[4,144,128]{2,1,0:T(8,128)(2,1)S(1)}, bf16[4,144,128]{2,1,0:T(8,128)(2,1)S(1)}, u32[]{:S(2)}, u32[]{:S(2)}) collective-permute-start(bf16[4,144,128]{2,1,0:T(8,128)(2,1)S(1)} %collective-permute-done.10.refs_8_), channel_id=1, source_target_pairs={{0,24},{8,0},{16,8},{24,16},{1,25},{9,1},{17,9},{25,17},{2,26},{10... | collective-permute-start | bytes 442376 | tf_op jit(solution)/shard_map/ppermute | solution.py:284
  27.9 6.5 %collective-permute-start.16 = (bf16[4,144,128]{2,1,0:T(8,128)(2,1)S(1)}, bf16[4,144,128]{2,1,0:T(8,128)(2,1)S(1)}, u32[]{:S(2)}, u32[]{:S(2)}) collective-permute-start(bf16[4,144,128]{2,1,0:T(8,128)(2,1)S(1)} %collective-permute-done.10.refs_8_), channel_id=1, source_target_pairs={{0,16},{8,24},{16,0},{24,8},{1,17},{9,25},{17,1},{25,9},{2,18},{10... | collective-permute-start | bytes 442376 | tf_op jit(solution)/shard_map/ppermute | solution.py:284
  29.6 7.1 %collective-permute-start.11 = (bf16[4,144,128]{2,1,0:T(8,128)(2,1)S(1)}, bf16[4,144,128]{2,1,0:T(8,128)(2,1)S(1)}, u32[]{:S(2)}, u32[]{:S(2)}) collective-permute-start(bf16[4,144,128]{2,1,0:T(8,128)(2,1)S(1)} %collective-permute-done.10.refs_8_), channel_id=1, source_target_pairs={{0,4},{4,0},{1,5},{5,1},{2,6},{6,2},{3,7},{7,3},{8,12},{12,8},{9,1... | collective-permute-start | bytes 442376 | tf_op jit(solution)/shard_map/ppermute | solution.py:284
  50.7 29.3 %all-to-all-start.1 = ((bf16[64,2,2048]{2,1,0:T(2,128)(2,1)}), bf16[64,2,2048]{2,1,0:T(2,128)(2,1)S(1)}, u32[]{:S(2)}, u32[]{:S(2)}) async-start(bf16[64,2,2048]{2,1,0:T(2,128)(2,1)} %get-tuple-element.23), calls=%async_computation.1 | async-start | bytes 1048576 | tf_op jit(solution)/shard_map/all_to_all | solution.py:333
  62.3 26.5 %collective-permute-start.20 = (bf16[256,2048]{1,0:T(8,128)(2,1)}, bf16[256,2048]{1,0:T(8,128)(2,1)}, u32[]{:S(2)}, u32[]{:S(2)}) collective-permute-start(bf16[256,2048]{1,0:T(8,128)(2,1)} %bitcast.23.refs_2_), channel_id=1, source_target_pairs={{0,1},{1,2},{2,3},{3,0},{4,5},{5,6},{6,7},{7,4},{8,9},{9,10},{10,1... | collective-permute-start | bytes 3145736 | tf_op jit(solution)/shard_map/ppermute | solution.py:284
  62.6 26.1 %collective-permute-start.21 = (bf16[256,2048]{1,0:T(8,128)(2,1)}, bf16[256,2048]{1,0:T(8,128)(2,1)}, u32[]{:S(2)}, u32[]{:S(2)}) collective-permute-start(bf16[256,2048]{1,0:T(8,128)(2,1)} %bitcast.23.refs_2_), channel_id=1, source_target_pairs={{0,3},{1,0},{2,1},{3,2},{4,7},{5,4},{6,5},{7,6},{8,11},{9,8},{10,9... | collective-permute-start | bytes 3145736 | tf_op jit(solution)/shard_map/ppermute | solution.py:284
  65.0 64.8 %collective-permute-start.29 = (bf16[256,2048]{1,0:T(8,128)(2,1)}, bf16[256,2048]{1,0:T(8,128)(2,1)S(1)}, u32[]{:S(2)}, u32[]{:S(2)}) collective-permute-start(bf16[256,2048]{1,0:T(8,128)(2,1)} %bitcast.23.refs_2_), channel_id=1, source_target_pairs={{0,2},{1,3},{2,0},{3,1},{4,6},{5,7},{6,4},{7,5},{8,10},{9,11},{10,... | collective-permute-start | bytes 3145736 | tf_op jit(solution)/shard_map/ppermute | solution.py:284
  80.3 35.8 %collective-permute-start.18 = (bf16[32,2,2048]{2,1,0:T(2,128)(2,1)S(1)}, bf16[32,2,2048]{2,1,0:T(2,128)(2,1)S(1)}, u32[]{:S(2)}, u32[]{:S(2)}) collective-permute-start(bf16[32,2,2048]{2,1,0:T(2,128)(2,1)S(1)} %get-tuple-element.36), channel_id=1, source_target_pairs={{0,1},{1,2},{2,3},{3,0},{4,5},{5,6},{6,7},{7,4},{8,9},{9,10},{10,1... | collective-permute-start | bytes 786440 | tf_op jit(solution)/shard_map/ppermute | solution.py:284
  80.7 35.4 %collective-permute-start.19 = (bf16[32,2,2048]{2,1,0:T(2,128)(2,1)S(1)}, bf16[32,2,2048]{2,1,0:T(2,128)(2,1)S(1)}, u32[]{:S(2)}, u32[]{:S(2)}) collective-permute-start(bf16[32,2,2048]{2,1,0:T(2,128)(2,1)S(1)} %get-tuple-element.35), channel_id=1, source_target_pairs={{0,3},{1,0},{2,1},{3,2},{4,7},{5,4},{6,5},{7,6},{8,11},{9,8},{10,9... | collective-permute-start | bytes 786440 | tf_op jit(solution)/shard_map/ppermute | solution.py:284
  88.8 33.0 %collective-permute-start.22 = (bf16[32,2,2048]{2,1,0:T(2,128)(2,1)S(1)}, bf16[32,2,2048]{2,1,0:T(2,128)(2,1)S(1)}, u32[]{:S(2)}, u32[]{:S(2)}) collective-permute-start(bf16[32,2,2048]{2,1,0:T(2,128)(2,1)S(1)} %get-tuple-element.35), channel_id=1, source_target_pairs={{0,1},{1,2},{2,3},{3,0},{4,5},{5,6},{6,7},{7,4},{8,9},{9,10},{10,1... | collective-permute-start | bytes 786440 | tf_op jit(solution)/shard_map/ppermute | solution.py:284
  88.8 33.0 %collective-permute-start.23 = (bf16[32,2,2048]{2,1,0:T(2,128)(2,1)S(1)}, bf16[32,2,2048]{2,1,0:T(2,128)(2,1)S(1)}, u32[]{:S(2)}, u32[]{:S(2)}) collective-permute-start(bf16[32,2,2048]{2,1,0:T(2,128)(2,1)S(1)} %get-tuple-element.36), channel_id=1, source_target_pairs={{0,3},{1,0},{2,1},{3,2},{4,7},{5,4},{6,5},{7,6},{8,11},{9,8},{10,9... | collective-permute-start | bytes 786440 | tf_op jit(solution)/shard_map/ppermute | solution.py:284
  116.1 11.2 %collective-permute-start.26 = (bf16[32,2,2048]{2,1,0:T(2,128)(2,1)S(1)}, bf16[32,2,2048]{2,1,0:T(2,128)(2,1)S(1)}, u32[]{:S(2)}, u32[]{:S(2)}) collective-permute-start(bf16[32,2,2048]{2,1,0:T(2,128)(2,1)S(1)} %collective-permute-done.18.left0), channel_id=1, source_target_pairs={{0,1},{1,2},{2,3},{3,0},{4,5},{5,6},{6,7},{7,4},{8,9},{9,10},{10,1... | collective-permute-start | bytes 786440 | tf_op jit(solution)/shard_map/ppermute | solution.py:284
  116.1 11.2 %collective-permute-start.27 = (bf16[32,2,2048]{2,1,0:T(2,128)(2,1)S(1)}, bf16[32,2,2048]{2,1,0:T(2,128)(2,1)S(1)}, u32[]{:S(2)}, u32[]{:S(2)}) collective-permute-start(bf16[32,2,2048]{2,1,0:T(2,128)(2,1)S(1)} %collective-permute-done.19.right1), channel_id=1, source_target_pairs={{0,3},{1,0},{2,1},{3,2},{4,7},{5,4},{6,5},{7,6},{8,11},{9,8},{10,9... | collective-permute-start | bytes 786440 | tf_op jit(solution)/shard_map/ppermute | solution.py:284
  122.6 6.6 %collective-permute-start.24 = (bf16[128,256]{1,0:T(8,128)(2,1)S(1)}, bf16[128,256]{1,0:T(8,128)(2,1)S(1)}, u32[]{:S(2)}, u32[]{:S(2)}) collective-permute-start(bf16[128,256]{1,0:T(8,128)(2,1)S(1)} %get-tuple-element.29), channel_id=1, source_target_pairs={{0,1},{1,2},{2,3},{3,0},{4,5},{5,6},{6,7},{7,4},{8,9},{9,10},{10,1... | collective-permute-start | bytes 196616 | tf_op jit(solution)/shard_map/ppermute | solution.py:284
  122.7 6.5 %collective-permute-start.25 = (bf16[128,256]{1,0:T(8,128)(2,1)S(1)}, bf16[128,256]{1,0:T(8,128)(2,1)S(1)}, u32[]{:S(2)}, u32[]{:S(2)}) collective-permute-start(bf16[128,256]{1,0:T(8,128)(2,1)S(1)} %get-tuple-element.30), channel_id=1, source_target_pairs={{0,3},{1,0},{2,1},{3,2},{4,7},{5,4},{6,5},{7,6},{8,11},{9,8},{10,9... | collective-permute-start | bytes 196616 | tf_op jit(solution)/shard_map/ppermute | solution.py:284
  (12 other events, 217.4 us)

commit v5 on v4

--- a/solution.py
+++ b/solution.py
@@ -13,6 +13,7 @@
 HEAD = 64
 HEADS = 4
 ROW = 32
+TP_STEPS = (0, 2, 1, 3)
 D = 2048
 BLOCK = TOK + 16
 BF16_MAX = 3.3895313892515355e38
@@ -97,7 +98,7 @@
 
 def attend_kernel(count, place_ref, query_ref, source_ref, *refs):
     chunks, refs = refs[:count], refs[count:]
-    out_ref, target_ref, m_ref, acc_ref, sem = refs
+    outs, (target_ref, m_ref, acc_ref, done_ref, sem) = refs[:NT], refs[NT:]
     copy = pltpu.make_async_copy(source_ref, target_ref, sem)
     copy.start()
     queries = query_ref[...]
@@ -149,7 +150,10 @@
     for h in range(HEADS):
         here = slice(h * TOK, (h + 1) * TOK)
         done.append((acc_ref[here, 16:] / acc_ref[here, ones : ones + 1]).astype(BF16))
-    out_ref[...] = jnp.concatenate(done, axis=1)
+    done_ref[...] = jnp.concatenate(done, axis=1)
+    own_x = place_ref[1 + count]
+    for step, out_ref in zip(TP_STEPS, outs):
+        out_ref[...] = done_ref[pl.ds((own_x + step) % NT * ROW, ROW), :]
     copy.wait()
 
 
@@ -158,17 +162,16 @@
     total_rows = HEADS * TOK
     return pl.pallas_call(
         functools.partial(attend_kernel, len(chunks)),
-        out_shape=[
-            jax.ShapeDtypeStruct((TOK, HEADS * HEAD), BF16),
-            jax.ShapeDtypeStruct(weight.shape, weight.dtype),
-        ],
+        out_shape=[jax.ShapeDtypeStruct((ROW, HEADS * HEAD), BF16)] * NT
+        + [jax.ShapeDtypeStruct(weight.shape, weight.dtype)],
         in_specs=[pl.BlockSpec(memory_space=pltpu.SMEM), vmem]
         + [pl.BlockSpec(memory_space=pltpu.HBM)]
         + [vmem] * len(chunks),
-        out_specs=[vmem] * 2,
+        out_specs=[vmem] * (NT + 1),
         scratch_shapes=[
             pltpu.VMEM((total_rows, TOK), F32),
             pltpu.VMEM((total_rows, HEAD + 16), F32),
+            pltpu.VMEM((TOK, HEADS * HEAD), BF16),
             pltpu.SemaphoreType.DMA,
         ],
         compiler_params=PARAMS,
@@ -190,16 +193,35 @@
     return chosen & named0, chosen & named1
 
 
-def project_kernel(att_ref, weight_ref, residual_ref, gain_ref, routes_ref, stream_ref, rows_ref):
+def project_kernel(
+    place_ref, h0, h2, h1, h3, weight_ref, residual_ref, gain_ref, routes_ref, stream_ref, rows_ref
+):
     total = residual_ref[...].astype(F32)
-    both = jnp.concatenate([att_ref[x] for x in range(NT)], axis=1)
-    total = total + dot(both, weight_ref[...])
+    wide = HEADS * HEAD
+    for step, ref in zip(TP_STEPS, (h0, h2, h1, h3)):
+        begin = (place_ref[0] + NT - step) % NT * wide
+        total = total + dot(ref[...], weight_ref[pl.ds(begin, wide), :])
     stream_ref[...] = total
     mean_square = jnp.mean(total * total, axis=1, keepdims=True)
     normed = (total * lax.rsqrt(mean_square + 1e-06) * gain_ref[...]).astype(BF16)
     first, second = picks(routes_ref)
     pick = jnp.where(first | second, 1.0, 0.0).astype(BF16)
     rows_ref[...] = dot(pick, normed).astype(BF16).reshape(rows_ref.shape)
+
+
+def project(*args):
+    vmem = pl.BlockSpec(memory_space=pltpu.VMEM)
+    return pl.pallas_call(
+        project_kernel,
+        out_shape=[
+            jax.ShapeDtypeStruct((ROW, D), F32),
+            jax.ShapeDtypeStruct((TOK // 2, 2, D), BF16),
+        ],
+        in_specs=[pl.BlockSpec(memory_space=pltpu.SMEM)] + [vmem] * (len(args) - 1),
+        out_specs=[vmem] * 2,
+        compiler_params=PARAMS,
+        name="project",
+    )(*args)
 
 
 def hidden(rows, gate_ref, up_ref):
@@ -314,17 +336,19 @@
             for parity in (c, 1 - c):
                 seen = (y - step) % NY * NC + parity <= own_order
                 kinds.append(jnp.where(seen, 1, 0) if name == "first" else z % 2)
-    place = jnp.stack([z // 2] + kinds).astype(jnp.int32)
-    attended, out_w = attend(place, rows_of_q, out_weight, chunks)
-
-    heads = lax.all_to_all(attended.reshape(NT, ROW, -1), "tp", 0, 0, tiled=True)
-    far_source, _ = lax.optimization_barrier((down_own, heads))
+    x = lax.axis_index("tp")
+    place = jnp.stack([z // 2] + kinds + [x]).astype(jnp.int32)
+    *attended, out_w = attend(place, rows_of_q, out_weight, chunks)
+
+    heads = [attended[0]] + [
+        moved(part, "tp", step) for part, step in zip(attended[1:], TP_STEPS[1:])
+    ]
+    far_source = down_own
     down_far = moved(far_source, "tp", 2)
     routes_row = routes.T
-    stream, rows = call(
-        project_kernel,
-        [((ROW, D), F32), ((TOK // 2, 2, D), BF16)],
-        heads,
+    stream, rows = project(
+        x.reshape(1).astype(jnp.int32),
+        *heads,
         out_w,
         residual,
         norm_gain.reshape(1, D),

time: 165 us -> 163 us (0.988)
  starting transfers between devices: 56.5 us -> 65.5 us
  blocking collectives: 38.8 us -> 30.1 us
  waiting for transfers between devices: 55.1 us -> 53.1 us
    ppermute x29 -> x32, starting transfers between devices: 44.2 us -> 53.3 us  [moved(): return lax.ppermute(x, axis, [(i, (i + by) % size) for i in range(size)])]
    all_to_all x1 -> x0, blocking collectives: 8.29 us -> none  [shards(): lax.all_to_all(attended.reshape(NT, ROW, -1), 'tp', 0, 0, tiled=True)]
    pallas_call x0 -> x1, Pallas kernels: none -> 2.02 us  [project(): pl.pallas_call(project_kernel, out_shape=[jax.ShapeDtypeStruct((ROW, D),...]
    pallas_call x7 -> x6, Pallas kernels: 5.49 us -> 3.49 us  [call(): pl.pallas_call(kernel, out_shape=[jax.ShapeDtypeStruct(s, t) for s, t in...]
    ppermute x29 -> x32, waiting for transfers between devices: 40.1 us -> 39.7 us  [moved(): return lax.ppermute(x, axis, [(i, (i + by) % size) for i in range(size)])]
  transfers between devices with their start and end apart: 31 -> 34, of which waited for: 8 -> 10; matrix products, arithmetic and copies ran while one was open for 0% -> 0% of each run, Pallas kernels for 3% -> 3%
where the time goes in v5:
time: 163 us
  starting transfers between devices  65.5 us (40%)
  waiting for transfers between devices  53.1 us (33%)
  blocking collectives  30.1 us (18%)
  Pallas kernels  12.8 us (8%)
    ppermute x32, starting transfers between devices, moved(): return lax.ppermute(x, axis, [(i, (i + by) % size) for i in range(size)])  53.3 us
    ppermute x32, waiting for transfers between devices, moved(): return lax.ppermute(x, axis, [(i, (i + by) % size) for i in range(size)])  39.7 us
    all_to_all x1, blocking collectives, shards(): back = lax.all_to_all(expert_out, SP, 0, 0, tiled=True)  30.1 us
    all_to_all x1, waiting for transfers between devices, shards(): arrived = lax.all_to_all(rows, SP, 0, 0, tiled=True)  13.5 us
    all_to_all x1, starting transfers between devices, shards(): arrived = lax.all_to_all(rows, SP, 0, 0, tiled=True)  11.5 us
    pallas_call x1, Pallas kernels, attend(): pl.pallas_call(functools.partial(attend_kernel, len(chunks)), out_shape=[...  3.73 us
    pallas_call x6, Pallas kernels, call(): pl.pallas_call(kernel, out_shape=[jax.ShapeDtypeStruct(s, t) for s, t in...  3.49 us
  transfers between devices with their start and end apart: 34, of which 10 were waited for; matrix products, arithmetic and copies ran while one was open for 0% of the time, Pallas kernels for 3%

profile of v5, /device:TPU:1, one launch (start us, length us, event | category | flops | bytes accessed | tf_op | source)
XLA Modules:
  0.0 163.2 jit_solution(15201480156828578816)
XLA Ops:
  0.8 6.9 %collective-permute-start.2 = (bf16[144,128]{1,0:T(8,128)(2,1)S(1)}, bf16[144,128]{1,0:T(8,128)(2,1)S(1)}, u32[]{:S(2)}, u32[]{:S(2)}) collective-permute-start(bf16[144,128]{1,0:T(8,128)(2,1)S(1)} %pack.1), channel_id=1, source_target_pairs={{0,192},{32,224},{64,0},{96,32},{128,64},{160,96},{192,128},{224,1... | collective-permute-start | bytes 110600 | tf_op jit(solution)/shard_map/ppermute | solution.py:306
  8.7 2.3 %collective-permute-start = (bf16[144,128]{1,0:T(8,128)(2,1)S(1)}, bf16[144,128]{1,0:T(8,128)(2,1)S(1)}, u32[]{:S(2)}, u32[]{:S(2)}) collective-permute-start(bf16[144,128]{1,0:T(8,128)(2,1)S(1)} %pack.1), channel_id=1, source_target_pairs={{0,64},{32,96},{64,128},{96,160},{128,192},{160,224},{192,0},{224,... | collective-permute-start | bytes 110600 | tf_op jit(solution)/shard_map/ppermute | solution.py:306
  11.0 3.5 %collective-permute-done.1 = bf16[144,128]{1,0:T(8,128)(2,1)S(1)} collective-permute-done((bf16[144,128]{1,0:T(8,128)(2,1)S(1)}, bf16[144,128]{1,0:T(8,128)(2,1)S(1)}, u32[]{:S(2)}, u32[]{:S(2)}) %collective-permute-start.1) | collective-permute-done | bytes 36896 | tf_op jit(solution)/shard_map/ppermute | solution.py:306
  18.1 2.8 %collective-permute-start.3 = (bf16[4,144,128]{2,1,0:T(8,128)(2,1)S(1)}, bf16[4,144,128]{2,1,0:T(8,128)(2,1)S(1)}, u32[]{:S(2)}, u32[]{:S(2)}) collective-permute-start(bf16[4,144,128]{2,1,0:T(8,128)(2,1)S(1)} %pad_maximum_fusion.refs_0_), channel_id=1, source_target_pairs={{0,4},{4,0},{1,5},{5,1},{2,6},{6,2},{3,7},{7,3},{8,12},{12,8},{9,1... | collective-permute-start | bytes 442376 | tf_op jit(solution)/shard_map/ppermute | solution.py:306
  31.9 2.4 %collective-permute-start.15 = (bf16[4,144,128]{2,1,0:T(8,128)(2,1)S(1)}, bf16[4,144,128]{2,1,0:T(8,128)(2,1)S(1)}, u32[]{:S(2)}, u32[]{:S(2)}) collective-permute-start(bf16[4,144,128]{2,1,0:T(8,128)(2,1)S(1)} %collective-permute-done.14.refs_12_), channel_id=1, source_target_pairs={{0,4},{4,0},{1,5},{5,1},{2,6},{6,2},{3,7},{7,3},{8,12},{12,8},{9,1... | collective-permute-start | bytes 442376 | tf_op jit(solution)/shard_map/ppermute | solution.py:306
  36.8 3.7 %attend.1 = (bf16[32,256]{1,0:T(8,128)(2,1)S(1)}, bf16[32,256]{1,0:T(8,128)(2,1)S(1)}, bf16[32,256]{1,0:T(8,128)(2,1)S(1)}, bf16[32,256]{1,0:T(8,128)(2,1)S(1)}, bf16[1024,2048]{1,0:T(8,128)(2,1)S(1)}) custom-call(s32[18]{0:T(128)S(1)} %stack.66.place_ref, bf16[512,80]{1,0:T(8,128)(2,1)S(1)} %shard_map.118.query_ref, bf16[1024,2048]{1,0:T(8,128)(2,1)} %source_ref.1, ...), custom_call_target="tpu_custom_call" | custom-call | tf_op jit(solution)/shard_map/attend/pallas_call | solution.py:163
  40.5 2.8 %collective-permute-start.18 = (bf16[32,256]{1,0:T(8,128)(2,1)S(1)}, bf16[32,256]{1,0:T(8,128)(2,1)S(1)}, u32[]{:S(2)}, u32[]{:S(2)}) collective-permute-start(bf16[32,256]{1,0:T(8,128)(2,1)S(1)} %get-tuple-element.23), channel_id=1, source_target_pairs={{0,2},{1,3},{2,0},{3,1},{4,6},{5,7},{6,4},{7,5},{8,10},{9,11},{10,... | collective-permute-start | bytes 49160 | tf_op jit(solution)/shard_map/ppermute | solution.py:306
  43.6 2.4 %collective-permute-start.20 = (bf16[32,256]{1,0:T(8,128)(2,1)S(1)}, bf16[32,256]{1,0:T(8,128)(2,1)S(1)}, u32[]{:S(2)}, u32[]{:S(2)}) collective-permute-start(bf16[32,256]{1,0:T(8,128)(2,1)S(1)} %get-tuple-element.25), channel_id=1, source_target_pairs={{0,3},{1,0},{2,1},{3,2},{4,7},{5,4},{6,5},{7,6},{8,11},{9,8},{10,9... | collective-permute-start | bytes 49160 | tf_op jit(solution)/shard_map/ppermute | solution.py:306
  47.1 2.0 %project.1 = (f32[32,2048]{1,0:T(8,128)S(1)}, bf16[64,2,2048]{2,1,0:T(2,128)(2,1)}) custom-call(s32[1]{0:T(128)} %bitcast.place_ref, bf16[32,256]{1,0:T(8,128)(2,1)S(1)} %get-tuple-element.22.h0, bf16[32,256]{1,0:T(8,128)(2,1)S(1)} %collective-permute-done.18.h2, bf16[32,256]{1,0:T(8,128)(2,1)S(1)} %collective-permute-done.19.h1, ...), custom_call_target="tpu_custom_call" | custom-call | tf_op jit(solution)/shard_map/project/pallas_call | solution.py:214
  49.2 11.5 %all-to-all-start = ((bf16[64,2,2048]{2,1,0:T(2,128)(2,1)}), bf16[64,2,2048]{2,1,0:T(2,128)(2,1)S(1)}, u32[]{:S(2)}, u32[]{:S(2)}) async-start(bf16[64,2,2048]{2,1,0:T(2,128)(2,1)} %get-tuple-element.28), calls=%async_computation | async-start | bytes 1048576 | tf_op jit(solution)/shard_map/all_to_all | solution.py:357
  60.8 3.0 %collective-permute-start.24 = (bf16[256,2048]{1,0:T(8,128)(2,1)}, bf16[256,2048]{1,0:T(8,128)(2,1)}, u32[]{:S(2)}, u32[]{:S(2)}) collective-permute-start(bf16[256,2048]{1,0:T(8,128)(2,1)} %bitcast.23.refs_2_), channel_id=1, source_target_pairs={{0,3},{1,0},{2,1},{3,2},{4,7},{5,4},{6,5},{7,6},{8,11},{9,8},{10,9... | collective-permute-start | bytes 3145736 | tf_op jit(solution)/shard_map/ppermute | solution.py:306
  64.9 13.5 %all-to-all-done.own = bf16[64,2,2048]{2,1,0:T(2,128)(2,1)S(1)} async-done(((bf16[64,2,2048]{2,1,0:T(2,128)(2,1)}), bf16[64,2,2048]{2,1,0:T(2,128)(2,1)S(1)}, u32[]{:S(2)}, u32[]{:S(2)}) %all-to-all-start) | async-done | bytes 524320 | tf_op jit(solution)/shard_map/all_to_all | solution.py:357
  78.8 3.0 %collective-permute-start.22 = (bf16[32,2,2048]{2,1,0:T(2,128)(2,1)S(1)}, bf16[32,2,2048]{2,1,0:T(2,128)(2,1)S(1)}, u32[]{:S(2)}, u32[]{:S(2)}) collective-permute-start(bf16[32,2,2048]{2,1,0:T(2,128)(2,1)S(1)} %get-tuple-element.39), channel_id=1, source_target_pairs={{0,3},{1,0},{2,1},{3,2},{4,7},{5,4},{6,5},{7,6},{8,11},{9,8},{10,9... | collective-permute-start | bytes 786440 | tf_op jit(solution)/shard_map/ppermute | solution.py:306
  81.8 5.3 %collective-permute-done.23.refs_3_ = bf16[256,2048]{1,0:T(8,128)(2,1)} collective-permute-done((bf16[256,2048]{1,0:T(8,128)(2,1)}, bf16[256,2048]{1,0:T(8,128)(2,1)}, u32[]{:S(2)}, u32[]{:S(2)}) %collective-permute-start.23) | collective-permute-done | bytes 1048608 | tf_op jit(solution)/shard_map/ppermute | solution.py:306
  87.1 20.9 %collective-permute-done.24.refs_4_ = bf16[256,2048]{1,0:T(8,128)(2,1)} collective-permute-done((bf16[256,2048]{1,0:T(8,128)(2,1)}, bf16[256,2048]{1,0:T(8,128)(2,1)}, u32[]{:S(2)}, u32[]{:S(2)}) %collective-permute-start.24) | collective-permute-done | bytes 1048608 | tf_op jit(solution)/shard_map/ppermute | solution.py:306
  108.0 3.9 %collective-permute-start.26 = (bf16[32,2,2048]{2,1,0:T(2,128)(2,1)S(1)}, bf16[32,2,2048]{2,1,0:T(2,128)(2,1)S(1)}, u32[]{:S(2)}, u32[]{:S(2)}) collective-permute-start(bf16[32,2,2048]{2,1,0:T(2,128)(2,1)S(1)} %get-tuple-element.40), channel_id=1, source_target_pairs={{0,3},{1,0},{2,1},{3,2},{4,7},{5,4},{6,5},{7,6},{8,11},{9,8},{10,9... | collective-permute-start | bytes 786440 | tf_op jit(solution)/shard_map/ppermute | solution.py:306
  111.9 3.1 %collective-permute-done.21.left0 = bf16[32,2,2048]{2,1,0:T(2,128)(2,1)S(1)} collective-permute-done((bf16[32,2,2048]{2,1,0:T(2,128)(2,1)S(1)}, bf16[32,2,2048]{2,1,0:T(2,128)(2,1)S(1)}, u32[]{:S(2)}, u32[]{:S(2)}) %collective-permute-start.21) | collective-permute-done | bytes 262176 | tf_op jit(solution)/shard_map/ppermute | solution.py:306
  115.1 2.7 %collective-permute-start.30 = (bf16[32,2,2048]{2,1,0:T(2,128)(2,1)S(1)}, bf16[32,2,2048]{2,1,0:T(2,128)(2,1)S(1)}, u32[]{:S(2)}, u32[]{:S(2)}) collective-permute-start(bf16[32,2,2048]{2,1,0:T(2,128)(2,1)S(1)} %collective-permute-done.22.right1), channel_id=1, source_target_pairs={{0,3},{1,0},{2,1},{3,2},{4,7},{5,4},{6,5},{7,6},{8,11},{9,8},{10,9... | collective-permute-start | bytes 786440 | tf_op jit(solution)/shard_map/ppermute | solution.py:306
  117.8 2.7 %near.1 = (bf16[128,256]{1,0:T(8,128)(2,1)S(1)}, bf16[64,256]{1,0:T(8,128)(2,1)S(1)}, bf16[64,256]{1,0:T(8,128)(2,1)S(1)}, bf16[2048,256]{1,0:T(8,128)(2,1)S(1)}...) custom-call(bf16[64,2,2048]{2,1,0:T(2,128)(2,1)S(1)} %all-to-all-don, ...), custom_call_target="tpu_custom_call" | custom-call | tf_op jit(solution)/shard_map/near/pallas_call | solution.py:250
  122.2 2.1 %collective-permute-start.28 = (bf16[128,256]{1,0:T(8,128)(2,1)S(1)}, bf16[128,256]{1,0:T(8,128)(2,1)S(1)}, u32[]{:S(2)}, u32[]{:S(2)}) collective-permute-start(bf16[128,256]{1,0:T(8,128)(2,1)S(1)} %get-tuple-element.35), channel_id=1, source_target_pairs={{0,3},{1,0},{2,1},{3,2},{4,7},{5,4},{6,5},{7,6},{8,11},{9,8},{10,9... | collective-permute-start | bytes 196616 | tf_op jit(solution)/shard_map/ppermute | solution.py:306
  124.3 2.0 %collective-permute-done.29.far0 = bf16[32,2,2048]{2,1,0:T(2,128)(2,1)S(1)} collective-permute-done((bf16[32,2,2048]{2,1,0:T(2,128)(2,1)S(1)}, bf16[32,2,2048]{2,1,0:T(2,128)(2,1)S(1)}, u32[]{:S(2)}, u32[]{:S(2)}) %collective-permute-start.29) | collective-permute-done | bytes 262176 | tf_op jit(solution)/shard_map/ppermute | solution.py:306
  126.8 2.2 %collective-permute-start.31 = (bf16[128,256]{1,0:T(8,128)(2,1)S(1)}, bf16[128,256]{1,0:T(8,128)(2,1)S(1)}, u32[]{:S(2)}, u32[]{:S(2)}) collective-permute-start(bf16[128,256]{1,0:T(8,128)(2,1)S(1)} %shard_map.121), channel_id=1, source_target_pairs={{0,2},{1,3},{2,0},{3,1},{4,6},{5,7},{6,4},{7,5},{8,10},{9,11},{10,... | collective-permute-start | bytes 196616 | tf_op jit(solution)/shard_map/ppermute | solution.py:306
  129.6 1.9 %collective-permute-done.31.far_ref = bf16[128,256]{1,0:T(8,128)(2,1)S(1)} collective-permute-done((bf16[128,256]{1,0:T(8,128)(2,1)S(1)}, bf16[128,256]{1,0:T(8,128)(2,1)S(1)}, u32[]{:S(2)}, u32[]{:S(2)}) %collective-permute-start.31) | collective-permute-done | bytes 65568 | tf_op jit(solution)/shard_map/ppermute | solution.py:306
  131.8 30.1 %all_to_all.10.back_ref = bf16[64,2,2048]{2,1,0:T(2,128)(2,1)S(1)} all-to-all(bf16[64,2,2048]{2,1,0:T(2,128)(2,1)S(1)} %shard_map.122), channel_id=1, replica_groups=mesh['z'=8,'y'=4,'c'=2,'tp'=4] {'z','y','c'}, dimensions={0} | all-to-all | bytes 1048576 | tf_op jit(solution)/shard_map/all_to_all | solution.py:378
  (68 shorter events, 26.1 us)
Async XLA Ops:
  0.8 10.2 %collective-permute-start.2 = (bf16[144,128]{1,0:T(8,128)(2,1)S(1)}, bf16[144,128]{1,0:T(8,128)(2,1)S(1)}, u32[]{:S(2)}, u32[]{:S(2)}) collective-permute-start(bf16[144,128]{1,0:T(8,128)(2,1)S(1)} %pack.1), channel_id=1, source_target_pairs={{0,192},{32,224},{64,0},{96,32},{128,64},{160,96},{192,128},{224,1... | collective-permute-start | bytes 110600 | tf_op jit(solution)/shard_map/ppermute | solution.py:306
  7.8 6.7 %collective-permute-start.1 = (bf16[144,128]{1,0:T(8,128)(2,1)S(1)}, bf16[144,128]{1,0:T(8,128)(2,1)S(1)}, u32[]{:S(2)}, u32[]{:S(2)}) collective-permute-start(bf16[144,128]{1,0:T(8,128)(2,1)S(1)} %pack.1), channel_id=1, source_target_pairs={{0,128},{32,160},{64,192},{96,224},{128,0},{160,32},{192,64},{224,... | collective-permute-start | bytes 110600 | tf_op jit(solution)/shard_map/ppermute | solution.py:306
  14.5 8.2 %collective-permute-start.4 = (bf16[4,144,128]{2,1,0:T(8,128)(2,1)S(1)}, bf16[4,144,128]{2,1,0:T(8,128)(2,1)S(1)}, u32[]{:S(2)}, u32[]{:S(2)}) collective-permute-start(bf16[4,144,128]{2,1,0:T(8,128)(2,1)S(1)} %pad_maximum_fusion.refs_0_), channel_id=1, source_target_pairs={{0,8},{8,16},{16,24},{24,0},{1,9},{9,17},{17,25},{25,1},{2,10},{10... | collective-permute-start | bytes 442376 | tf_op jit(solution)/shard_map/ppermute | solution.py:306
  15.9 7.3 %collective-permute-start.6 = (bf16[4,144,128]{2,1,0:T(8,128)(2,1)S(1)}, bf16[4,144,128]{2,1,0:T(8,128)(2,1)S(1)}, u32[]{:S(2)}, u32[]{:S(2)}) collective-permute-start(bf16[4,144,128]{2,1,0:T(8,128)(2,1)S(1)} %pad_maximum_fusion.refs_0_), channel_id=1, source_target_pairs={{0,24},{8,0},{16,8},{24,16},{1,25},{9,1},{17,9},{25,17},{2,26},{10... | collective-permute-start | bytes 442376 | tf_op jit(solution)/shard_map/ppermute | solution.py:306
  18.1 6.7 %collective-permute-start.3 = (bf16[4,144,128]{2,1,0:T(8,128)(2,1)S(1)}, bf16[4,144,128]{2,1,0:T(8,128)(2,1)S(1)}, u32[]{:S(2)}, u32[]{:S(2)}) collective-permute-start(bf16[4,144,128]{2,1,0:T(8,128)(2,1)S(1)} %pad_maximum_fusion.refs_0_), channel_id=1, source_target_pairs={{0,4},{4,0},{1,5},{5,1},{2,6},{6,2},{3,7},{7,3},{8,12},{12,8},{9,1... | collective-permute-start | bytes 442376 | tf_op jit(solution)/shard_map/ppermute | solution.py:306
  21.0 6.9 %collective-permute-start.8 = (bf16[4,144,128]{2,1,0:T(8,128)(2,1)S(1)}, bf16[4,144,128]{2,1,0:T(8,128)(2,1)S(1)}, u32[]{:S(2)}, u32[]{:S(2)}) collective-permute-start(bf16[4,144,128]{2,1,0:T(8,128)(2,1)S(1)} %pad_maximum_fusion.refs_0_), channel_id=1, source_target_pairs={{0,16},{8,24},{16,0},{24,8},{1,17},{9,25},{17,1},{25,9},{2,18},{10... | collective-permute-start | bytes 442376 | tf_op jit(solution)/shard_map/ppermute | solution.py:306
  22.7 6.9 %collective-permute-start.5 = (bf16[4,144,128]{2,1,0:T(8,128)(2,1)S(1)}, bf16[4,144,128]{2,1,0:T(8,128)(2,1)S(1)}, u32[]{:S(2)}, u32[]{:S(2)}) collective-permute-start(bf16[4,144,128]{2,1,0:T(8,128)(2,1)S(1)} %collective-permute-done.4.refs_2_), channel_id=1, source_target_pairs={{0,4},{4,0},{1,5},{5,1},{2,6},{6,2},{3,7},{7,3},{8,12},{12,8},{9,1... | collective-permute-start | bytes 442376 | tf_op jit(solution)/shard_map/ppermute | solution.py:306
  23.2 8.0 %collective-permute-start.7 = (bf16[4,144,128]{2,1,0:T(8,128)(2,1)S(1)}, bf16[4,144,128]{2,1,0:T(8,128)(2,1)S(1)}, u32[]{:S(2)}, u32[]{:S(2)}) collective-permute-start(bf16[4,144,128]{2,1,0:T(8,128)(2,1)S(1)} %collective-permute-done.6.refs_4_), channel_id=1, source_target_pairs={{0,4},{4,0},{1,5},{5,1},{2,6},{6,2},{3,7},{7,3},{8,12},{12,8},{9,1... | collective-permute-start | bytes 442376 | tf_op jit(solution)/shard_map/ppermute | solution.py:306
  23.6 7.7 %collective-permute-start.12 = (bf16[4,144,128]{2,1,0:T(8,128)(2,1)S(1)}, bf16[4,144,128]{2,1,0:T(8,128)(2,1)S(1)}, u32[]{:S(2)}, u32[]{:S(2)}) collective-permute-start(bf16[4,144,128]{2,1,0:T(8,128)(2,1)S(1)} %collective-permute-done.10.refs_8_), channel_id=1, source_target_pairs={{0,8},{8,16},{16,24},{24,0},{1,9},{9,17},{17,25},{25,1},{2,10},{10... | collective-permute-start | bytes 442376 | tf_op jit(solution)/shard_map/ppermute | solution.py:306
  24.9 7.0 %collective-permute-start.14 = (bf16[4,144,128]{2,1,0:T(8,128)(2,1)S(1)}, bf16[4,144,128]{2,1,0:T(8,128)(2,1)S(1)}, u32[]{:S(2)}, u32[]{:S(2)}) collective-permute-start(bf16[4,144,128]{2,1,0:T(8,128)(2,1)S(1)} %collective-permute-done.10.refs_8_), channel_id=1, source_target_pairs={{0,24},{8,0},{16,8},{24,16},{1,25},{9,1},{17,9},{25,17},{2,26},{10... | collective-permute-start | bytes 442376 | tf_op jit(solution)/shard_map/ppermute | solution.py:306
  27.9 6.5 %collective-permute-start.16 = (bf16[4,144,128]{2,1,0:T(8,128)(2,1)S(1)}, bf16[4,144,128]{2,1,0:T(8,128)(2,1)S(1)}, u32[]{:S(2)}, u32[]{:S(2)}) collective-permute-start(bf16[4,144,128]{2,1,0:T(8,128)(2,1)S(1)} %collective-permute-done.10.refs_8_), channel_id=1, source_target_pairs={{0,16},{8,24},{16,0},{24,8},{1,17},{9,25},{17,1},{25,9},{2,18},{10... | collective-permute-start | bytes 442376 | tf_op jit(solution)/shard_map/ppermute | solution.py:306
  29.6 7.1 %collective-permute-start.11 = (bf16[4,144,128]{2,1,0:T(8,128)(2,1)S(1)}, bf16[4,144,128]{2,1,0:T(8,128)(2,1)S(1)}, u32[]{:S(2)}, u32[]{:S(2)}) collective-permute-start(bf16[4,144,128]{2,1,0:T(8,128)(2,1)S(1)} %collective-permute-done.10.refs_8_), channel_id=1, source_target_pairs={{0,4},{4,0},{1,5},{5,1},{2,6},{6,2},{3,7},{7,3},{8,12},{12,8},{9,1... | collective-permute-start | bytes 442376 | tf_op jit(solution)/shard_map/ppermute | solution.py:306
  49.2 29.2 %all-to-all-start = ((bf16[64,2,2048]{2,1,0:T(2,128)(2,1)}), bf16[64,2,2048]{2,1,0:T(2,128)(2,1)S(1)}, u32[]{:S(2)}, u32[]{:S(2)}) async-start(bf16[64,2,2048]{2,1,0:T(2,128)(2,1)} %get-tuple-element.28), calls=%async_computation | async-start | bytes 1048576 | tf_op jit(solution)/shard_map/all_to_all | solution.py:357
  60.7 26.4 %collective-permute-start.23 = (bf16[256,2048]{1,0:T(8,128)(2,1)}, bf16[256,2048]{1,0:T(8,128)(2,1)}, u32[]{:S(2)}, u32[]{:S(2)}) collective-permute-start(bf16[256,2048]{1,0:T(8,128)(2,1)} %bitcast.23.refs_2_), channel_id=1, source_target_pairs={{0,1},{1,2},{2,3},{3,0},{4,5},{5,6},{6,7},{7,4},{8,9},{9,10},{10,1... | collective-permute-start | bytes 3145736 | tf_op jit(solution)/shard_map/ppermute | solution.py:306
  60.8 47.3 %collective-permute-start.24 = (bf16[256,2048]{1,0:T(8,128)(2,1)}, bf16[256,2048]{1,0:T(8,128)(2,1)}, u32[]{:S(2)}, u32[]{:S(2)}) collective-permute-start(bf16[256,2048]{1,0:T(8,128)(2,1)} %bitcast.23.refs_2_), channel_id=1, source_target_pairs={{0,3},{1,0},{2,1},{3,2},{4,7},{5,4},{6,5},{7,6},{8,11},{9,8},{10,9... | collective-permute-start | bytes 3145736 | tf_op jit(solution)/shard_map/ppermute | solution.py:306
  63.8 65.8 %collective-permute-start.32 = (bf16[256,2048]{1,0:T(8,128)(2,1)}, bf16[256,2048]{1,0:T(8,128)(2,1)S(1)}, u32[]{:S(2)}, u32[]{:S(2)}) collective-permute-start(bf16[256,2048]{1,0:T(8,128)(2,1)} %bitcast.23.refs_2_), channel_id=1, source_target_pairs={{0,2},{1,3},{2,0},{3,1},{4,6},{5,7},{6,4},{7,5},{8,10},{9,11},{10,... | collective-permute-start | bytes 3145736 | tf_op jit(solution)/shard_map/ppermute | solution.py:306
  78.7 36.4 %collective-permute-start.21 = (bf16[32,2,2048]{2,1,0:T(2,128)(2,1)S(1)}, bf16[32,2,2048]{2,1,0:T(2,128)(2,1)S(1)}, u32[]{:S(2)}, u32[]{:S(2)}) collective-permute-start(bf16[32,2,2048]{2,1,0:T(2,128)(2,1)S(1)} %get-tuple-element.40), channel_id=1, source_target_pairs={{0,1},{1,2},{2,3},{3,0},{4,5},{5,6},{6,7},{7,4},{8,9},{9,10},{10,1... | collective-permute-start | bytes 786440 | tf_op jit(solution)/shard_map/ppermute | solution.py:306
  78.8 36.3 %collective-permute-start.22 = (bf16[32,2,2048]{2,1,0:T(2,128)(2,1)S(1)}, bf16[32,2,2048]{2,1,0:T(2,128)(2,1)S(1)}, u32[]{:S(2)}, u32[]{:S(2)}) collective-permute-start(bf16[32,2,2048]{2,1,0:T(2,128)(2,1)S(1)} %get-tuple-element.39), channel_id=1, source_target_pairs={{0,3},{1,0},{2,1},{3,2},{4,7},{5,4},{6,5},{7,6},{8,11},{9,8},{10,9... | collective-permute-start | bytes 786440 | tf_op jit(solution)/shard_map/ppermute | solution.py:306
  87.1 33.6 %collective-permute-start.25 = (bf16[32,2,2048]{2,1,0:T(2,128)(2,1)S(1)}, bf16[32,2,2048]{2,1,0:T(2,128)(2,1)S(1)}, u32[]{:S(2)}, u32[]{:S(2)}) collective-permute-start(bf16[32,2,2048]{2,1,0:T(2,128)(2,1)S(1)} %get-tuple-element.39), channel_id=1, source_target_pairs={{0,1},{1,2},{2,3},{3,0},{4,5},{5,6},{6,7},{7,4},{8,9},{9,10},{10,1... | collective-permute-start | bytes 786440 | tf_op jit(solution)/shard_map/ppermute | solution.py:306
  108.0 12.7 %collective-permute-start.26 = (bf16[32,2,2048]{2,1,0:T(2,128)(2,1)S(1)}, bf16[32,2,2048]{2,1,0:T(2,128)(2,1)S(1)}, u32[]{:S(2)}, u32[]{:S(2)}) collective-permute-start(bf16[32,2,2048]{2,1,0:T(2,128)(2,1)S(1)} %get-tuple-element.40), channel_id=1, source_target_pairs={{0,3},{1,0},{2,1},{3,2},{4,7},{5,4},{6,5},{7,6},{8,11},{9,8},{10,9... | collective-permute-start | bytes 786440 | tf_op jit(solution)/shard_map/ppermute | solution.py:306
  115.1 11.2 %collective-permute-start.29 = (bf16[32,2,2048]{2,1,0:T(2,128)(2,1)S(1)}, bf16[32,2,2048]{2,1,0:T(2,128)(2,1)S(1)}, u32[]{:S(2)}, u32[]{:S(2)}) collective-permute-start(bf16[32,2,2048]{2,1,0:T(2,128)(2,1)S(1)} %collective-permute-done.21.left0), channel_id=1, source_target_pairs={{0,1},{1,2},{2,3},{3,0},{4,5},{5,6},{6,7},{7,4},{8,9},{9,10},{10,1... | collective-permute-start | bytes 786440 | tf_op jit(solution)/shard_map/ppermute | solution.py:306
  115.1 11.2 %collective-permute-start.30 = (bf16[32,2,2048]{2,1,0:T(2,128)(2,1)S(1)}, bf16[32,2,2048]{2,1,0:T(2,128)(2,1)S(1)}, u32[]{:S(2)}, u32[]{:S(2)}) collective-permute-start(bf16[32,2,2048]{2,1,0:T(2,128)(2,1)S(1)} %collective-permute-done.22.right1), channel_id=1, source_target_pairs={{0,3},{1,0},{2,1},{3,2},{4,7},{5,4},{6,5},{7,6},{8,11},{9,8},{10,9... | collective-permute-start | bytes 786440 | tf_op jit(solution)/shard_map/ppermute | solution.py:306
  121.6 7.4 %collective-permute-start.27 = (bf16[128,256]{1,0:T(8,128)(2,1)S(1)}, bf16[128,256]{1,0:T(8,128)(2,1)S(1)}, u32[]{:S(2)}, u32[]{:S(2)}) collective-permute-start(bf16[128,256]{1,0:T(8,128)(2,1)S(1)} %get-tuple-element.34), channel_id=1, source_target_pairs={{0,1},{1,2},{2,3},{3,0},{4,5},{5,6},{6,7},{7,4},{8,9},{9,10},{10,1... | collective-permute-start | bytes 196616 | tf_op jit(solution)/shard_map/ppermute | solution.py:306
  122.2 6.8 %collective-permute-start.28 = (bf16[128,256]{1,0:T(8,128)(2,1)S(1)}, bf16[128,256]{1,0:T(8,128)(2,1)S(1)}, u32[]{:S(2)}, u32[]{:S(2)}) collective-permute-start(bf16[128,256]{1,0:T(8,128)(2,1)S(1)} %get-tuple-element.35), channel_id=1, source_target_pairs={{0,3},{1,0},{2,1},{3,2},{4,7},{5,4},{6,5},{7,6},{8,11},{9,8},{10,9... | collective-permute-start | bytes 196616 | tf_op jit(solution)/shard_map/ppermute | solution.py:306
  (15 other events, 225.1 us)
